TPU v7x, 512 devices: a whole 4x4x16 slice. The times are simulated.
512 devices in a mesh: sp: 64 (over z, y), tp: 8 (over x, core).
Axes of the slice: x: 4, y: 4, z: 16, core: 2. Of those that a mesh axis runs over, the one named last changes fastest.
Arguments:
- query_content: bfloat16 [12288, 1024], P('sp'), may hold values from -6 to 6
- query_rotary: bfloat16 [12288, 512], P('sp'), may hold values from -8 to 8
- latents: bfloat16 [12288, 256], P(('sp', 'tp')), may hold values from -6 to 6
- key_rotary: bfloat16 [12288, 64], P(('sp', 'tp')), may hold values from -8 to 8
- latent_gain: float32 [256], replicated, may hold values from 0.1 to 1.9
- key_up: bfloat16 [256, 1024], P(None, 'tp'), may hold values from -0.375 to 0.375
- value_up: bfloat16 [256, 1024], P(None, 'tp'), may hold values from -0.375 to 0.375
- out_proj: bfloat16 [1024, 2048], P(None, 'tp'), may hold values from -2 to 2
- residual: bfloat16 [12288, 2048], P('sp', 'tp'), may hold values from -6 to 6
- mixer_gain: float32 [2048], replicated, may hold values from 0.1 to 1.9
- gate_proj: bfloat16 [2048, 5632], P('sp', 'tp'), may hold values from -0.125 to 0.125
- up_proj: bfloat16 [2048, 5632], P('sp', 'tp'), may hold values from -0.125 to 0.125
- down_proj: bfloat16 [5632, 2048], P('tp', 'sp'), may hold values from -0.078125 to 0.078125
Outputs:
- layer_out: bfloat16 [12288, 2048], P('sp', 'tp')
All inputs are finite; a program needn't handle non-finite values.
Results may differ from a plain program's by a relative error of at most 0.011.
Values may be sent and summed in bfloat16 or wider, within the bound.
No kernel may reach another device: no remote copies, remote signals or barrier semaphores. Data moves between devices by JAX's collectives and lax.ppermute only.
A program may use at most 64 MiB of HBM per device.

v0:
```python
import math

import jax
import jax.numpy as jnp
from jax import lax
from jax.sharding import PartitionSpec as P

H = 8
DN = 128
DR = 64
DV = 128
SPAN = 64


epsilon = 1e-06
masked_score = -1e30
heads_per_step = 2


def sent_together(arrays, axis, dim, along):
    ends, at = ([], 0)
    for a in arrays[:-1]:
        at += a.shape[along]
        ends.append(at)
    both = jnp.concatenate(arrays, axis=along)
    return tuple(jnp.split(lax.all_gather(both, axis, axis=dim, tiled=True), ends, axis=along))


def in_one_piece(arrays, axis, split_dim, concat_dim, along):
    columns = [a.reshape(*a.shape[:along], -1) for a in arrays]
    both = jnp.concatenate(columns, axis=along)
    out, at, gathered = (
        lax.all_to_all(both, axis, split_axis=split_dim, concat_axis=concat_dim, tiled=True),
        0,
        [],
    )
    for a, column in zip(arrays, columns):
        slab = out[..., at : at + column.shape[along]]
        gathered.append(slab.reshape(*slab.shape[:along], *a.shape[along:]))
        at += column.shape[along]
    return tuple(gathered)


def in_order(tiles, dim):
    lengths = list(tiles.shape[1:])
    lengths[dim] *= tiles.shape[0]
    return jnp.moveaxis(tiles, 0, dim).reshape(lengths)


def from_everyone(x, axis):
    copies = jnp.broadcast_to(x, (lax.axis_size(axis), *x.shape))
    return lax.all_to_all(copies, axis, split_axis=0, concat_axis=0, tiled=True)


def collect(x, axis, dim):
    return in_order(from_everyone(x, axis), dim)


def rows_first(arrays, axis, dims):
    turned = [jnp.moveaxis(a, dim, 0) for a, dim in zip(arrays, dims)]
    both = jnp.concatenate([t.reshape(len(t), -1) for t in turned], axis=1)
    out, at, gathered = (lax.all_gather(both, axis, axis=0, tiled=True), 0, [])
    for t, dim in zip(turned, dims):
        slab = out[:, at : at + t[0].size].reshape(-1, *t.shape[1:])
        gathered.append(jnp.moveaxis(slab, 0, dim))
        at += t[0].size
    return tuple(gathered)


def cut_along(x, dim, length):
    before, after = (x.shape[:dim], x.shape[dim + 1 :])
    return jnp.moveaxis(x.reshape(*before, length, -1, *after), dim, 0)


def sum_at_owner(x, axis, dim):
    tiles = cut_along(x, dim, lax.axis_size(axis))
    arrived = lax.all_to_all(tiles, axis, split_axis=0, concat_axis=0, tiled=True)
    return arrived.astype(jnp.float32).sum(axis=0)


def norm_round(inputs, scales):
    widened = inputs.astype(jnp.float32)
    factor = lax.rsqrt(jnp.mean(widened * widened, axis=-1, keepdims=True) + epsilon)
    return (widened * factor * scales).astype(jnp.bfloat16)


def rotate(inputs, places):
    dimension = inputs.shape[-1]
    middle = dimension // 2
    inverse = 10000.0 ** (-jnp.arange(0, dimension, 2, dtype=jnp.float32) / dimension)
    angles = places.astype(jnp.float32)[:, None, None] * inverse[None, None, :]
    cosine_table = jnp.cos(angles)
    sine_table = jnp.sin(angles)
    widened = inputs.astype(jnp.float32)
    first_half = widened[..., :middle]
    second_half = widened[..., middle:]
    return jnp.concatenate(
        [
            first_half * cosine_table - second_half * sine_table,
            second_half * cosine_table + first_half * sine_table,
        ],
        axis=-1,
    ).astype(jnp.bfloat16)


def shards(
    query_content,
    query_rotary,
    latents,
    key_rotary,
    latent_gain,
    key_up,
    value_up,
    out_proj,
    residual,
    mixer_gain,
    gate_proj,
    up_proj,
    down_proj,
):
    query_rows = query_content.shape[0]
    tp_count = lax.axis_size("tp")
    sp_index = lax.axis_index("sp")
    tp_index = lax.axis_index("tp")
    latent_whole, turn_whole = sent_together((latents, key_rotary), "sp", 0, 1)
    key_weights, value_weights = sent_together((key_up, value_up), "tp", 1, 0)
    per_device = latents.shape[0]
    row_count = latent_whole.shape[0]
    position_index = jnp.arange(row_count, dtype=jnp.int32)
    key_places = (
        position_index // per_device * tp_count + tp_index
    ) * per_device + position_index % per_device
    query_places = sp_index * query_rows + jnp.arange(query_rows, dtype=jnp.int32)
    normed = norm_round(latent_whole, latent_gain)
    key_turned = rotate(turn_whole[:, None, :], key_places)[:, 0, :]
    query_turned = rotate(query_rotary.reshape(query_rows, H, DR), query_places)
    allowed = (key_places[None, :] // SPAN <= query_places[:, None] // SPAN)[:, None, :]
    groups = H // heads_per_step
    score_scale = 1.0 / math.sqrt(DN + DR)

    def by_group(inputs):
        shaped = inputs.reshape((inputs.shape[0], groups, heads_per_step) + inputs.shape[2:])
        return jnp.moveaxis(shaped, 1, 0)

    def weight_group(weights, width):
        return jnp.moveaxis(weights.reshape(weights.shape[0], groups, heads_per_step * width), 1, 0)

    def attend(inputs):
        contents, turned, key_weight, value_weight = inputs
        key_rows = jnp.dot(normed, key_weight, preferred_element_type=jnp.float32).astype(
            jnp.bfloat16
        )
        value_rows = jnp.dot(normed, value_weight, preferred_element_type=jnp.float32).astype(
            jnp.bfloat16
        )
        key_rows = key_rows.reshape(row_count, heads_per_step, DN)
        value_rows = value_rows.reshape(row_count, heads_per_step, DV)
        scores = (
            jnp.einsum("qhd,khd->qhk", contents, key_rows, preferred_element_type=jnp.float32)
            + jnp.einsum("qhr,kr->qhk", turned, key_turned, preferred_element_type=jnp.float32)
        ) * score_scale
        highest = jnp.max(jnp.where(allowed, scores, masked_score), axis=-1)
        weights = jnp.where(allowed, jnp.exp(scores - highest[..., None]), 0.0)
        weight_sum = jnp.sum(weights, axis=-1)
        weighted = jnp.einsum(
            "qhk,khv->qhv",
            weights.astype(jnp.bfloat16),
            value_rows,
            preferred_element_type=jnp.float32,
        )
        return (highest, weight_sum, weighted)

    highest, weight_sum, weighted = lax.map(
        attend,
        (
            by_group(query_content.reshape(query_rows, H, DN)),
            by_group(query_turned),
            weight_group(key_weights, DN),
            weight_group(value_weights, DV),
        ),
    )
    highest = jnp.moveaxis(highest, 0, 1).reshape(query_rows, H)
    weight_sum = jnp.moveaxis(weight_sum, 0, 1).reshape(query_rows, H)
    weighted = jnp.moveaxis(weighted, 0, 1).reshape(query_rows, H, DV)
    high_parts, sum_parts, acc_parts = in_one_piece(
        (highest[None], weight_sum[None], weighted[None]), "tp", 2, 0, 3
    )
    overall = jnp.max(high_parts, axis=0)
    factor = jnp.exp(high_parts - overall)
    own_heads = (
        jnp.sum(factor[..., None] * acc_parts, axis=0)
        / jnp.sum(factor * sum_parts, axis=0)[..., None]
    ).astype(jnp.bfloat16)
    attended = collect(own_heads.reshape(query_rows, -1), "tp", 1)
    mixed_rows = (
        residual.astype(jnp.float32)
        + jnp.dot(attended, out_proj, preferred_element_type=jnp.float32)
    ).astype(jnp.bfloat16)
    whole_rows = collect(mixed_rows, "tp", 1)
    normed_rows = norm_round(whole_rows, mixer_gain)
    gate_whole, up_whole, down_whole = rows_first((gate_proj, up_proj, down_proj), "sp", (0, 0, 1))
    hidden = (
        jax.nn.silu(jnp.dot(normed_rows, gate_whole, preferred_element_type=jnp.float32))
        * jnp.dot(normed_rows, up_whole, preferred_element_type=jnp.float32)
    ).astype(jnp.bfloat16)
    partial_value = jnp.dot(hidden, down_whole, preferred_element_type=jnp.float32)
    mixer_out = sum_at_owner(partial_value.astype(jnp.bfloat16), "tp", 1)
    return (mixed_rows.astype(jnp.float32) + mixer_out).astype(jnp.bfloat16)


def solution(mesh):
    return jax.shard_map(
        shards,
        mesh=mesh,
        in_specs=(
            P("sp", None),
            P("sp", None),
            P(("sp", "tp"), None),
            P(("sp", "tp"), None),
            P(),
            P(None, "tp"),
            P(None, "tp"),
            P(None, "tp"),
            P("sp", "tp"),
            P(),
            P("sp", "tp"),
            P("sp", "tp"),
            P("tp", "sp"),
        ),
        out_specs=P("sp", "tp"),
        check_vma=False,
    )
```

profile of v0, /device:TPU:1, one launch (start us, length us, event | category | flops | bytes accessed | tf_op | source)
XLA Modules:
  0.0 239.9 jit_solution(4656235675163388719)
XLA Ops:
  6.5 1.0 copy.95
  7.5 0.9 copy.96
  8.5 0.7 pad_maximum_fusion.2
  9.3 1.6 concatenate.41
  11.0 1.1 copy.97
  12.1 86.9 %all_gather.10 = bf16[1536,320]{1,0:T(8,128)(2,1)S(1)} all-gather(bf16[24,320]{1,0:T(8,128)(2,1)S(1)} %pad_maximum_fusion.3), channel_id=1, replica_groups=mesh['sp'=64,'tp'=8] {'sp'}, dimensions={0}, use_global_device_ids=true | all-gather | bytes 998400 | tf_op jit(solution)/shard_map/all_gather | solution.py:26
  99.9 0.3 fusion.36
  100.3 0.8 fusion.67
  101.4 1.3 fusion.87
  102.7 17.9 %while.15 = (s32[]{:T(128)}, f32[4,192,2]{1,2,0:T(2,128)S(1)}, f32[4,192,2]{1,2,0:T(2,128)S(1)}, f32[4,192,2,128]{3,1,2,0:T(8,128)}, bf16[4,256,256]{1,2,0:T(8,1...) while((s32[]{:T(128)}, f32[4,192,2]{1,2,0:T(2,128)S(1)}, ...), condition=%wide.region_4.5_spmd.clone, body=%wide.region_1.4_spmd.clone.sunk | while | flops 787119360 | bytes 18732432 | solution.py:173
  102.7 0.4 convolution_convert_fusion.4
  103.2 0.4 convolution_bitcast_fusion.2
  103.9 0.9 select_reduce_fusion.2
  104.8 0.4 convolution_convert_fusion.5
  105.2 1.2 fusion.111
  106.4 0.7 fusion.110
  107.2 0.4 convolution_convert_fusion.4
  107.7 0.4 convolution_bitcast_fusion.2
  108.4 0.9 select_reduce_fusion.2
  109.2 0.4 convolution_convert_fusion.5
  109.7 1.2 fusion.111
  110.9 0.7 fusion.110
  111.6 0.4 convolution_convert_fusion.4
  112.1 0.5 convolution_bitcast_fusion.2
  112.8 0.9 select_reduce_fusion.2
  113.7 0.4 convolution_convert_fusion.5
  114.1 1.2 fusion.111
  115.4 0.7 fusion.110
  116.1 0.4 convolution_convert_fusion.4
  116.6 0.4 convolution_bitcast_fusion.2
  117.3 0.9 select_reduce_fusion.2
  118.2 0.4 convolution_convert_fusion.5
  118.6 1.3 fusion.111
  119.8 0.7 fusion.110
  120.6 0.7 reshape_broadcast_in_dim_reshape.8
  121.3 1.6 reshape_broadcast_in_dim_reshape.9
  122.9 2.2 pad_maximum_fusion
  125.1 1.1 copy.104
  126.2 42.9 %all_to_all.33 = f32[1,192,8,130]{1,0,3,2:T(1,128)S(1)} all-to-all(f32[1,192,8,130]{1,0,3,2:T(1,128)S(1)} %copy.104), channel_id=1, replica_groups=mesh['sp'=64,'tp'=8] {'tp'}, dimensions={2} | all-to-all | bytes 1597440 | tf_op jit(solution)/shard_map/all_to_all | solution.py:33
  169.2 0.3 fusion.49
  169.9 11.0 %all_to_all.34 = bf16[8,192,128]{2,1,0:T(8,128)(2,1)S(1)} all-to-all(bf16[8,192,128]{2,1,0:T(8,128)(2,1)S(1)} %broadcast_in_dim.57), channel_id=1, replica_groups=mesh['sp'=64,'tp'=8] {'tp'}, dimensions={0} | all-to-all | bytes 786432 | tf_op jit(solution)/shard_map/all_to_all | solution.py:52
  180.8 0.3 fusion.48
  181.2 15.4 %all_to_all.35 = bf16[8,192,256]{2,1,0:T(8,128)(2,1)S(1)} all-to-all(bf16[8,192,256]{2,1,0:T(8,128)(2,1)S(1)} %broadcast_in_dim.58), channel_id=1, replica_groups=mesh['sp'=64,'tp'=8] {'tp'}, dimensions={0} | all-to-all | bytes 1572864 | tf_op jit(solution)/shard_map/all_to_all | solution.py:52
  197.2 1.7 all-gather.5.cloned.1.call-done
  198.9 3.6 %fusion.31 = f32[192,704]{1,0:T(8,128)} fusion(bf16[2048,2112]{1,0:T(8,128)(2,1)} %all-gather.5.cloned.1.call-done, f32[192,2048]{1,0:T(8,128)S(1)} %bitcast.156, f32[2048]{0:T(1024)S(1)} %copy-done.6, f32[192]{0:T(256)S(1)} %add_rsqrt_fusion.1), kind=kOutput, calls=%fused_computation.36 | convolution fusion | flops 554827776 | bytes 5268224 | tf_op jit(solution)/shard_map/dot_general | solution.py:203
  202.5 5.5 %fusion.33 = bf16[192,2048]{1,0:T(8,128)(2,1)S(1)} fusion(bf16[2048,2112]{1,0:T(8,128)(2,1)} %all-gather.5.cloned.1.call-done, f32[192,704]{1,0:T(8,128)} %fusion.31, f32[192,2048]{1,0:T(8,128)S(1)} %bitcast.157, f32[2048]{0:T(1024)S(1)} %copy-done.6, f32[192]{0:T(256)S(1)} %add_rsqrt_fusion.1), kind=kOutput, calls=%fused_computation.38 | convolution fusion | flops 1109680128 | bytes 9249536 | tf_op jit(solution)/shard_map/dot_general | solution.py:206
  208.1 24.2 %all_to_all.36 = bf16[8,192,256]{2,1,0:T(8,128)(2,1)S(1)} all-to-all(bf16[8,192,256]{2,1,0:T(8,128)(2,1)S(1)} %bitcast.152), channel_id=1, replica_groups=mesh['sp'=64,'tp'=8] {'tp'}, dimensions={0} | all-to-all | bytes 1572864 | tf_op jit(solution)/shard_map/all_to_all | solution.py:77
  232.4 0.7 add_convert_fusion.1
  (65 shorter events, 3.8 us)
Async XLA Ops:
  6.5 174.3 %copy-start = (bf16[1024,256]{1,0:T(8,128)(2,1)S(1)}, bf16[1024,256]{1,0:T(8,128)(2,1)}, u32[]{:S(2)}) copy-start(bf16[1024,256]{1,0:T(8,128)(2,1)} %param.22) | copy-start | bytes 1572868
  6.5 5.5 %copy-start.2 = (bf16[24,256]{1,0:T(8,128)(2,1)S(1)}, bf16[24,256]{1,0:T(8,128)(2,1)}, u32[]{:S(2)}) copy-start(bf16[24,256]{1,0:T(8,128)(2,1)} %param.17) | copy-start | bytes 36868
  6.5 5.5 %copy-start.3 = (bf16[24,64]{1,0:T(8,128)(2,1)S(1)}, bf16[24,64]{1,0:T(8,128)(2,1)}, u32[]{:S(2)}) copy-start(bf16[24,64]{1,0:T(8,128)(2,1)} %param.18) | copy-start | bytes 9220
  6.5 94.9 %all-gather.3.cloned.1.call-start = ((), (), s32[]{:S(2)}) async-start(), calls=%async_computation.4 | async-start | bytes 1179648 | tf_op jit(solution)/shard_map/all_gather | solution.py:26
  9.2 189.7 %all-gather.5.cloned.1.call-start = ((), (), s32[]{:S(2)}) async-start(), calls=%async_computation.5 | async-start | bytes 9052160 | tf_op jit(solution)/shard_map/all_gather | solution.py:62
  12.0 87.3 %copy-start.1 = (bf16[192,1024]{1,0:T(8,128)(2,1)S(1)}, bf16[192,1024]{1,0:T(8,128)(2,1)}, u32[]{:S(2)}) copy-start(bf16[192,1024]{1,0:T(8,128)(2,1)} %param.15) | copy-start | bytes 1179652
  99.9 1.2 copy-start.4
  169.2 11.7 %copy-start.5 = (bf16[192,256]{1,0:T(8,128)(2,1)S(1)}, bf16[192,256]{1,0:T(8,128)(2,1)}, u32[]{:S(2)}) copy-start(bf16[192,256]{1,0:T(8,128)(2,1)} %param.23) | copy-start | bytes 294916
  196.7 2.2 copy-start.6
Sparse Core Ops, SparseCore 0:
  9.5 36.7 all-gather.2
  49.2 149.6 all-gather.4
where the time goes:
time: 240 us
  blocking collectives  180 us (75%)
  matrix products  22.9 us (10%)
  between operations  13.8 us (6%)
  local copies, waits for them, and re-layouts  10.6 us (4%)
  other arithmetic  10.2 us (4%)
    all_gather x1, blocking collectives, sent_together(): lax.all_gather(both, axis, axis=dim, tiled=True)  86.9 us
    all_to_all x1, blocking collectives, in_one_piece(): lax.all_to_all(both, axis, split_axis=split_dim, concat_axis=concat_dim,...  42.9 us
    all_to_all x2, blocking collectives, from_everyone(): return lax.all_to_all(copies, axis, split_axis=0, concat_axis=0, tiled=True)  26.4 us
    all_to_all x1, blocking collectives, sum_at_owner(): lax.all_to_all(tiles, axis, split_axis=0, concat_axis=0, tiled=True)  24.2 us
    dot_general x1, matrix products, shards(): jnp.dot(hidden, down_whole, preferred_element_type=jnp.float32)  5.52 us
    dot_general x4, matrix products, attend(): jnp.einsum('qhk,khv->qhv', weights.astype(jnp.bfloat16), value_rows, pref...  4.98 us
  transfers between devices with their start and end apart: 2, of which 1 were waited for; matrix products, arithmetic and copies ran while one was open for 13% of the time, Pallas kernels for 0%

commit v1 on v0

v1 whole, which is shorter than its diff:
```python
import math

import jax
import jax.numpy as jnp
from jax import lax
from jax.experimental import pallas as pl
from jax.experimental.pallas import tpu as pltpu
from jax.sharding import Mesh, PartitionSpec as P

H = 8
DN = 128
DR = 64
DV = 128
SPAN = 64
NZ, NY, NX, NC = 16, 4, 4, 2
TOK = 192
HALF = TOK // 2
KEYS = 1536
PAD = 208

epsilon = 1e-06
masked_score = -1e30
LOG2E = 1.4426950408889634
VMEM_LIMIT = 60 * 1024 * 1024


def norm_round(inputs, scales):
    widened = inputs.astype(jnp.float32)
    factor = lax.rsqrt(jnp.mean(widened * widened, axis=-1, keepdims=True) + epsilon)
    return (widened * factor * scales).astype(jnp.bfloat16)


def tables(places):
    inverse = 10000.0 ** (-jnp.arange(0, DR, 2, dtype=jnp.float32) / DR)
    angles = places.astype(jnp.float32)[:, None] * inverse[None, :]
    return jnp.cos(angles), jnp.sin(angles)


def rotate_rows(inputs, places):
    cosine, sine = tables(places)
    widened = inputs.astype(jnp.float32)
    a, b = widened[:, : DR // 2], widened[:, DR // 2 :]
    return jnp.concatenate([a * cosine - b * sine, b * cosine + a * sine], axis=-1).astype(
        jnp.bfloat16
    )


def attend_kernel(q_ref, qr_ref, cos_ref, sin_ref, lat_ref, seg_ref, w_ref, out_ref, key_ref):
    scale = LOG2E / math.sqrt(DN + DR)
    step = pl.program_id(0)

    @pl.when(step == 0)
    def _():
        lane = lax.broadcasted_iota(jnp.int32, (KEYS, 64), 1)
        mask = jnp.where(seg_ref[:, :64] > lane, masked_score, 0.0)
        mask = jnp.where(lane < TOK // SPAN, mask, 0.0).astype(jnp.bfloat16)
        key_ref[:, DN : DN + DR] = lat_ref[:, 256:320]
        key_ref[:, DN + DR :] = mask

    turned = qr_ref[...].astype(jnp.float32)
    lane = lax.broadcasted_iota(jnp.int32, turned.shape, 1)
    first = lane % DR < DR // 2
    swapped = jnp.where(
        first, pltpu.roll(turned, 2 * DR - DR // 2, 1), pltpu.roll(turned, DR // 2, 1)
    )
    signed = jnp.where(first, -swapped, swapped)
    turned = (turned * cos_ref[...] + signed * sin_ref[...]).astype(jnp.bfloat16)
    row = lax.broadcasted_iota(jnp.int32, (TOK, 64), 0)
    col = lax.broadcasted_iota(jnp.int32, (TOK, 64), 1)
    segment = jnp.where(row // SPAN == col, 1.0, 0.0).astype(jnp.bfloat16)
    normed = lat_ref[:, :256]
    keys = jnp.dot(normed, w_ref[:256], preferred_element_type=jnp.float32).astype(jnp.bfloat16)
    values = jnp.dot(normed, w_ref[256:], preferred_element_type=jnp.float32).astype(jnp.bfloat16)
    ones = jnp.ones((KEYS, 128), jnp.bfloat16)
    r128 = lax.broadcasted_iota(jnp.int32, (128, 128), 0)
    c128 = lax.broadcasted_iota(jnp.int32, (128, 128), 1)
    r64 = lax.broadcasted_iota(jnp.int32, (64, 128), 0)
    c64 = lax.broadcasted_iota(jnp.int32, (64, 128), 1)
    for h in range(2):
        key_ref[:, :DN] = keys[:, h * DN : (h + 1) * DN]
        query = jnp.concatenate(
            [q_ref[:, h * DN : (h + 1) * DN], turned[:, h * DR : (h + 1) * DR], segment], axis=1
        )
        scores = lax.dot_general(
            query, key_ref[...], (((1,), (1,)), ((), ())), preferred_element_type=jnp.float32
        )
        highest = jnp.max(scores, axis=1, keepdims=True) * scale
        weights = jnp.exp2(scores * scale - highest).astype(jnp.bfloat16)
        both = jnp.concatenate([values[:, h * DV : (h + 1) * DV], ones], axis=1)
        sums = jnp.dot(weights, both, preferred_element_type=jnp.float32)
        norm = sums[:, DV:]
        out_ref[h, :TOK, :] = (sums[:, :DV] / norm).astype(jnp.bfloat16)
        level = highest + jnp.log2(norm)
        upper = jnp.sum(jnp.where(r128 == c128, level[:128], 0.0), axis=0, keepdims=True)
        lower = jnp.sum(jnp.where(r64 == c64, level[128:], 0.0), axis=0, keepdims=True)
        rest = jnp.concatenate([upper, lower], axis=0)
        rows = []
        for _ in range(3):
            part = rest.astype(jnp.bfloat16).astype(jnp.float32)
            rows.append(part)
            rest = rest - part
        rows.append(jnp.zeros((PAD - TOK - 6, 128), jnp.float32))
        out_ref[h, TOK:, :] = jnp.concatenate(rows, axis=0).astype(jnp.bfloat16)


def attend(query, query_rotary, cosine, sine, lat, seg, weights):
    return pl.pallas_call(
        attend_kernel,
        grid=(H // 2,),
        in_specs=[
            pl.BlockSpec((TOK, 2 * DN), lambda i: (0, i)),
            pl.BlockSpec((TOK, 2 * DR), lambda i: (0, i)),
            pl.BlockSpec((TOK, 2 * DR), lambda i: (0, 0)),
            pl.BlockSpec((TOK, 2 * DR), lambda i: (0, 0)),
            pl.BlockSpec((KEYS, 320), lambda i: (0, 0)),
            pl.BlockSpec((KEYS, 128), lambda i: (0, 0)),
            pl.BlockSpec((512, 2 * DN), lambda i: (0, i)),
        ],
        out_specs=pl.BlockSpec((2, PAD, 128), lambda i: (i, 0, 0)),
        out_shape=jax.ShapeDtypeStruct((H, PAD, 128), jnp.bfloat16),
        scratch_shapes=[pltpu.VMEM((KEYS, 256), jnp.bfloat16)],
        compiler_params=pltpu.CompilerParams(
            dimension_semantics=("arbitrary",), vmem_limit_bytes=VMEM_LIMIT
        ),
        cost_estimate=pl.CostEstimate(
            flops=3_000_000_000, bytes_accessed=4_000_000, transcendentals=2_400_000
        ),
        name="attend",
    )(query, query_rotary, cosine, sine, lat, seg, weights)


def merge_kernel(in_ref, out_ref):
    levels = []
    for j in range(H):
        tail = in_ref[j, TOK:, :].astype(jnp.float32)
        levels.append(tail[0:2] + tail[2:4] + tail[4:6])
    top = levels[0]
    for level in levels[1:]:
        top = jnp.maximum(top, level)
    factors = [jnp.exp2(level - top) for level in levels]
    total = factors[0]
    for factor in factors[1:]:
        total = total + factor
    r128 = lax.broadcasted_iota(jnp.int32, (128, 128), 0)
    c128 = lax.broadcasted_iota(jnp.int32, (128, 128), 1)
    acc = jnp.zeros((TOK, 128), jnp.float32)
    for j in range(H):
        share = factors[j] / total
        upper = jnp.sum(jnp.where(r128 == c128, share[0:1], 0.0), axis=1, keepdims=True)
        lower = jnp.sum(
            jnp.where(r128[:64] == c128[:64], share[1:2], 0.0), axis=1, keepdims=True
        )
        column = jnp.concatenate([upper, lower], axis=0)
        acc = acc + column * in_ref[j, :TOK, :].astype(jnp.float32)
    out_ref[...] = acc.astype(jnp.bfloat16)


def merge(parts):
    return pl.pallas_call(
        merge_kernel,
        out_shape=jax.ShapeDtypeStruct((TOK, 128), jnp.bfloat16),
        compiler_params=pltpu.CompilerParams(vmem_limit_bytes=VMEM_LIMIT),
        cost_estimate=pl.CostEstimate(flops=1_000_000, bytes_accessed=500_000, transcendentals=3000),
        name="merge",
    )(parts)


def mix_kernel(rows_ref, gain_ref, w_ref, out_ref, n_ref, g_ref, u_ref, d_ref):
    for z in range(NZ):
        for c in range(NC):
            block = slice(c * 176, (c + 1) * 176)
            lanes = slice(z * 128, (z + 1) * 128)
            g_ref[block, lanes] = w_ref[z, c, 0:176, :]
            u_ref[block, lanes] = w_ref[z, c, 176:352, :]
            d_ref[block, lanes] = w_ref[z, c, 352:528, :]
    for y in range(NY):
        square = jnp.zeros((HALF, 256), jnp.float32)
        for f in range(H):
            piece = rows_ref[y * H + f].astype(jnp.float32)
            square = square + piece * piece
        factor = lax.rsqrt(jnp.sum(square, axis=1, keepdims=True) / 2048.0 + epsilon)
        for f in range(H):
            piece = rows_ref[y * H + f].astype(jnp.float32)
            n_ref[y * HALF : (y + 1) * HALF, f * 256 : (f + 1) * 256] = (
                piece * factor * gain_ref[:, f * 256 : (f + 1) * 256]
            ).astype(jnp.bfloat16)
    dims = (((1,), (1,)), ((), ()))
    gate = lax.dot_general(n_ref[...], g_ref[...], dims, preferred_element_type=jnp.float32)
    up = lax.dot_general(n_ref[...], u_ref[...], dims, preferred_element_type=jnp.float32)
    hidden = (gate / (1.0 + jnp.exp(-gate)) * up).astype(jnp.bfloat16)
    for f in range(H):
        part = jnp.dot(
            hidden, d_ref[:, f * 256 : (f + 1) * 256], preferred_element_type=jnp.float32
        ).astype(jnp.bfloat16)
        for y in range(NY):
            out_ref[y * H + f] = part[y * HALF : (y + 1) * HALF]


def mix(rows, gain, weights):
    return pl.pallas_call(
        mix_kernel,
        out_shape=jax.ShapeDtypeStruct((NY * H, HALF, 256), jnp.bfloat16),
        scratch_shapes=[
            pltpu.VMEM((NY * HALF, 2048), jnp.bfloat16),
            pltpu.VMEM((352, 2048), jnp.bfloat16),
            pltpu.VMEM((352, 2048), jnp.bfloat16),
            pltpu.VMEM((352, 2048), jnp.bfloat16),
        ],
        compiler_params=pltpu.CompilerParams(vmem_limit_bytes=VMEM_LIMIT),
        cost_estimate=pl.CostEstimate(
            flops=1_700_000_000, bytes_accessed=8_000_000, transcendentals=140_000
        ),
        name="mix",
    )(rows, gain, weights)


def from_everyone(x, axis, count):
    copies = jnp.broadcast_to(x, (count, *x.shape))
    return lax.all_to_all(copies, axis, split_axis=0, concat_axis=0, tiled=True)


def shards(
    query_content,
    query_rotary,
    latents,
    key_rotary,
    latent_gain,
    key_up,
    value_up,
    out_proj,
    residual,
    mixer_gain,
    gate_proj,
    up_proj,
    down_proj,
):
    zi, yi = lax.axis_index("z"), lax.axis_index("y")
    sp_index = zi * NY + yi
    tp_index = lax.axis_index("x") * NC + lax.axis_index("c")

    kv = lax.all_gather(
        jnp.concatenate([key_up, value_up], axis=0), ("x", "c"), axis=1, tiled=True
    )

    own_places = (sp_index * 8 + tp_index) * 24 + jnp.arange(24, dtype=jnp.int32)
    own = jnp.concatenate(
        [norm_round(latents, latent_gain), rotate_rows(key_rotary, own_places)], axis=1
    )
    lat = from_everyone(own, "z", NZ).reshape(NZ * 24, 320)

    stacked = jnp.stack([gate_proj, up_proj, down_proj.T])
    slices = stacked.reshape(3, 32, NY, 176).transpose(2, 1, 0, 3).reshape(NY, 32, 528)
    slices, lat = lax.optimization_barrier((slices, lat))
    slices = lax.all_to_all(slices, "y", split_axis=0, concat_axis=0, tiled=True)
    slices, lat = lax.optimization_barrier((slices, lat))
    own_slice = slices.reshape(128, 528).T
    mixer = lax.all_gather(own_slice, ("z", "c"), axis=0, tiled=False).reshape(NZ, NC, 528, 128)

    lat = lax.all_gather(lat, "y", axis=0, tiled=True)

    index = jnp.arange(KEYS, dtype=jnp.int32)
    y_of, z_of, i_of = index // 384, index // 24 % NZ, index % 24
    key_segment = (((z_of * NY + y_of) * 8 + tp_index) * 24 + i_of) // SPAN
    seg = jnp.broadcast_to((key_segment - sp_index * (TOK // SPAN))[:, None], (KEYS, 128))
    cosine, sine = tables(sp_index * TOK + jnp.arange(TOK, dtype=jnp.int32))
    cosine, sine = (jnp.concatenate([t] * 4, axis=1) for t in (cosine, sine))

    parts = attend(query_content, query_rotary, cosine, sine, lat, seg, kv)
    parts = lax.all_to_all(parts, ("x", "c"), split_axis=0, concat_axis=0, tiled=True)
    attended = lax.all_gather(merge(parts), ("x", "c"), axis=1, tiled=True)
    mixed_rows = (
        residual.astype(jnp.float32)
        + jnp.dot(attended, out_proj, preferred_element_type=jnp.float32)
    ).astype(jnp.bfloat16)

    halves = mixed_rows.reshape(NC, HALF, 256)
    sent = jnp.broadcast_to(halves, (NY * NX, NC, HALF, 256)).reshape(32, HALF, 256)
    rows = lax.all_to_all(sent, ("y", "x", "c"), split_axis=0, concat_axis=0, tiled=True)
    partial_sums = mix(rows, mixer_gain.reshape(1, -1), mixer)
    arrived = lax.all_to_all(
        partial_sums, ("y", "x", "c"), split_axis=0, concat_axis=0, tiled=True
    )
    summed = arrived.reshape(NY * NX, TOK, 256).astype(jnp.float32).sum(axis=0)
    return (mixed_rows.astype(jnp.float32) + summed).astype(jnp.bfloat16)


def solution(mesh):
    fine = Mesh(mesh.devices.reshape(NZ, NY, NX, NC), ("z", "y", "x", "c"))
    sp, tp = ("z", "y"), ("x", "c")
    return jax.shard_map(
        shards,
        mesh=fine,
        in_specs=(
            P(sp, None),
            P(sp, None),
            P((*sp, *tp), None),
            P((*sp, *tp), None),
            P(),
            P(None, tp),
            P(None, tp),
            P(None, tp),
            P(sp, tp),
            P(),
            P(sp, tp),
            P(sp, tp),
            P(tp, sp),
        ),
        out_specs=P(sp, tp),
        check_vma=False,
    )
```

time: 240 us -> 187 us (0.78)
  blocking collectives: 180 us -> 112 us
  matrix products: 22.9 us -> 0.27 us
  Pallas kernels: 0 us -> 20.6 us
  starting transfers between devices: 0.04 us -> 15.8 us
  waiting for transfers between devices: 1.79 us -> 12 us
  local copies, waits for them, and re-layouts: 10.6 us -> 4.47 us
  other arithmetic: 10.2 us -> 6.89 us
    all_gather x1 -> x2, blocking collectives: 86.9 us -> 25.2 us  [the longest x1 12.7 us: shards(): attended = lax.all_gather(merge(parts), ('x', 'c'), axis=1, tiled=True)]
    dot_general x22 -> x0, matrix products: 22.6 us -> none  [the longest x1 5.52 us: shards(): jnp.dot(hidden, down_whole, preferred_element_type=jnp.float32)]
    pallas_call x0 -> x3, Pallas kernels: none -> 20.6 us  [the longest x1 11.4 us: attend(): pl.pallas_call(attend_kernel, grid=(H // 2,), in_specs=[pl.BlockSpec((TOK...]
    all_to_all x0 -> x1, starting transfers between devices: none -> 15.7 us  [from_everyone(): return lax.all_to_all(copies, axis, split_axis=0, concat_axis=0, tiled=True)]
    all_to_all x0 -> x1, waiting for transfers between devices: none -> 11.9 us  [from_everyone(): return lax.all_to_all(copies, axis, split_axis=0, concat_axis=0, tiled=True)]
    all_to_all x4, blocking collectives: 93.4 us -> 87.1 us  [the longest x1 27.6 us: shards(): lax.all_to_all(sent, ('y', 'x', 'c'), split_axis=0, concat_axis=0, tiled=...]
    unnamed x18 -> x8, local copies, waits for them, and re-layouts: 3.19 us -> 0.02 us
    reduce_sum x7 -> x1, other arithmetic: 3.34 us -> 0.22 us  [shards(): summed = arrived.reshape(NY * NX, TOK, 256).astype(jnp.float32).sum(axis=0)]
  transfers between devices with their start and end apart: 2 -> 3, of which waited for: 1 -> 1; matrix products, arithmetic and copies ran while one was open for 13% -> 5% of each run, Pallas kernels for 0% -> 7%
where the time goes in v1:
time: 187 us; the launch traced here: 186 us
  blocking collectives  112 us (60%)
  Pallas kernels  20.6 us (11%)
  starting transfers between devices  15.8 us (8%)
  between operations  13.6 us (7%)
  waiting for transfers between devices  12 us (6%)
  other arithmetic  6.89 us (4%)
  local copies, waits for them, and re-layouts  4.47 us (2%)
    all_to_all x1, blocking collectives, shards(): lax.all_to_all(sent, ('y', 'x', 'c'), split_axis=0, concat_axis=0, tiled=...  27.6 us
    all_to_all x1, blocking collectives, shards(): lax.all_to_all(partial_sums, ('y', 'x', 'c'), split_axis=0, concat_axis=0...  26.8 us
    all_to_all x1, blocking collectives, shards(): lax.all_to_all(parts, ('x', 'c'), split_axis=0, concat_axis=0, tiled=True)  23.8 us
    all_to_all x1, starting transfers between devices, from_everyone(): return lax.all_to_all(copies, axis, split_axis=0, concat_axis=0, tiled=True)  15.7 us
    all_gather x1, blocking collectives, shards(): attended = lax.all_gather(merge(parts), ('x', 'c'), axis=1, tiled=True)  12.7 us
    all_gather x1, blocking collectives, shards(): lat = lax.all_gather(lat, 'y', axis=0, tiled=True)  12.5 us
    all_to_all x1, waiting for transfers between devices, from_everyone(): return lax.all_to_all(copies, axis, split_axis=0, concat_axis=0, tiled=True)  11.9 us
    pallas_call x1, Pallas kernels, attend(): pl.pallas_call(attend_kernel, grid=(H // 2,), in_specs=[pl.BlockSpec((TOK...  11.4 us
  transfers between devices with their start and end apart: 3, of which 1 were waited for; matrix products, arithmetic and copies ran while one was open for 5% of the time, Pallas kernels for 7%

profile of v1, /device:TPU:1, one launch (start us, length us, event | category | flops | bytes accessed | tf_op | source)
XLA Modules:
  0.0 185.8 jit_solution(6262866085584148758)
XLA Ops:
  6.5 0.0 copy-start
  6.5 0.0 copy-start.2
  6.5 0.0 copy-start.3
  6.5 0.0 all-gather.4.cloned.1.call-start
  6.5 1.6 pad_maximum_fusion
  8.1 0.0 all-gather.4.cloned.1.call-update
  8.2 0.8 fusion.1
  9.0 0.7 convert_element_type.46
  9.7 0.1 fusion.13
  9.9 0.8 fusion.3
  10.7 0.1 pad_maximum_fusion.3
  10.7 0.7 broadcast_in_dim.6
  11.5 15.7 %all-to-all-start = ((bf16[16,24,320]{2,1,0:T(8,128)(2,1)}), bf16[16,24,320]{2,1,0:T(8,128)(2,1)S(1)}, u32[]{:S(2)}, u32[]{:S(2)}) async-start(bf16[16,24,320]{2,1,0:T(8,128)(2,1)} %broadcast_in_dim.6), calls=%async_computation | async-start | bytes 589824 | tf_op jit(solution)/shard_map/all_to_all | solution.py:219
  27.2 0.0 all-gather.6.cloned.1.call-start
  27.3 0.9 stack.12
  28.2 0.1 copy.18
  28.3 0.0 copy-done.2
  28.3 0.1 stack.13
  28.4 0.1 copy.19
  28.5 0.0 copy-done.3
  28.5 0.1 stack.14
  28.7 0.1 copy.20
  28.8 0.5 maximum_bitcast_fusion
  29.3 0.2 reshape.115
  29.5 11.9 %all-to-all-done = bf16[16,24,320]{2,1,0:T(8,128)(2,1)S(1)} async-done(((bf16[16,24,320]{2,1,0:T(8,128)(2,1)}), bf16[16,24,320]{2,1,0:T(8,128)(2,1)S(1)}, u32[]{:S(2)}, u32[]{:S(2)}) %all-to-all-start) | async-done | bytes 245792 | tf_op jit(solution)/shard_map/all_to_all | solution.py:219
  41.4 9.0 %all_to_all.25 = bf16[4,32,528]{2,1,0:T(8,128)(2,1)S(1)} all-to-all(bf16[4,32,528]{2,1,0:T(8,128)(2,1)S(1)} %reshape.115), channel_id=1, replica_groups=mesh['z'=16,'y'=4,'x'=4,'c'=2] {'y'}, dimensions={0} | all-to-all | bytes 270336 | tf_op jit(solution)/shard_map/all_to_all | solution.py:254
  50.4 0.8 copy.21
  51.2 0.0 all-gather.6.cloned.1.call-update
  51.2 0.4 multiply_sine_fusion
  51.7 0.9 pad_maximum_fusion.1
  52.6 12.5 %all_gather.15.lat_ref = bf16[1536,320]{1,0:T(8,128)(2,1)} all-gather(bf16[384,320]{1,0:T(8,128)(2,1)S(1)} %bitcast.20), channel_id=1, replica_groups=mesh['z'=16,'y'=4,'x'=4,'c'=2] {'y'}, dimensions={0}, use_global_device_ids=true | all-gather | bytes 1228800 | tf_op jit(solution)/shard_map/all_gather | solution.py:259
  65.1 0.0 all-gather.4.cloned.1.call-done.w_ref
  65.1 1.2 broadcast_in_dim.7.seg_ref
  66.2 11.4 %attend.1 = bf16[8,208,128]{2,1,0:T(8,128)(2,1)} custom-call(bf16[192,1024]{1,0:T(8,128)(2,1)} %q_ref.1, bf16[192,512]{1,0:T(8,128)(2,1)} %qr_ref.1, f32[192,128]{1,0:T(8,128)} %get-tuple-element.17.cos_ref, f32[192,128]{1,0:T(8,128)} %get-tuple-element.18.sin_ref, bf16[1536,320]{1,0:T(8,128)(2,1)} %all_gather.15.lat_ref, ...), custom_call_target="tpu_custom_call" | custom-call | flops 3000000000 | bytes 4000000 | tf_op jit(solution)/shard_map/attend/pallas_call | solution.py:107
  77.6 0.0 copy-start.1
  77.6 23.8 %all_to_all.26.in_ref = bf16[8,208,128]{2,1,0:T(8,128)(2,1)} all-to-all(bf16[8,208,128]{2,1,0:T(8,128)(2,1)} %attend.1), channel_id=1, replica_groups=mesh['z'=16,'y'=4,'x'=4,'c'=2] {'x','c'}, dimensions={0} | all-to-all | bytes 851968 | tf_op jit(solution)/shard_map/all_to_all | solution.py:269
  101.3 2.2 %merge.1 = bf16[192,128]{1,0:T(8,128)(2,1)} custom-call(bf16[8,208,128]{2,1,0:T(8,128)(2,1)} %all_to_all.26.in_ref), custom_call_target="tpu_custom_call" | custom-call | flops 1000000 | bytes 500000 | tf_op jit(solution)/shard_map/merge/pallas_call | solution.py:159
  103.5 12.7 %all_gather.17 = bf16[192,1024]{1,0:T(8,128)(2,1)S(1)} all-gather(bf16[192,128]{1,0:T(8,128)(2,1)} %merge.1), channel_id=1, replica_groups=mesh['z'=16,'y'=4,'x'=4,'c'=2] {'x','c'}, dimensions={1}, use_global_device_ids=true | all-gather | bytes 442368 | tf_op jit(solution)/shard_map/all_gather | solution.py:270
  116.2 0.0 copy-done
  116.2 0.0 copy-done.1
  116.2 0.3 fusion
  116.5 0.2 broadcast_in_dim.8
  116.7 27.6 %all_to_all.27.rows_ref = bf16[32,96,256]{2,1,0:T(8,128)(2,1)} all-to-all(bf16[32,96,256]{2,1,0:T(8,128)(2,1)S(1)} %bitcast.18), channel_id=1, replica_groups=mesh['z'=16,'y'=4,'x'=4,'c'=2] {'y','x','c'}, dimensions={0} | all-to-all | bytes 3145728 | tf_op jit(solution)/shard_map/all_to_all | solution.py:278
  144.3 0.0 all-gather.6.cloned.1.call-done
  144.3 7.1 %mix.1 = bf16[32,96,256]{2,1,0:T(8,128)(2,1)} custom-call(bf16[32,96,256]{2,1,0:T(8,128)(2,1)} %all_to_all.27.rows_ref, f32[1,2048]{1,0:T(1,128)} %bitcast.24, bf16[16,2,528,128]{3,2,1,0:T(8,128)(2,1)} %bitcast.19), custom_call_target="tpu_custom_call" | custom-call | flops 1700000000 | bytes 8000000 | tf_op jit(solution)/shard_map/mix/pallas_call | solution.py:200
  151.3 26.8 %all_to_all.28 = bf16[32,96,256]{2,1,0:T(8,128)(2,1)S(1)} all-to-all(bf16[32,96,256]{2,1,0:T(8,128)(2,1)} %mix.1), channel_id=1, replica_groups=mesh['z'=16,'y'=4,'x'=4,'c'=2] {'y','x','c'}, dimensions={0} | all-to-all | bytes 3145728 | tf_op jit(solution)/shard_map/all_to_all | solution.py:280
  178.1 0.2 convert_reduce_fusion
  178.3 0.7 add_convert_fusion
  (5 shorter events, 0.1 us)
Async XLA Ops:
  6.5 109.7 %copy-start = (bf16[1024,256]{1,0:T(8,128)(2,1)S(1)}, bf16[1024,256]{1,0:T(8,128)(2,1)}, u32[]{:S(2)}) copy-start(bf16[1024,256]{1,0:T(8,128)(2,1)} %param.20) | copy-start | bytes 1572868
  6.5 21.8 %copy-start.2 = (bf16[32,704]{1,0:T(8,128)(2,1)S(1)}, bf16[32,704]{1,0:T(8,128)(2,1)}, u32[]{:S(2)}) copy-start(bf16[32,704]{1,0:T(8,128)(2,1)} %param.24) | copy-start | bytes 135172
  6.5 22.0 %copy-start.3 = (bf16[704,32]{0,1:T(8,128)(2,1)S(1)}, bf16[704,32]{0,1:T(8,128)(2,1)}, u32[]{:S(2)}) copy-start(bf16[704,32]{0,1:T(8,128)(2,1)} %param.25) | copy-start | bytes 135172
  6.5 58.5 %all-gather.4.cloned.1.call-start = ((), (), s32[]{:S(2)}) async-start(), calls=%async_computation.5 | async-start | bytes 1179648 | tf_op jit(solution)/shard_map/all_gather | solution.py:241
  11.5 29.9 %all-to-all-start = ((bf16[16,24,320]{2,1,0:T(8,128)(2,1)}), bf16[16,24,320]{2,1,0:T(8,128)(2,1)S(1)}, u32[]{:S(2)}, u32[]{:S(2)}) async-start(bf16[16,24,320]{2,1,0:T(8,128)(2,1)} %broadcast_in_dim.6), calls=%async_computation | async-start | bytes 589824 | tf_op jit(solution)/shard_map/all_to_all | solution.py:219
  27.2 117.0 %all-gather.6.cloned.1.call-start = ((), (), s32[]{:S(2)}) async-start(), calls=%async_computation.6 | async-start | bytes 4460544 | tf_op jit(solution)/shard_map/all_gather | solution.py:257
  77.6 38.7 %copy-start.1 = (bf16[192,256]{1,0:T(8,128)(2,1)S(1)}, bf16[192,256]{1,0:T(8,128)(2,1)}, u32[]{:S(2)}) copy-start(bf16[192,256]{1,0:T(8,128)(2,1)} %param.21) | copy-start | bytes 294916
Sparse Core Ops, SparseCore 0:
  9.5 36.5 all-gather.3
  51.3 74.4 all-gather.5

commit v2 on v1

v2 whole, which is shorter than its diff:
```python
import math

import jax
import jax.numpy as jnp
from jax import lax
from jax.experimental import pallas as pl
from jax.experimental.pallas import tpu as pltpu
from jax.sharding import Mesh, PartitionSpec as P


H = 8
DN = 128
DR = 64
DV = 128
SPAN = 64
NZ, NY, NX, NC = 16, 4, 4, 2
TOK = 192
HALF = TOK // 2
KEYS = 1536
PAD = 208
GROUP = 4

epsilon = 1e-06
masked_score = -1e30
LOG2E = 1.4426950408889634


def tables(places):
    inverse = 10000.0 ** (-jnp.arange(0, DR, 2, dtype=jnp.float32) / DR)
    angles = places.astype(jnp.float32)[:, None] * inverse[None, :]
    return jnp.cos(angles), jnp.sin(angles)


def prepare_kernel(lat_ref, rot_ref, gain_ref, cos_ref, sin_ref, k_ref, v_ref, out_ref, kv_ref):
    kv_ref[:, :DN] = k_ref[...]
    kv_ref[:, DN:] = v_ref[...]
    widened = lat_ref[...].astype(jnp.float32)
    factor = lax.rsqrt(jnp.mean(widened * widened, axis=-1, keepdims=True) + epsilon)
    normed = (widened * factor * gain_ref[...]).astype(jnp.bfloat16)
    widened = rot_ref[...].astype(jnp.float32)
    a, b = widened[:, : DR // 2], widened[:, DR // 2 :]
    cosine, sine = cos_ref[...], sin_ref[...]
    turned = jnp.concatenate([a * cosine - b * sine, b * cosine + a * sine], axis=-1)
    turned = turned.astype(jnp.bfloat16)
    for z in range(NZ):
        out_ref[z, :, :256] = normed
        out_ref[z, :, 256:] = turned


def prepare(*inputs):
    return pl.pallas_call(
        prepare_kernel,
        out_shape=(
            jax.ShapeDtypeStruct((NZ, 24, 320), jnp.bfloat16),
            jax.ShapeDtypeStruct((256, 256), jnp.bfloat16),
        ),
        compiler_params=pltpu.CompilerParams(vmem_limit_bytes=4 * 1024 * 1024),
        cost_estimate=pl.CostEstimate(flops=100_000, bytes_accessed=300_000, transcendentals=24),
        name="prepare",
    )(*inputs)


def attend_kernel(q_ref, qr_ref, cos_ref, sin_ref, lat_ref, seg_ref, w_ref, out_ref, key_ref):
    scale = LOG2E / math.sqrt(DN + DR)

    @pl.when(pl.program_id(0) == 0)
    def _():
        lane = lax.broadcasted_iota(jnp.int32, (KEYS, 64), 1)
        mask = jnp.where(seg_ref[:, :64] > lane, masked_score, 0.0)
        mask = jnp.where(lane < TOK // SPAN, mask, 0.0).astype(jnp.bfloat16)
        for h in range(GROUP):
            key_ref[h, :, DN : DN + DR] = lat_ref[:, 256:320]
            key_ref[h, :, DN + DR :] = mask

    turned = qr_ref[...].astype(jnp.float32)
    lane = lax.broadcasted_iota(jnp.int32, turned.shape, 1)
    first = lane % DR < DR // 2
    swapped = jnp.where(
        first, pltpu.roll(turned, GROUP * DR - DR // 2, 1), pltpu.roll(turned, DR // 2, 1)
    )
    signed = jnp.where(first, -swapped, swapped)
    cosine = jnp.concatenate([cos_ref[...]] * (GROUP // 2), axis=1)
    sine = jnp.concatenate([sin_ref[...]] * (GROUP // 2), axis=1)
    turned = (turned * cosine + signed * sine).astype(jnp.bfloat16)
    row = lax.broadcasted_iota(jnp.int32, (TOK, 64), 0)
    col = lax.broadcasted_iota(jnp.int32, (TOK, 64), 1)
    segment = jnp.where(row // SPAN == col, 1.0, 0.0).astype(jnp.bfloat16)
    normed = lat_ref[:, :256]
    ones = jnp.ones((KEYS, 128), jnp.bfloat16)
    r128 = lax.broadcasted_iota(jnp.int32, (128, 128), 0)
    c128 = lax.broadcasted_iota(jnp.int32, (128, 128), 1)
    for h in range(GROUP):
        pair = jnp.dot(normed, w_ref[h], preferred_element_type=jnp.float32).astype(jnp.bfloat16)
        query = jnp.concatenate(
            [q_ref[:, h * DN : (h + 1) * DN], turned[:, h * DR : (h + 1) * DR], segment], axis=1
        )
        key_ref[h, :, :DN] = pair[:, :DN]
        scores = lax.dot_general(
            query, key_ref[h], (((1,), (1,)), ((), ())), preferred_element_type=jnp.float32
        )
        highest = jnp.max(scores, axis=1, keepdims=True) * scale
        weights = jnp.exp2(scores * scale - highest).astype(jnp.bfloat16)
        both = jnp.concatenate([pair[:, DN:], ones], axis=1)
        sums = jnp.dot(weights, both, preferred_element_type=jnp.float32)
        norm = sums[:, DV:]
        out_ref[h, :TOK, :] = (sums[:, :DV] / norm).astype(jnp.bfloat16)
        level = highest + jnp.log2(norm)
        upper = jnp.sum(jnp.where(r128 == c128, level[:128], 0.0), axis=0, keepdims=True)
        lower = jnp.sum(
            jnp.where(r128[:64] == c128[:64], level[128:], 0.0), axis=0, keepdims=True
        )
        rest = jnp.concatenate([upper, lower], axis=0)
        rows = []
        for _ in range(3):
            part = rest.astype(jnp.bfloat16).astype(jnp.float32)
            rows.append(part)
            rest = rest - part
        rows.append(jnp.zeros((PAD - TOK - 6, 128), jnp.float32))
        out_ref[h, TOK:, :] = jnp.concatenate(rows, axis=0).astype(jnp.bfloat16)


def attend(query, query_rotary, cosine, sine, lat, seg, weights):
    return pl.pallas_call(
        attend_kernel,
        grid=(H // GROUP,),
        in_specs=[
            pl.BlockSpec((TOK, GROUP * DN), lambda i: (0, i)),
            pl.BlockSpec((TOK, GROUP * DR), lambda i: (0, i)),
            pl.BlockSpec((TOK, 2 * DR), lambda i: (0, 0)),
            pl.BlockSpec((TOK, 2 * DR), lambda i: (0, 0)),
            pl.BlockSpec((KEYS, 320), lambda i: (0, 0)),
            pl.BlockSpec((KEYS, 128), lambda i: (0, 0)),
            pl.BlockSpec((GROUP, 256, 256), lambda i: (i, 0, 0)),
        ],
        out_specs=pl.BlockSpec((GROUP, PAD, 128), lambda i: (i, 0, 0)),
        out_shape=jax.ShapeDtypeStruct((H, PAD, 128), jnp.bfloat16),
        scratch_shapes=[pltpu.VMEM((GROUP, KEYS, 256), jnp.bfloat16)],
        compiler_params=pltpu.CompilerParams(
            dimension_semantics=("arbitrary",), vmem_limit_bytes=24 * 1024 * 1024
        ),
        cost_estimate=pl.CostEstimate(
            flops=3_000_000_000, bytes_accessed=4_000_000, transcendentals=2_400_000
        ),
        name="attend",
    )(query, query_rotary, cosine, sine, lat, seg, weights)


def merge_kernel(in_ref, out_ref):
    levels = []
    for j in range(H):
        tail = in_ref[j, TOK:, :].astype(jnp.float32)
        levels.append(tail[0:2] + tail[2:4] + tail[4:6])
    top = levels[0]
    for level in levels[1:]:
        top = jnp.maximum(top, level)
    factors = [jnp.exp2(level - top) for level in levels]
    total = factors[0]
    for factor in factors[1:]:
        total = total + factor
    r128 = lax.broadcasted_iota(jnp.int32, (128, 128), 0)
    c128 = lax.broadcasted_iota(jnp.int32, (128, 128), 1)
    acc = jnp.zeros((TOK, 128), jnp.float32)
    for j in range(H):
        share = factors[j] / total
        upper = jnp.sum(jnp.where(r128 == c128, share[0:1], 0.0), axis=1, keepdims=True)
        lower = jnp.sum(
            jnp.where(r128[:64] == c128[:64], share[1:2], 0.0), axis=1, keepdims=True
        )
        column = jnp.concatenate([upper, lower], axis=0)
        acc = acc + column * in_ref[j, :TOK, :].astype(jnp.float32)
    out_ref[...] = acc.astype(jnp.bfloat16)


def merge(parts):
    return pl.pallas_call(
        merge_kernel,
        out_shape=jax.ShapeDtypeStruct((TOK, 128), jnp.bfloat16),
        compiler_params=pltpu.CompilerParams(vmem_limit_bytes=8 * 1024 * 1024),
        cost_estimate=pl.CostEstimate(flops=1_000_000, bytes_accessed=500_000, transcendentals=3000),
        name="merge",
    )(parts)


def mix_kernel(rows_ref, gain_ref, w_hbm, out_ref, n_ref, w_ref, sem):
    copies = [
        pltpu.make_async_copy(w_hbm.at[z], w_ref.at[:, pl.ds(z * 128, 128)], sem.at[z])
        for z in range(NZ)
    ]
    for copy in copies:
        copy.start()
    for y in range(NY):
        square = jnp.zeros((HALF, 256), jnp.float32)
        for f in range(H):
            piece = rows_ref[y * H + f].astype(jnp.float32)
            square = square + piece * piece
        factor = lax.rsqrt(jnp.sum(square, axis=1, keepdims=True) / 2048.0 + epsilon)
        for f in range(H):
            piece = rows_ref[y * H + f].astype(jnp.float32)
            n_ref[y * HALF : (y + 1) * HALF, f * 256 : (f + 1) * 256] = (
                piece * factor * gain_ref[:, f * 256 : (f + 1) * 256]
            ).astype(jnp.bfloat16)
    for copy in copies:
        copy.wait()
    dims = (((1,), (1,)), ((), ()))
    hidden = []
    for c in range(NC):
        gate = lax.dot_general(
            n_ref[...], w_ref[c * 528 : c * 528 + 176], dims, preferred_element_type=jnp.float32
        )
        up = lax.dot_general(
            n_ref[...], w_ref[c * 528 + 176 : c * 528 + 352], dims,
            preferred_element_type=jnp.float32,
        )
        hidden.append((gate / (1.0 + jnp.exp(-gate)) * up).astype(jnp.bfloat16))
    for f in range(H):
        lanes = slice(f * 256, (f + 1) * 256)
        part = sum(
            jnp.dot(
                hidden[c], w_ref[c * 528 + 352 : (c + 1) * 528, lanes],
                preferred_element_type=jnp.float32,
            )
            for c in range(NC)
        ).astype(jnp.bfloat16)
        for y in range(NY):
            out_ref[y * H + f] = part[y * HALF : (y + 1) * HALF]


def mix(rows, gain, weights):
    whole = pl.BlockSpec(memory_space=pltpu.VMEM)
    return pl.pallas_call(
        mix_kernel,
        in_specs=[whole, whole, pl.BlockSpec(memory_space=pltpu.HBM)],
        out_specs=whole,
        out_shape=jax.ShapeDtypeStruct((NY * H, HALF, 256), jnp.bfloat16),
        scratch_shapes=[
            pltpu.VMEM((NY * HALF, 2048), jnp.bfloat16),
            pltpu.VMEM((1056, 2048), jnp.bfloat16),
            pltpu.SemaphoreType.DMA((NZ,)),
        ],
        compiler_params=pltpu.CompilerParams(vmem_limit_bytes=63_200_000),
        cost_estimate=pl.CostEstimate(
            flops=1_700_000_000, bytes_accessed=8_000_000, transcendentals=140_000
        ),
        name="mix",
    )(rows, gain, weights)


def project_kernel(heads_ref, w_ref, res_ref, mixed_ref, sent_ref):
    heads = jnp.concatenate([heads_ref[h] for h in range(H)], axis=1)
    mixed = (
        res_ref[...].astype(jnp.float32)
        + jnp.dot(heads, w_ref[...], preferred_element_type=jnp.float32)
    ).astype(jnp.bfloat16)
    mixed_ref[...] = mixed
    for d in range(NY * NX):
        for c in range(NC):
            sent_ref[d * NC + c] = mixed[c * HALF : (c + 1) * HALF]


def project(heads, weights, residual):
    return pl.pallas_call(
        project_kernel,
        out_shape=(
            jax.ShapeDtypeStruct((TOK, 256), jnp.bfloat16),
            jax.ShapeDtypeStruct((NY * NX * NC, HALF, 256), jnp.bfloat16),
        ),
        compiler_params=pltpu.CompilerParams(vmem_limit_bytes=12 * 1024 * 1024),
        cost_estimate=pl.CostEstimate(
            flops=100_000_000, bytes_accessed=3_000_000, transcendentals=0
        ),
        name="project",
    )(heads, weights, residual)


def layer(
    query_content,
    query_rotary,
    latents,
    key_rotary,
    latent_gain,
    key_up,
    value_up,
    out_proj,
    residual,
    mixer_gain,
    gate_proj,
    up_proj,
    down_proj,
):
    zi, yi = lax.axis_index("z"), lax.axis_index("y")
    sp_index = zi * NY + yi
    tp_index = lax.axis_index("x") * NC + lax.axis_index("c")

    own_places = (sp_index * 8 + tp_index) * 24 + jnp.arange(24, dtype=jnp.int32)
    cosine, sine = tables(own_places)
    own, kv = prepare(
        latents, key_rotary, latent_gain.reshape(1, -1), cosine, sine, key_up, value_up
    )
    kv = lax.all_gather(kv, ("x", "c"), axis=0, tiled=False)

    stacked = jnp.stack([gate_proj, up_proj, down_proj.T])
    slices = stacked.reshape(3, 32, NY, 176).transpose(2, 1, 0, 3).reshape(NY, 32, 528)
    ahead = lax.dynamic_slice_in_dim(jnp.concatenate([slices, slices]), yi, NY, axis=0)
    lat = lax.all_to_all(own, "z", split_axis=0, concat_axis=0, tiled=True)
    lat = lat.reshape(NZ * 24, 320)
    back = [ahead[0]] + [
        lax.ppermute(ahead[s], "y", [(i, (i + s) % NY) for i in range(NY)]) for s in range(1, NY)
    ]
    turn = jnp.stack(back[::-1] * 2)
    own_slice = lax.dynamic_slice_in_dim(turn, NY - 1 - yi, NY, axis=0).reshape(128, 528).T
    mixer = lax.all_gather(own_slice, ("z", "c"), axis=0, tiled=True).reshape(
        NZ, NC * 528, 128
    )

    lat = lax.all_gather(lat, "y", axis=0, tiled=True)

    index = jnp.arange(KEYS, dtype=jnp.int32)
    y_of, z_of, i_of = index // 384, index // 24 % NZ, index % 24
    key_segment = (((z_of * NY + y_of) * 8 + tp_index) * 24 + i_of) // SPAN
    seg = jnp.broadcast_to((key_segment - sp_index * (TOK // SPAN))[:, None], (KEYS, 128))
    cosine, sine = tables(sp_index * TOK + jnp.arange(TOK, dtype=jnp.int32))
    cosine, sine = (jnp.concatenate([t] * 4, axis=1) for t in (cosine, sine))

    parts = attend(query_content, query_rotary, cosine, sine, lat, seg, kv)
    parts = lax.all_to_all(parts, ("x", "c"), split_axis=0, concat_axis=0, tiled=True)
    heads = lax.all_gather(merge(parts), ("x", "c"), axis=0, tiled=False)
    mixed_rows, sent = project(heads, out_proj, residual)
    rows = lax.all_to_all(sent, ("y", "x", "c"), split_axis=0, concat_axis=0, tiled=True)
    partial_sums = mix(rows, mixer_gain.reshape(1, -1), mixer)
    arrived = lax.all_to_all(
        partial_sums, ("y", "x", "c"), split_axis=0, concat_axis=0, tiled=True
    )
    summed = arrived.reshape(NY * NX, TOK, 256).astype(jnp.float32).sum(axis=0)
    return (mixed_rows.astype(jnp.float32) + summed).astype(jnp.bfloat16)


def solution(mesh):
    fine = Mesh(mesh.devices.reshape(NZ, NY, NX, NC), ("z", "y", "x", "c"))
    sp, tp = ("z", "y"), ("x", "c")
    return jax.shard_map(
        layer,
        mesh=fine,
        in_specs=(
            P(sp, None),
            P(sp, None),
            P((*sp, *tp), None),
            P((*sp, *tp), None),
            P(),
            P(None, tp),
            P(None, tp),
            P(None, tp),
            P(sp, tp),
            P(),
            P(sp, tp),
            P(sp, tp),
            P(tp, sp),
        ),
        out_specs=P(sp, tp),
        check_vma=False,
    )
```

time: 187 us -> 183 us (0.979)
  blocking collectives: 112 us -> 101 us
  starting transfers between devices: 15.8 us -> 25.3 us
  other arithmetic: 6.89 us -> 2.3 us
  waiting for transfers between devices: 12 us -> 15.7 us
  Pallas kernels: 20.6 us -> 17.9 us
    all_to_all x4 -> x3, blocking collectives: 87.1 us -> 76.2 us  [the longest x1 26.8 us: layer(): lax.all_to_all(partial_sums, ('y', 'x', 'c'), split_axis=0, concat_axis=0...]
    ppermute x0 -> x3, starting transfers between devices: none -> 10.3 us  [layer(): lax.ppermute(ahead[s], 'y', [(i, (i + s) % NY) for i in range(NY)])]
    ppermute x0 -> x3, waiting for transfers between devices: none -> 3.32 us  [layer(): lax.ppermute(ahead[s], 'y', [(i, (i + s) % NY) for i in range(NY)])]
    concatenate x3 -> x2, other arithmetic: 2.58 us -> 0.31 us  [the longest x1 0.22 us: layer(): cosine, sine = (jnp.concatenate([t] * 4, axis=1) for t in (cosine, sine))]
    pallas_call x2 -> x4, Pallas kernels: 18.4 us -> 17.4 us  [the longest x1 8.55 us: attend(): pl.pallas_call(attend_kernel, grid=(H // GROUP,), in_specs=[pl.BlockSpec(...]
  transfers between devices with their start and end apart: 3 -> 6, of which waited for: 1 -> 3; matrix products, arithmetic and copies ran while one was open for 5% -> 1% of each run, Pallas kernels for 7% -> 6%
where the time goes in v2:
time: 183 us; the launch traced here: 182 us
  blocking collectives  101 us (55%)
  starting transfers between devices  25.3 us (14%)
  Pallas kernels  17.9 us (10%)
  waiting for transfers between devices  15.7 us (9%)
  between operations  13.8 us (8%)
  local copies, waits for them, and re-layouts  5.66 us (3%)
  other arithmetic  2.3 us (1%)
    all_to_all x1, blocking collectives, layer(): lax.all_to_all(partial_sums, ('y', 'x', 'c'), split_axis=0, concat_axis=0...  26.8 us
    all_to_all x1, blocking collectives, layer(): lax.all_to_all(sent, ('y', 'x', 'c'), split_axis=0, concat_axis=0, tiled=...  26.5 us
    all_to_all x1, blocking collectives, layer(): lax.all_to_all(parts, ('x', 'c'), split_axis=0, concat_axis=0, tiled=True)  22.9 us
    all_to_all x1, starting transfers between devices, layer(): lat = lax.all_to_all(own, 'z', split_axis=0, concat_axis=0, tiled=True)  14.9 us
    all_gather x1, blocking collectives, layer(): heads = lax.all_gather(merge(parts), ('x', 'c'), axis=0, tiled=False)  13.7 us
    all_to_all x1, waiting for transfers between devices, layer(): lat = lax.all_to_all(own, 'z', split_axis=0, concat_axis=0, tiled=True)  12.3 us
    all_gather x1, blocking collectives, layer(): lat = lax.all_gather(lat, 'y', axis=0, tiled=True)  11.5 us
    ppermute x3, starting transfers between devices, layer(): lax.ppermute(ahead[s], 'y', [(i, (i + s) % NY) for i in range(NY)])  10.3 us
  transfers between devices with their start and end apart: 6, of which 3 were waited for; matrix products, arithmetic and copies ran while one was open for 1% of the time, Pallas kernels for 6%

profile of v2, /device:TPU:1, one launch (start us, length us, event | category | flops | bytes accessed | tf_op | source)
XLA Modules:
  0.0 182.0 jit_solution(11282807225793943682)
XLA Ops:
  6.5 0.0 all-gather.7.cloned.1.call-start
  6.6 0.9 stack.29
  7.6 0.1 copy.26
  7.7 0.9 stack.28
  8.6 0.1 copy.25
  8.7 0.9 stack.27
  9.6 0.1 copy.24
  9.7 0.5 maximum_bitcast_fusion
  10.2 0.2 reshape.106
  10.4 0.1 fusion
  10.5 5.5 %collective-permute-start = (bf16[32,528]{1,0:T(8,128)(2,1)S(1)}, bf16[32,528]{1,0:T(8,128)(2,1)S(1)}, u32[]{:S(2)}, u32[]{:S(2)}) collective-permute-start(bf16[32,528]{1,0:T(8,128)(2,1)S(1)} %get-tuple-element.15), channel_id=1, source_target_pairs={{0,24},{8,0},{16,8},{24,16},{1,25},{9,1},{17,9},{25,17},{2,26},{10... | collective-permute-start | bytes 101384 | tf_op jit(solution)/shard_map/ppermute | solution.py:307
  16.0 0.1 multiply_sine_fusion.1
  16.2 0.0 copy-done.4
  16.2 0.0 copy-done.5
  16.2 0.0 copy-done.6
  16.2 0.0 copy-done.2
  16.2 0.9 prepare.1
  17.1 0.0 all-gather.7.cloned.1.call-update
  17.1 0.0 all-gather.5.cloned.1.call-start
  17.2 2.3 %collective-permute-start.1 = (bf16[32,528]{1,0:T(8,128)(2,1)S(1)}, bf16[32,528]{1,0:T(8,128)(2,1)S(1)}, u32[]{:S(2)}, u32[]{:S(2)}) collective-permute-start(bf16[32,528]{1,0:T(8,128)(2,1)S(1)} %get-tuple-element.14), channel_id=1, source_target_pairs={{0,16},{8,24},{16,0},{24,8},{1,17},{9,25},{17,1},{25,9},{2,18},{10... | collective-permute-start | bytes 101384 | tf_op jit(solution)/shard_map/ppermute | solution.py:307
  19.4 2.6 %collective-permute-start.2 = (bf16[32,528]{1,0:T(8,128)(2,1)S(1)}, bf16[32,528]{1,0:T(8,128)(2,1)S(1)}, u32[]{:S(2)}, u32[]{:S(2)}) collective-permute-start(bf16[32,528]{1,0:T(8,128)(2,1)S(1)} %get-tuple-element.13), channel_id=1, source_target_pairs={{0,8},{8,16},{16,24},{24,0},{1,9},{9,17},{17,25},{25,1},{2,10},{10... | collective-permute-start | bytes 101384 | tf_op jit(solution)/shard_map/ppermute | solution.py:307
  22.1 0.0 collective-permute-done
  22.1 1.4 collective-permute-done.1
  23.4 2.0 %collective-permute-done.2 = bf16[32,528]{1,0:T(8,128)(2,1)S(1)} collective-permute-done((bf16[32,528]{1,0:T(8,128)(2,1)S(1)}, bf16[32,528]{1,0:T(8,128)(2,1)S(1)}, u32[]{:S(2)}, u32[]{:S(2)}) %collective-permute-start.2) | collective-permute-done | bytes 33824 | tf_op jit(solution)/shard_map/ppermute | solution.py:307
  25.5 0.8 copy.27
  26.3 0.0 all-gather.5.cloned.1.call-update
  26.3 14.9 %all-to-all-start = ((bf16[16,24,320]{2,1,0:T(8,128)(2,1)}), bf16[16,24,320]{2,1,0:T(8,128)(2,1)S(1)}, u32[]{:S(2)}, u32[]{:S(2)}) async-start(bf16[16,24,320]{2,1,0:T(8,128)(2,1)} %get-tuple-element.9), calls=%async_computation | async-start | bytes 589824 | tf_op jit(solution)/shard_map/all_to_all | solution.py:304
  41.2 0.0 copy-start.8
  41.3 0.0 copy-start.9
  41.3 0.4 multiply_sine_fusion
  41.7 0.2 pad_maximum_fusion
  42.0 12.3 %all-to-all-done = bf16[16,24,320]{2,1,0:T(8,128)(2,1)S(1)} async-done(((bf16[16,24,320]{2,1,0:T(8,128)(2,1)}), bf16[16,24,320]{2,1,0:T(8,128)(2,1)S(1)}, u32[]{:S(2)}, u32[]{:S(2)}) %all-to-all-start) | async-done | bytes 245792 | tf_op jit(solution)/shard_map/all_to_all | solution.py:304
  54.3 11.5 %all_gather.18.lat_ref = bf16[1536,320]{1,0:T(8,128)(2,1)S(1)} all-gather(bf16[384,320]{1,0:T(8,128)(2,1)S(1)} %bitcast.36), channel_id=1, replica_groups=mesh['z'=16,'y'=4,'x'=4,'c'=2] {'y'}, dimensions={0}, use_global_device_ids=true | all-gather | bytes 1228800 | tf_op jit(solution)/shard_map/all_gather | solution.py:315
  65.8 0.3 broadcast_in_dim.2.seg_ref
  66.1 1.2 copy-done.7
  67.3 8.5 %attend.1 = bf16[8,208,128]{2,1,0:T(8,128)(2,1)S(1)} custom-call(bf16[192,1024]{1,0:T(8,128)(2,1)S(1)} %copy-done.8, bf16[192,512]{1,0:T(8,128)(2,1)S(1)} %copy-done.9, f32[192,128]{1,0:T(8,128)S(1)} %get-tuple-element.20.cos_ref, f32[192,128]{1,0:T(8,128)S(1)} %get-tuple-element.21.sin_ref, bf16[1536,320]{1,0:T(8,128)(2,1)S(1)} %all_gather.18.lat_ref, ...), custom_call_target="tpu_custom_call" | custom-call | flops 3000000000 | bytes 4000000 | tf_op jit(solution)/shard_map/attend/pallas_call | solution.py:123
  75.8 0.0 copy-start
  75.8 0.0 copy-start.1
  75.9 22.9 %all_to_all.20.in_ref = bf16[8,208,128]{2,1,0:T(8,128)(2,1)S(1)} all-to-all(bf16[8,208,128]{2,1,0:T(8,128)(2,1)S(1)} %attend.1), channel_id=1, replica_groups=mesh['z'=16,'y'=4,'x'=4,'c'=2] {'x','c'}, dimensions={0} | all-to-all | bytes 851968 | tf_op jit(solution)/shard_map/all_to_all | solution.py:325
  98.7 0.6 merge.1
  99.3 13.7 %all-gather.1 = bf16[1536,128]{1,0:T(8,128)(2,1)S(1)} all-gather(bf16[192,128]{1,0:T(8,128)(2,1)S(1)} %merge.1), channel_id=3, replica_groups=mesh['z'=16,'y'=4,'x'=4,'c'=2] {'x','c'}, dimensions={0}, use_global_device_ids=true | all-gather | bytes 442368 | tf_op jit(solution)/shard_map/all_gather | solution.py:326
  113.0 0.0 copy-done
  113.0 0.4 project.1
  113.4 26.5 %all_to_all.21.rows_ref = bf16[32,96,256]{2,1,0:T(8,128)(2,1)} all-to-all(bf16[32,96,256]{2,1,0:T(8,128)(2,1)S(1)} %get-tuple-element.12), channel_id=1, replica_groups=mesh['z'=16,'y'=4,'x'=4,'c'=2] {'y','x','c'}, dimensions={0} | all-to-all | bytes 3145728 | tf_op jit(solution)/shard_map/all_to_all | solution.py:328
  139.9 7.5 %mix.1 = bf16[32,96,256]{2,1,0:T(8,128)(2,1)} custom-call(bf16[32,96,256]{2,1,0:T(8,128)(2,1)} %all_to_all.21.rows_ref, f32[1,2048]{1,0:T(1,128)} %bitcast.39, bf16[16,1056,128]{2,1,0:T(8,128)(2,1)} %bitcast.35), custom_call_target="tpu_custom_call" | custom-call | flops 1700000000 | bytes 8000000 | tf_op jit(solution)/shard_map/mix/pallas_call | solution.py:230
  147.5 26.8 %all_to_all.22 = bf16[32,96,256]{2,1,0:T(8,128)(2,1)S(1)} all-to-all(bf16[32,96,256]{2,1,0:T(8,128)(2,1)} %mix.1), channel_id=1, replica_groups=mesh['z'=16,'y'=4,'x'=4,'c'=2] {'y','x','c'}, dimensions={0} | all-to-all | bytes 3145728 | tf_op jit(solution)/shard_map/all_to_all | solution.py:330
  174.3 0.2 convert_reduce_fusion
  174.5 0.7 add_convert_fusion
  (26 shorter events, 0.2 us)
Async XLA Ops:
  6.5 9.6 %copy-start.4 = (bf16[24,256]{1,0:T(8,128)(2,1)S(1)}, bf16[24,256]{1,0:T(8,128)(2,1)}, u32[]{:S(2)}) copy-start(bf16[24,256]{1,0:T(8,128)(2,1)} %lat_ref.1) | copy-start | bytes 36868
  6.5 9.7 %copy-start.5 = (bf16[24,64]{1,0:T(8,128)(2,1)S(1)}, bf16[24,64]{1,0:T(8,128)(2,1)}, u32[]{:S(2)}) copy-start(bf16[24,64]{1,0:T(8,128)(2,1)} %rot_ref.1) | copy-start | bytes 9220
  6.5 9.7 %copy-start.6 = (f32[256]{0:T(256)S(1)}, f32[256]{0:T(256)}, u32[]{:S(2)}) copy-start(f32[256]{0:T(256)} %param.17) | copy-start | bytes 3076
  6.5 9.7 %copy-start.2 = (bf16[256,128]{1,0:T(8,128)(2,1)S(1)}, bf16[256,128]{1,0:T(8,128)(2,1)}, u32[]{:S(2)}) copy-start(bf16[256,128]{1,0:T(8,128)(2,1)} %k_ref.1) | copy-start | bytes 196612
  6.5 9.7 %copy-start.3 = (bf16[256,128]{1,0:T(8,128)(2,1)S(1)}, bf16[256,128]{1,0:T(8,128)(2,1)}, u32[]{:S(2)}) copy-start(bf16[256,128]{1,0:T(8,128)(2,1)} %v_ref.1) | copy-start | bytes 196612
  6.5 59.2 %all-gather.7.cloned.1.call-start = ((), (), s32[]{:S(2)}) async-start(), calls=%async_computation.5 | async-start | bytes 1179648 | tf_op jit(solution)/shard_map/all_gather | solution.py:299
  10.5 11.5 %collective-permute-start = (bf16[32,528]{1,0:T(8,128)(2,1)S(1)}, bf16[32,528]{1,0:T(8,128)(2,1)S(1)}, u32[]{:S(2)}, u32[]{:S(2)}) collective-permute-start(bf16[32,528]{1,0:T(8,128)(2,1)S(1)} %get-tuple-element.15), channel_id=1, source_target_pairs={{0,24},{8,0},{16,8},{24,16},{1,25},{9,1},{17,9},{25,17},{2,26},{10... | collective-permute-start | bytes 101384 | tf_op jit(solution)/shard_map/ppermute | solution.py:307
  17.1 122.8 %all-gather.5.cloned.1.call-start = ((), (), s32[]{:S(2)}) async-start(), calls=%async_computation.4 | async-start | bytes 4460544 | tf_op jit(solution)/shard_map/all_gather | solution.py:311
  17.2 6.3 %collective-permute-start.1 = (bf16[32,528]{1,0:T(8,128)(2,1)S(1)}, bf16[32,528]{1,0:T(8,128)(2,1)S(1)}, u32[]{:S(2)}, u32[]{:S(2)}) collective-permute-start(bf16[32,528]{1,0:T(8,128)(2,1)S(1)} %get-tuple-element.14), channel_id=1, source_target_pairs={{0,16},{8,24},{16,0},{24,8},{1,17},{9,25},{17,1},{25,9},{2,18},{10... | collective-permute-start | bytes 101384 | tf_op jit(solution)/shard_map/ppermute | solution.py:307
  19.4 6.0 %collective-permute-start.2 = (bf16[32,528]{1,0:T(8,128)(2,1)S(1)}, bf16[32,528]{1,0:T(8,128)(2,1)S(1)}, u32[]{:S(2)}, u32[]{:S(2)}) collective-permute-start(bf16[32,528]{1,0:T(8,128)(2,1)S(1)} %get-tuple-element.13), channel_id=1, source_target_pairs={{0,8},{8,16},{16,24},{24,0},{1,9},{9,17},{17,25},{25,1},{2,10},{10... | collective-permute-start | bytes 101384 | tf_op jit(solution)/shard_map/ppermute | solution.py:307
  26.3 28.0 %all-to-all-start = ((bf16[16,24,320]{2,1,0:T(8,128)(2,1)}), bf16[16,24,320]{2,1,0:T(8,128)(2,1)S(1)}, u32[]{:S(2)}, u32[]{:S(2)}) async-start(bf16[16,24,320]{2,1,0:T(8,128)(2,1)} %get-tuple-element.9), calls=%async_computation | async-start | bytes 589824 | tf_op jit(solution)/shard_map/all_to_all | solution.py:304
  41.2 24.8 %copy-start.8 = (bf16[192,1024]{1,0:T(8,128)(2,1)S(1)}, bf16[192,1024]{1,0:T(8,128)(2,1)}, u32[]{:S(2)}) copy-start(bf16[192,1024]{1,0:T(8,128)(2,1)} %q_ref.1) | copy-start | bytes 1179652
  41.3 24.8 %copy-start.9 = (bf16[192,512]{1,0:T(8,128)(2,1)S(1)}, bf16[192,512]{1,0:T(8,128)(2,1)}, u32[]{:S(2)}) copy-start(bf16[192,512]{1,0:T(8,128)(2,1)} %qr_ref.1) | copy-start | bytes 589828
  66.1 1.2 copy-start.7
  75.8 37.2 %copy-start = (bf16[1024,256]{1,0:T(8,128)(2,1)S(1)}, bf16[1024,256]{1,0:T(8,128)(2,1)}, u32[]{:S(2)}) copy-start(bf16[1024,256]{1,0:T(8,128)(2,1)} %w_ref.1) | copy-start | bytes 1572868
  75.8 37.2 %copy-start.1 = (bf16[192,256]{1,0:T(8,128)(2,1)S(1)}, bf16[192,256]{1,0:T(8,128)(2,1)}, u32[]{:S(2)}) copy-start(bf16[192,256]{1,0:T(8,128)(2,1)} %res_ref.1) | copy-start | bytes 294916
Sparse Core Ops, SparseCore 0:
  17.3 33.7 all-gather.6
  53.2 73.3 all-gather.4

commit v3 on v2

--- a/solution.py
+++ b/solution.py
@@ -31,7 +31,15 @@
     return jnp.cos(angles), jnp.sin(angles)
 
 
-def prepare_kernel(lat_ref, rot_ref, gain_ref, cos_ref, sin_ref, k_ref, v_ref, out_ref, kv_ref):
+def prepare_kernel(
+    y_ref, lat_ref, rot_ref, gain_ref, cos_ref, sin_ref, k_ref, v_ref, gate_ref, up_ref, down_ref,
+    out_ref, kv_ref, cut_ref,
+):
+    for k in range(NY):
+        block = slice(k * 176, (k + 1) * 176)
+        cut_ref[(k + NY - y_ref[0]) % NY] = jnp.concatenate(
+            [gate_ref[:, block], up_ref[:, block], down_ref[:, block]], axis=1
+        )
     kv_ref[:, :DN] = k_ref[...]
     kv_ref[:, DN:] = v_ref[...]
     widened = lat_ref[...].astype(jnp.float32)
@@ -53,11 +61,39 @@
         out_shape=(
             jax.ShapeDtypeStruct((NZ, 24, 320), jnp.bfloat16),
             jax.ShapeDtypeStruct((256, 256), jnp.bfloat16),
-        ),
-        compiler_params=pltpu.CompilerParams(vmem_limit_bytes=4 * 1024 * 1024),
+            jax.ShapeDtypeStruct((NY, 32, 528), jnp.bfloat16),
+        ),
+        in_specs=[pl.BlockSpec(memory_space=pltpu.SMEM)]
+        + [pl.BlockSpec(memory_space=pltpu.VMEM)] * 10,
+        compiler_params=pltpu.CompilerParams(vmem_limit_bytes=66_900_000),
         cost_estimate=pl.CostEstimate(flops=100_000, bytes_accessed=300_000, transcendentals=24),
         name="prepare",
     )(*inputs)
+
+
+def put_kernel(y_ref, a_ref, b_ref, c_ref, d_ref, out_ref, all_ref):
+    y = y_ref[0]
+    for s, ref in enumerate((a_ref, b_ref, c_ref, d_ref)):
+        all_ref[(y + NY - s) % NY, :, :528] = ref[...].astype(jnp.float32)
+    for k in range(5):
+        lanes = jnp.concatenate(
+            [all_ref[r, :, k * 128 : (k + 1) * 128] for r in range(NY)], axis=0
+        )
+        rows = min(128, 528 - k * 128)
+        out_ref[k * 128 : k * 128 + rows] = lanes.T[:rows].astype(jnp.bfloat16)
+
+
+def put(y, *pieces):
+    small = pl.BlockSpec(memory_space=pltpu.VMEM)
+    return pl.pallas_call(
+        put_kernel,
+        in_specs=[pl.BlockSpec(memory_space=pltpu.SMEM), small, small, small, small],
+        out_shape=jax.ShapeDtypeStruct((528, 128), jnp.bfloat16),
+        scratch_shapes=[pltpu.VMEM((NY, 32, 640), jnp.float32)],
+        compiler_params=pltpu.CompilerParams(vmem_limit_bytes=4 * 1024 * 1024),
+        cost_estimate=pl.CostEstimate(flops=100_000, bytes_accessed=300_000, transcendentals=0),
+        name="put",
+    )(y, *pieces)
 
 
 def attend_kernel(q_ref, qr_ref, cos_ref, sin_ref, lat_ref, seg_ref, w_ref, out_ref, key_ref):
@@ -168,13 +204,15 @@
         )
         column = jnp.concatenate([upper, lower], axis=0)
         acc = acc + column * in_ref[j, :TOK, :].astype(jnp.float32)
-    out_ref[...] = acc.astype(jnp.bfloat16)
+    merged = acc.astype(jnp.bfloat16)
+    for j in range(H):
+        out_ref[j] = merged
 
 
 def merge(parts):
     return pl.pallas_call(
         merge_kernel,
-        out_shape=jax.ShapeDtypeStruct((TOK, 128), jnp.bfloat16),
+        out_shape=jax.ShapeDtypeStruct((H, TOK, 128), jnp.bfloat16),
         compiler_params=pltpu.CompilerParams(vmem_limit_bytes=8 * 1024 * 1024),
         cost_estimate=pl.CostEstimate(flops=1_000_000, bytes_accessed=500_000, transcendentals=3000),
         name="merge",
@@ -293,21 +331,20 @@
 
     own_places = (sp_index * 8 + tp_index) * 24 + jnp.arange(24, dtype=jnp.int32)
     cosine, sine = tables(own_places)
-    own, kv = prepare(
-        latents, key_rotary, latent_gain.reshape(1, -1), cosine, sine, key_up, value_up
+    y_word = yi.reshape(1).astype(jnp.int32)
+    own, kv, ahead = prepare(
+        y_word, latents, key_rotary, latent_gain.reshape(1, -1), cosine, sine, key_up, value_up,
+        gate_proj, up_proj, down_proj.T,
     )
     kv = lax.all_gather(kv, ("x", "c"), axis=0, tiled=False)
 
-    stacked = jnp.stack([gate_proj, up_proj, down_proj.T])
-    slices = stacked.reshape(3, 32, NY, 176).transpose(2, 1, 0, 3).reshape(NY, 32, 528)
-    ahead = lax.dynamic_slice_in_dim(jnp.concatenate([slices, slices]), yi, NY, axis=0)
     lat = lax.all_to_all(own, "z", split_axis=0, concat_axis=0, tiled=True)
     lat = lat.reshape(NZ * 24, 320)
-    back = [ahead[0]] + [
-        lax.ppermute(ahead[s], "y", [(i, (i + s) % NY) for i in range(NY)]) for s in range(1, NY)
+    pieces = [ahead[s] for s in range(NY)]
+    back = [
+        lax.ppermute(pieces[s], "y", [(i, (i + s) % NY) for i in range(NY)]) for s in range(1, NY)
     ]
-    turn = jnp.stack(back[::-1] * 2)
-    own_slice = lax.dynamic_slice_in_dim(turn, NY - 1 - yi, NY, axis=0).reshape(128, 528).T
+    own_slice = put(y_word, pieces[0], *back)
     mixer = lax.all_gather(own_slice, ("z", "c"), axis=0, tiled=True).reshape(
         NZ, NC * 528, 128
     )
@@ -323,7 +360,7 @@
 
     parts = attend(query_content, query_rotary, cosine, sine, lat, seg, kv)
     parts = lax.all_to_all(parts, ("x", "c"), split_axis=0, concat_axis=0, tiled=True)
-    heads = lax.all_gather(merge(parts), ("x", "c"), axis=0, tiled=False)
+    heads = lax.all_to_all(merge(parts), ("x", "c"), split_axis=0, concat_axis=0, tiled=True)
     mixed_rows, sent = project(heads, out_proj, residual)
     rows = lax.all_to_all(sent, ("y", "x", "c"), split_axis=0, concat_axis=0, tiled=True)
     partial_sums = mix(rows, mixer_gain.reshape(1, -1), mixer)

time: 183 us -> 180 us (0.984)
  local copies, waits for them, and re-layouts: 5.66 us -> 2.36 us
  Pallas kernels: 17.9 us -> 19.8 us
    all_gather x1 -> x0, blocking collectives: 13.7 us -> none  [layer(): heads = lax.all_gather(merge(parts), ('x', 'c'), axis=0, tiled=False)]
    all_to_all x0 -> x1, blocking collectives: none -> 11.3 us  [layer(): lax.all_to_all(merge(parts), ('x', 'c'), split_axis=0, concat_axis=0, til...]
    another operation x7 -> x0, local copies, waits for them, and re-layouts: 3.09 us -> none  [the longest x6 3.07 us: layer(): stacked = jnp.stack([gate_proj, up_proj, down_proj.T])]
  transfers between devices with their start and end apart: 6 -> 6, of which waited for: 3 -> 2; matrix products, arithmetic and copies ran while one was open for 1% -> 1% of each run, Pallas kernels for 6% -> 6%
where the time goes in v3:
time: 180 us; the launch traced here: 179 us
  blocking collectives  101 us (56%)
  starting transfers between devices  26.3 us (15%)
  Pallas kernels  19.8 us (11%)
  waiting for transfers between devices  14.3 us (8%)
  between operations  13.6 us (8%)
  local copies, waits for them, and re-layouts  2.36 us (1%)
  other arithmetic  2.31 us (1%)
    all_to_all x1, blocking collectives, layer(): lax.all_to_all(sent, ('y', 'x', 'c'), split_axis=0, concat_axis=0, tiled=...  28 us
    all_to_all x1, blocking collectives, layer(): lax.all_to_all(partial_sums, ('y', 'x', 'c'), split_axis=0, concat_axis=0...  26.8 us
    all_to_all x1, blocking collectives, layer(): lax.all_to_all(parts, ('x', 'c'), split_axis=0, concat_axis=0, tiled=True)  22.6 us
    all_to_all x1, starting transfers between devices, layer(): lat = lax.all_to_all(own, 'z', split_axis=0, concat_axis=0, tiled=True)  14.7 us
    all_to_all x1, waiting for transfers between devices, layer(): lat = lax.all_to_all(own, 'z', split_axis=0, concat_axis=0, tiled=True)  12.3 us
    all_gather x1, blocking collectives, layer(): lat = lax.all_gather(lat, 'y', axis=0, tiled=True)  11.8 us
    ppermute x3, starting transfers between devices, layer(): lax.ppermute(pieces[s], 'y', [(i, (i + s) % NY) for i in range(NY)])  11.5 us
    all_to_all x1, blocking collectives, layer(): lax.all_to_all(merge(parts), ('x', 'c'), split_axis=0, concat_axis=0, til...  11.3 us
  transfers between devices with their start and end apart: 6, of which 2 were waited for; matrix products, arithmetic and copies ran while one was open for 1% of the time, Pallas kernels for 6%

profile of v3, /device:TPU:1, one launch (start us, length us, event | category | flops | bytes accessed | tf_op | source)
XLA Modules:
  0.0 179.2 jit_solution(10100764739109813017)
XLA Ops:
  6.5 0.0 all-gather.6.cloned.1.call-start
  6.6 0.7 multiply_sine_fusion.1
  7.3 1.9 %prepare.1 = (bf16[16,24,320]{2,1,0:T(8,128)(2,1)}, bf16[256,256]{1,0:T(8,128)(2,1)}, bf16[4,32,528]{2,1,0:T(8,128)(2,1)}) custom-call(s32[1]{0:T(128)} %bitcast.y_ref, bf16[24,256]{1,0:T(8,128)(2,1)} %lat_ref.1, bf16[24,64]{1,0:T(8,128)(2,1)} %rot_ref.1, f32[1,256]{1,0:T(1,128)} %bitcast.25, f32[24,32]{1,0:T(8,128)} %get-tuple-element.22.cos_ref, ...), custom_call_target="tpu_custom_call" | custom-call | flops 100000 | bytes 300000 | tf_op jit(solution)/shard_map/prepare/pallas_call | solution.py:59
  9.2 0.0 all-gather.6.cloned.1.call-update
  9.2 0.0 all-gather.4.cloned.1.call-start
  9.3 0.9 slice_bitcast_fusion
  10.2 4.0 %collective-permute-start = (bf16[32,528]{1,0:T(8,128)(2,1)S(1)}, bf16[32,528]{1,0:T(8,128)(2,1)S(1)}, u32[]{:S(2)}, u32[]{:S(2)}) collective-permute-start(bf16[32,528]{1,0:T(8,128)(2,1)S(1)} %get-tuple-element.17), channel_id=1, source_target_pairs={{0,8},{8,16},{16,24},{24,0},{1,9},{9,17},{17,25},{25,1},{2,10},{10... | collective-permute-start | bytes 101384 | tf_op jit(solution)/shard_map/ppermute | solution.py:345
  14.2 4.5 %collective-permute-start.1 = (bf16[32,528]{1,0:T(8,128)(2,1)S(1)}, bf16[32,528]{1,0:T(8,128)(2,1)S(1)}, u32[]{:S(2)}, u32[]{:S(2)}) collective-permute-start(bf16[32,528]{1,0:T(8,128)(2,1)S(1)} %get-tuple-element.16), channel_id=1, source_target_pairs={{0,16},{8,24},{16,0},{24,8},{1,17},{9,25},{17,1},{25,9},{2,18},{10... | collective-permute-start | bytes 101384 | tf_op jit(solution)/shard_map/ppermute | solution.py:345
  18.7 3.0 %collective-permute-start.2 = (bf16[32,528]{1,0:T(8,128)(2,1)S(1)}, bf16[32,528]{1,0:T(8,128)(2,1)S(1)}, u32[]{:S(2)}, u32[]{:S(2)}) collective-permute-start(bf16[32,528]{1,0:T(8,128)(2,1)S(1)} %get-tuple-element.15), channel_id=1, source_target_pairs={{0,24},{8,0},{16,8},{24,16},{1,25},{9,1},{17,9},{25,17},{2,26},{10... | collective-permute-start | bytes 101384 | tf_op jit(solution)/shard_map/ppermute | solution.py:345
  21.7 0.0 collective-permute-done.b_ref
  21.7 0.0 collective-permute-done.1.c_ref
  21.7 2.0 %collective-permute-done.2.d_ref = bf16[32,528]{1,0:T(8,128)(2,1)S(1)} collective-permute-done((bf16[32,528]{1,0:T(8,128)(2,1)S(1)}, bf16[32,528]{1,0:T(8,128)(2,1)S(1)}, u32[]{:S(2)}, u32[]{:S(2)}) %collective-permute-start.2) | collective-permute-done | bytes 33824 | tf_op jit(solution)/shard_map/ppermute | solution.py:345
  23.7 0.8 put.1
  24.5 0.0 all-gather.4.cloned.1.call-update
  24.5 14.7 %all-to-all-start = ((bf16[16,24,320]{2,1,0:T(8,128)(2,1)}), bf16[16,24,320]{2,1,0:T(8,128)(2,1)S(1)}, u32[]{:S(2)}, u32[]{:S(2)}) async-start(bf16[16,24,320]{2,1,0:T(8,128)(2,1)} %get-tuple-element.10), calls=%async_computation | async-start | bytes 589824 | tf_op jit(solution)/shard_map/all_to_all | solution.py:341
  39.2 0.0 copy-start.3
  39.2 0.0 copy-start.4
  39.3 0.4 multiply_sine_fusion
  39.7 0.2 pad_maximum_fusion
  39.9 12.3 %all-to-all-done = bf16[16,24,320]{2,1,0:T(8,128)(2,1)S(1)} async-done(((bf16[16,24,320]{2,1,0:T(8,128)(2,1)}), bf16[16,24,320]{2,1,0:T(8,128)(2,1)S(1)}, u32[]{:S(2)}, u32[]{:S(2)}) %all-to-all-start) | async-done | bytes 245792 | tf_op jit(solution)/shard_map/all_to_all | solution.py:341
  52.2 11.8 %all_gather.12.lat_ref = bf16[1536,320]{1,0:T(8,128)(2,1)S(1)} all-gather(bf16[384,320]{1,0:T(8,128)(2,1)S(1)} %bitcast.22), channel_id=1, replica_groups=mesh['z'=16,'y'=4,'x'=4,'c'=2] {'y'}, dimensions={0}, use_global_device_ids=true | all-gather | bytes 1228800 | tf_op jit(solution)/shard_map/all_gather | solution.py:352
  64.0 0.0 all-gather.6.cloned.1.call-done
  64.0 0.3 broadcast_in_dim.2.seg_ref
  64.3 0.0 copy-done.3
  64.3 0.0 copy-done.4
  64.3 0.0 copy-start.2
  64.3 1.2 copy-done.2
  65.5 8.5 %attend.1 = bf16[8,208,128]{2,1,0:T(8,128)(2,1)S(1)} custom-call(bf16[192,1024]{1,0:T(8,128)(2,1)S(1)} %copy-done.3, bf16[192,512]{1,0:T(8,128)(2,1)S(1)} %copy-done.4, f32[192,128]{1,0:T(8,128)S(1)} %get-tuple-element.23.cos_ref, f32[192,128]{1,0:T(8,128)S(1)} %get-tuple-element.24.sin_ref, bf16[1536,320]{1,0:T(8,128)(2,1)S(1)} %all_gather.12.lat_ref, ...), custom_call_target="tpu_custom_call" | custom-call | flops 3000000000 | bytes 4000000 | tf_op jit(solution)/shard_map/attend/pallas_call | solution.py:159
  74.1 0.0 copy-start
  74.1 0.0 copy-start.1
  74.1 22.6 %all_to_all.25.in_ref = bf16[8,208,128]{2,1,0:T(8,128)(2,1)S(1)} all-to-all(bf16[8,208,128]{2,1,0:T(8,128)(2,1)S(1)} %attend.1), channel_id=1, replica_groups=mesh['z'=16,'y'=4,'x'=4,'c'=2] {'x','c'}, dimensions={0} | all-to-all | bytes 851968 | tf_op jit(solution)/shard_map/all_to_all | solution.py:362
  96.7 0.6 merge.1
  97.3 11.3 %all_to_all.26.heads_ref = bf16[8,192,128]{2,1,0:T(8,128)(2,1)S(1)} all-to-all(bf16[8,192,128]{2,1,0:T(8,128)(2,1)S(1)} %merge.1), channel_id=1, replica_groups=mesh['z'=16,'y'=4,'x'=4,'c'=2] {'x','c'}, dimensions={0} | all-to-all | bytes 786432 | tf_op jit(solution)/shard_map/all_to_all | solution.py:363
  108.6 0.0 copy-done
  108.6 0.0 copy-done.1
  108.6 0.4 project.1
  109.0 28.0 %all_to_all.27.rows_ref = bf16[32,96,256]{2,1,0:T(8,128)(2,1)} all-to-all(bf16[32,96,256]{2,1,0:T(8,128)(2,1)S(1)} %get-tuple-element.13), channel_id=1, replica_groups=mesh['z'=16,'y'=4,'x'=4,'c'=2] {'y','x','c'}, dimensions={0} | all-to-all | bytes 3145728 | tf_op jit(solution)/shard_map/all_to_all | solution.py:365
  137.1 0.0 all-gather.4.cloned.1.call-done
  137.1 7.6 %mix.1 = bf16[32,96,256]{2,1,0:T(8,128)(2,1)} custom-call(bf16[32,96,256]{2,1,0:T(8,128)(2,1)} %all_to_all.27.rows_ref, f32[1,2048]{1,0:T(1,128)} %bitcast.24, bf16[16,1056,128]{2,1,0:T(8,128)(2,1)} %bitcast.21), custom_call_target="tpu_custom_call" | custom-call | flops 1700000000 | bytes 8000000 | tf_op jit(solution)/shard_map/mix/pallas_call | solution.py:268
  144.6 26.8 %all_to_all.28 = bf16[32,96,256]{2,1,0:T(8,128)(2,1)S(1)} all-to-all(bf16[32,96,256]{2,1,0:T(8,128)(2,1)} %mix.1), channel_id=1, replica_groups=mesh['z'=16,'y'=4,'x'=4,'c'=2] {'y','x','c'}, dimensions={0} | all-to-all | bytes 3145728 | tf_op jit(solution)/shard_map/all_to_all | solution.py:367
  171.4 0.2 convert_reduce_fusion
  171.7 0.7 add_convert_fusion
  (4 shorter events, 0.1 us)
Async XLA Ops:
  6.5 57.5 %all-gather.6.cloned.1.call-start = ((), (), s32[]{:S(2)}) async-start(), calls=%async_computation.6 | async-start | bytes 1179648 | tf_op jit(solution)/shard_map/all_gather | solution.py:339
  9.2 127.8 %all-gather.4.cloned.1.call-start = ((), (), s32[]{:S(2)}) async-start(), calls=%async_computation.5 | async-start | bytes 4460544 | tf_op jit(solution)/shard_map/all_gather | solution.py:348
  10.2 11.6 %collective-permute-start = (bf16[32,528]{1,0:T(8,128)(2,1)S(1)}, bf16[32,528]{1,0:T(8,128)(2,1)S(1)}, u32[]{:S(2)}, u32[]{:S(2)}) collective-permute-start(bf16[32,528]{1,0:T(8,128)(2,1)S(1)} %get-tuple-element.17), channel_id=1, source_target_pairs={{0,8},{8,16},{16,24},{24,0},{1,9},{9,17},{17,25},{25,1},{2,10},{10... | collective-permute-start | bytes 101384 | tf_op jit(solution)/shard_map/ppermute | solution.py:345
  14.2 7.5 %collective-permute-start.1 = (bf16[32,528]{1,0:T(8,128)(2,1)S(1)}, bf16[32,528]{1,0:T(8,128)(2,1)S(1)}, u32[]{:S(2)}, u32[]{:S(2)}) collective-permute-start(bf16[32,528]{1,0:T(8,128)(2,1)S(1)} %get-tuple-element.16), channel_id=1, source_target_pairs={{0,16},{8,24},{16,0},{24,8},{1,17},{9,25},{17,1},{25,9},{2,18},{10... | collective-permute-start | bytes 101384 | tf_op jit(solution)/shard_map/ppermute | solution.py:345
  18.7 5.0 %collective-permute-start.2 = (bf16[32,528]{1,0:T(8,128)(2,1)S(1)}, bf16[32,528]{1,0:T(8,128)(2,1)S(1)}, u32[]{:S(2)}, u32[]{:S(2)}) collective-permute-start(bf16[32,528]{1,0:T(8,128)(2,1)S(1)} %get-tuple-element.15), channel_id=1, source_target_pairs={{0,24},{8,0},{16,8},{24,16},{1,25},{9,1},{17,9},{25,17},{2,26},{10... | collective-permute-start | bytes 101384 | tf_op jit(solution)/shard_map/ppermute | solution.py:345
  24.5 27.7 %all-to-all-start = ((bf16[16,24,320]{2,1,0:T(8,128)(2,1)}), bf16[16,24,320]{2,1,0:T(8,128)(2,1)S(1)}, u32[]{:S(2)}, u32[]{:S(2)}) async-start(bf16[16,24,320]{2,1,0:T(8,128)(2,1)} %get-tuple-element.10), calls=%async_computation | async-start | bytes 589824 | tf_op jit(solution)/shard_map/all_to_all | solution.py:341
  39.2 25.1 %copy-start.3 = (bf16[192,1024]{1,0:T(8,128)(2,1)S(1)}, bf16[192,1024]{1,0:T(8,128)(2,1)}, u32[]{:S(2)}) copy-start(bf16[192,1024]{1,0:T(8,128)(2,1)} %q_ref.1) | copy-start | bytes 1179652
  39.2 25.1 %copy-start.4 = (bf16[192,512]{1,0:T(8,128)(2,1)S(1)}, bf16[192,512]{1,0:T(8,128)(2,1)}, u32[]{:S(2)}) copy-start(bf16[192,512]{1,0:T(8,128)(2,1)} %qr_ref.1) | copy-start | bytes 589828
  64.3 1.2 copy-start.2
  74.1 34.5 %copy-start = (bf16[1024,256]{1,0:T(8,128)(2,1)S(1)}, bf16[1024,256]{1,0:T(8,128)(2,1)}, u32[]{:S(2)}) copy-start(bf16[1024,256]{1,0:T(8,128)(2,1)} %w_ref.1) | copy-start | bytes 1572868
  74.1 34.5 %copy-start.1 = (bf16[192,256]{1,0:T(8,128)(2,1)S(1)}, bf16[192,256]{1,0:T(8,128)(2,1)}, u32[]{:S(2)}) copy-start(bf16[192,256]{1,0:T(8,128)(2,1)} %res_ref.1) | copy-start | bytes 294916
Sparse Core Ops, SparseCore 0:
  9.5 36.7 all-gather.5
  48.4 73.5 all-gather.3

commit v4 on v3

--- a/solution.py
+++ b/solution.py
@@ -19,6 +19,7 @@
 KEYS = 1536
 PAD = 208
 GROUP = 4
+ROWS = KEYS // 3
 
 epsilon = 1e-06
 masked_score = -1e30
@@ -50,16 +51,17 @@
     cosine, sine = cos_ref[...], sin_ref[...]
     turned = jnp.concatenate([a * cosine - b * sine, b * cosine + a * sine], axis=-1)
     turned = turned.astype(jnp.bfloat16)
+    keys = [slice(j * 8, (j + 1) * 8) for j in range(3)]
+    row = jnp.concatenate([normed[k] for k in keys] + [turned[k] for k in keys], axis=1)
     for z in range(NZ):
-        out_ref[z, :, :256] = normed
-        out_ref[z, :, 256:] = turned
+        out_ref[z] = row
 
 
 def prepare(*inputs):
     return pl.pallas_call(
         prepare_kernel,
         out_shape=(
-            jax.ShapeDtypeStruct((NZ, 24, 320), jnp.bfloat16),
+            jax.ShapeDtypeStruct((NZ, 8, 960), jnp.bfloat16),
             jax.ShapeDtypeStruct((256, 256), jnp.bfloat16),
             jax.ShapeDtypeStruct((NY, 32, 528), jnp.bfloat16),
         ),
@@ -101,12 +103,13 @@
 
     @pl.when(pl.program_id(0) == 0)
     def _():
-        lane = lax.broadcasted_iota(jnp.int32, (KEYS, 64), 1)
-        mask = jnp.where(seg_ref[:, :64] > lane, masked_score, 0.0)
-        mask = jnp.where(lane < TOK // SPAN, mask, 0.0).astype(jnp.bfloat16)
-        for h in range(GROUP):
-            key_ref[h, :, DN : DN + DR] = lat_ref[:, 256:320]
-            key_ref[h, :, DN + DR :] = mask
+        low = lax.broadcasted_iota(jnp.int32, (ROWS, 128), 1) < DR
+        for j in range(3):
+            rows = slice(j * ROWS, (j + 1) * ROWS)
+            pair = lat_ref[:, 768 + j * DR : 832 + j * DR]
+            tail = jnp.where(low, jnp.concatenate([pair, pair], axis=1), seg_ref[rows])
+            for h in range(GROUP):
+                key_ref[h, rows, DN:] = tail
 
     turned = qr_ref[...].astype(jnp.float32)
     lane = lax.broadcasted_iota(jnp.int32, turned.shape, 1)
@@ -121,12 +124,20 @@
     row = lax.broadcasted_iota(jnp.int32, (TOK, 64), 0)
     col = lax.broadcasted_iota(jnp.int32, (TOK, 64), 1)
     segment = jnp.where(row // SPAN == col, 1.0, 0.0).astype(jnp.bfloat16)
-    normed = lat_ref[:, :256]
     ones = jnp.ones((KEYS, 128), jnp.bfloat16)
     r128 = lax.broadcasted_iota(jnp.int32, (128, 128), 0)
     c128 = lax.broadcasted_iota(jnp.int32, (128, 128), 1)
     for h in range(GROUP):
-        pair = jnp.dot(normed, w_ref[h], preferred_element_type=jnp.float32).astype(jnp.bfloat16)
+        pair = jnp.concatenate(
+            [
+                jnp.dot(
+                    lat_ref[:, j * 256 : (j + 1) * 256], w_ref[h],
+                    preferred_element_type=jnp.float32,
+                ).astype(jnp.bfloat16)
+                for j in range(3)
+            ],
+            axis=0,
+        )
         query = jnp.concatenate(
             [q_ref[:, h * DN : (h + 1) * DN], turned[:, h * DR : (h + 1) * DR], segment], axis=1
         )
@@ -164,7 +175,7 @@
             pl.BlockSpec((TOK, GROUP * DR), lambda i: (0, i)),
             pl.BlockSpec((TOK, 2 * DR), lambda i: (0, 0)),
             pl.BlockSpec((TOK, 2 * DR), lambda i: (0, 0)),
-            pl.BlockSpec((KEYS, 320), lambda i: (0, 0)),
+            pl.BlockSpec((ROWS, 960), lambda i: (0, 0)),
             pl.BlockSpec((KEYS, 128), lambda i: (0, 0)),
             pl.BlockSpec((GROUP, 256, 256), lambda i: (i, 0, 0)),
         ],
@@ -275,7 +286,7 @@
             pltpu.VMEM((1056, 2048), jnp.bfloat16),
             pltpu.SemaphoreType.DMA((NZ,)),
         ],
-        compiler_params=pltpu.CompilerParams(vmem_limit_bytes=63_200_000),
+        compiler_params=pltpu.CompilerParams(vmem_limit_bytes=52_000_000),
         cost_estimate=pl.CostEstimate(
             flops=1_700_000_000, bytes_accessed=8_000_000, transcendentals=140_000
         ),
@@ -339,7 +350,7 @@
     kv = lax.all_gather(kv, ("x", "c"), axis=0, tiled=False)
 
     lat = lax.all_to_all(own, "z", split_axis=0, concat_axis=0, tiled=True)
-    lat = lat.reshape(NZ * 24, 320)
+    lat = lat.reshape(NZ * 8, 960)
     pieces = [ahead[s] for s in range(NY)]
     back = [
         lax.ppermute(pieces[s], "y", [(i, (i + s) % NY) for i in range(NY)]) for s in range(1, NY)
@@ -352,9 +363,12 @@
     lat = lax.all_gather(lat, "y", axis=0, tiled=True)
 
     index = jnp.arange(KEYS, dtype=jnp.int32)
-    y_of, z_of, i_of = index // 384, index // 24 % NZ, index % 24
+    y_of, z_of, i_of = index // 128 % NY, index // 8 % NZ, index // 512 * 8 + index % 8
     key_segment = (((z_of * NY + y_of) * 8 + tp_index) * 24 + i_of) // SPAN
-    seg = jnp.broadcast_to((key_segment - sp_index * (TOK // SPAN))[:, None], (KEYS, 128))
+    ahead_of = (key_segment - sp_index * (TOK // SPAN))[:, None]
+    lane = jnp.arange(128, dtype=jnp.int32)[None, :] - DR
+    hidden_from = (lane >= 0) & (lane < TOK // SPAN) & (ahead_of > lane)
+    seg = jnp.where(hidden_from, masked_score, 0.0).astype(jnp.bfloat16)
     cosine, sine = tables(sp_index * TOK + jnp.arange(TOK, dtype=jnp.int32))
     cosine, sine = (jnp.concatenate([t] * 4, axis=1) for t in (cosine, sine))
 

time: 180 us -> 175 us (0.972)
  Pallas kernels: 19.8 us -> 16.5 us
    pallas_call x1, Pallas kernels: 7.56 us -> 5.02 us  [mix(): pl.pallas_call(mix_kernel, in_specs=[whole, whole, pl.BlockSpec(memory_sp...]
  transfers between devices with their start and end apart: 6 -> 6, of which waited for: 2 -> 2; matrix products, arithmetic and copies ran while one was open for 1% -> 1% of each run, Pallas kernels for 6% -> 5%
where the time goes in v4:
time: 175 us; the launch traced here: 174 us
  blocking collectives  99.3 us (57%)
  starting transfers between devices  26.4 us (15%)
  Pallas kernels  16.5 us (9%)
  waiting for transfers between devices  13.7 us (8%)
  between operations  13.6 us (8%)
  other arithmetic  2.58 us (1%)
  local copies, waits for them, and re-layouts  2.14 us (1%)
    all_to_all x1, blocking collectives, layer(): lax.all_to_all(sent, ('y', 'x', 'c'), split_axis=0, concat_axis=0, tiled=...  27.9 us
    all_to_all x1, blocking collectives, layer(): lax.all_to_all(partial_sums, ('y', 'x', 'c'), split_axis=0, concat_axis=0...  26.3 us
    all_to_all x1, blocking collectives, layer(): lax.all_to_all(parts, ('x', 'c'), split_axis=0, concat_axis=0, tiled=True)  22.3 us
    all_to_all x1, starting transfers between devices, layer(): lat = lax.all_to_all(own, 'z', split_axis=0, concat_axis=0, tiled=True)  14.8 us
    all_to_all x1, waiting for transfers between devices, layer(): lat = lax.all_to_all(own, 'z', split_axis=0, concat_axis=0, tiled=True)  11.7 us
    ppermute x3, starting transfers between devices, layer(): lax.ppermute(pieces[s], 'y', [(i, (i + s) % NY) for i in range(NY)])  11.5 us
    all_gather x1, blocking collectives, layer(): lat = lax.all_gather(lat, 'y', axis=0, tiled=True)  11.5 us
    all_to_all x1, blocking collectives, layer(): lax.all_to_all(merge(parts), ('x', 'c'), split_axis=0, concat_axis=0, til...  11.3 us
  transfers between devices with their start and end apart: 6, of which 2 were waited for; matrix products, arithmetic and copies ran while one was open for 1% of the time, Pallas kernels for 5%

profile of v4, /device:TPU:1, one launch (start us, length us, event | category | flops | bytes accessed | tf_op | source)
XLA Modules:
  0.0 174.3 jit_solution(17001178262868932526)
XLA Ops:
  6.5 0.0 all-gather.6.cloned.1.call-start
  6.6 0.7 multiply_sine_fusion.1
  7.3 2.0 %prepare.1 = (bf16[16,8,960]{2,1,0:T(8,128)(2,1)}, bf16[256,256]{1,0:T(8,128)(2,1)}, bf16[4,32,528]{2,1,0:T(8,128)(2,1)}) custom-call(s32[1]{0:T(128)} %bitcast.y_ref, bf16[24,256]{1,0:T(8,128)(2,1)} %lat_ref.1, bf16[24,64]{1,0:T(8,128)(2,1)} %rot_ref.1, f32[1,256]{1,0:T(1,128)} %bitcast.25, f32[24,32]{1,0:T(8,128)} %get-tuple-element.22.cos_ref, ...), custom_call_target="tpu_custom_call" | custom-call | flops 100000 | bytes 300000 | tf_op jit(solution)/shard_map/prepare/pallas_call | solution.py:61
  9.3 0.0 all-gather.6.cloned.1.call-update
  9.3 0.0 all-gather.4.cloned.1.call-start
  9.4 0.9 slice_bitcast_fusion
  10.2 4.0 %collective-permute-start = (bf16[32,528]{1,0:T(8,128)(2,1)S(1)}, bf16[32,528]{1,0:T(8,128)(2,1)S(1)}, u32[]{:S(2)}, u32[]{:S(2)}) collective-permute-start(bf16[32,528]{1,0:T(8,128)(2,1)S(1)} %get-tuple-element.17), channel_id=1, source_target_pairs={{0,8},{8,16},{16,24},{24,0},{1,9},{9,17},{17,25},{25,1},{2,10},{10... | collective-permute-start | bytes 101384 | tf_op jit(solution)/shard_map/ppermute | solution.py:356
  14.2 4.5 %collective-permute-start.1 = (bf16[32,528]{1,0:T(8,128)(2,1)S(1)}, bf16[32,528]{1,0:T(8,128)(2,1)S(1)}, u32[]{:S(2)}, u32[]{:S(2)}) collective-permute-start(bf16[32,528]{1,0:T(8,128)(2,1)S(1)} %get-tuple-element.16), channel_id=1, source_target_pairs={{0,16},{8,24},{16,0},{24,8},{1,17},{9,25},{17,1},{25,9},{2,18},{10... | collective-permute-start | bytes 101384 | tf_op jit(solution)/shard_map/ppermute | solution.py:356
  18.8 3.0 %collective-permute-start.2 = (bf16[32,528]{1,0:T(8,128)(2,1)S(1)}, bf16[32,528]{1,0:T(8,128)(2,1)S(1)}, u32[]{:S(2)}, u32[]{:S(2)}) collective-permute-start(bf16[32,528]{1,0:T(8,128)(2,1)S(1)} %get-tuple-element.15), channel_id=1, source_target_pairs={{0,24},{8,0},{16,8},{24,16},{1,25},{9,1},{17,9},{25,17},{2,26},{10... | collective-permute-start | bytes 101384 | tf_op jit(solution)/shard_map/ppermute | solution.py:356
  21.8 0.0 collective-permute-done.b_ref
  21.8 0.0 collective-permute-done.1.c_ref
  21.8 2.0 %collective-permute-done.2.d_ref = bf16[32,528]{1,0:T(8,128)(2,1)S(1)} collective-permute-done((bf16[32,528]{1,0:T(8,128)(2,1)S(1)}, bf16[32,528]{1,0:T(8,128)(2,1)S(1)}, u32[]{:S(2)}, u32[]{:S(2)}) %collective-permute-start.2) | collective-permute-done | bytes 33824 | tf_op jit(solution)/shard_map/ppermute | solution.py:356
  23.8 0.8 put.1
  24.5 0.0 copy-start.4
  24.6 0.0 copy-start.5
  24.6 0.0 all-gather.4.cloned.1.call-update
  24.6 14.8 %all-to-all-start = ((bf16[16,8,960]{2,1,0:T(8,128)(2,1)}), bf16[16,8,960]{2,1,0:T(8,128)(2,1)S(1)}, u32[]{:S(2)}, u32[]{:S(2)}) async-start(bf16[16,8,960]{2,1,0:T(8,128)(2,1)} %get-tuple-element.10), calls=%async_computation | async-start | bytes 524288 | tf_op jit(solution)/shard_map/all_to_all | solution.py:352
  39.5 0.4 multiply_sine_fusion
  39.9 0.2 pad_maximum_fusion
  40.1 0.3 select_convert_fusion.seg_ref
  40.4 11.7 %all-to-all-done = bf16[16,8,960]{2,1,0:T(8,128)(2,1)S(1)} async-done(((bf16[16,8,960]{2,1,0:T(8,128)(2,1)}), bf16[16,8,960]{2,1,0:T(8,128)(2,1)S(1)}, u32[]{:S(2)}, u32[]{:S(2)}) %all-to-all-start) | async-done | bytes 245792 | tf_op jit(solution)/shard_map/all_to_all | solution.py:352
  52.1 11.5 %all_gather.12.lat_ref = bf16[512,960]{1,0:T(8,128)(2,1)S(1)} all-gather(bf16[128,960]{1,0:T(8,128)(2,1)S(1)} %bitcast.23), channel_id=1, replica_groups=mesh['z'=16,'y'=4,'x'=4,'c'=2] {'y'}, dimensions={0}, use_global_device_ids=true | all-gather | bytes 1228800 | tf_op jit(solution)/shard_map/all_gather | solution.py:363
  63.7 0.0 all-gather.6.cloned.1.call-done
  63.7 0.0 copy-done.4
  63.7 0.0 copy-done.5
  63.7 0.0 copy-start.3
  63.7 1.3 copy-done.3
  64.9 7.8 %attend.1 = bf16[8,208,128]{2,1,0:T(8,128)(2,1)S(1)} custom-call(bf16[192,1024]{1,0:T(8,128)(2,1)S(1)} %copy-done.4, bf16[192,512]{1,0:T(8,128)(2,1)S(1)} %copy-done.5, f32[192,128]{1,0:T(8,128)S(1)} %get-tuple-element.23.cos_ref, f32[192,128]{1,0:T(8,128)S(1)} %get-tuple-element.24.sin_ref, bf16[512,960]{1,0:T(8,128)(2,1)S(1)} %all_gather.12.lat_ref, ...), custom_call_target="tpu_custom_call" | custom-call | flops 3000000000 | bytes 4000000 | tf_op jit(solution)/shard_map/attend/pallas_call | solution.py:170
  72.7 0.0 copy-start
  72.7 0.0 copy-start.1
  72.8 22.3 %all_to_all.25.in_ref = bf16[8,208,128]{2,1,0:T(8,128)(2,1)S(1)} all-to-all(bf16[8,208,128]{2,1,0:T(8,128)(2,1)S(1)} %attend.1), channel_id=1, replica_groups=mesh['z'=16,'y'=4,'x'=4,'c'=2] {'x','c'}, dimensions={0} | all-to-all | bytes 851968 | tf_op jit(solution)/shard_map/all_to_all | solution.py:376
  95.1 0.6 merge.1
  95.6 11.3 %all_to_all.26.heads_ref = bf16[8,192,128]{2,1,0:T(8,128)(2,1)S(1)} all-to-all(bf16[8,192,128]{2,1,0:T(8,128)(2,1)S(1)} %merge.1), channel_id=1, replica_groups=mesh['z'=16,'y'=4,'x'=4,'c'=2] {'x','c'}, dimensions={0} | all-to-all | bytes 786432 | tf_op jit(solution)/shard_map/all_to_all | solution.py:377
  106.9 0.0 copy-done
  106.9 0.0 copy-done.1
  106.9 0.4 project.1
  107.3 0.0 copy-start.2
  107.3 27.9 %all_to_all.27.rows_ref = bf16[32,96,256]{2,1,0:T(8,128)(2,1)S(1)} all-to-all(bf16[32,96,256]{2,1,0:T(8,128)(2,1)S(1)} %get-tuple-element.13), channel_id=1, replica_groups=mesh['z'=16,'y'=4,'x'=4,'c'=2] {'y','x','c'}, dimensions={0} | all-to-all | bytes 3145728 | tf_op jit(solution)/shard_map/all_to_all | solution.py:379
  135.2 0.0 all-gather.4.cloned.1.call-done
  135.2 0.0 copy-done.2
  135.2 5.0 %mix.1 = bf16[32,96,256]{2,1,0:T(8,128)(2,1)S(1)} custom-call(bf16[32,96,256]{2,1,0:T(8,128)(2,1)S(1)} %all_to_all.27.rows_ref, f32[1,2048]{1,0:T(1,128)S(1)} %bitcast.19, bf16[16,1056,128]{2,1,0:T(8,128)(2,1)} %bitcast.22), custom_call_target="tpu_custom_call" | custom-call | flops 1700000000 | bytes 8000000 | tf_op jit(solution)/shard_map/mix/pallas_call | solution.py:279
  140.3 26.3 %all_to_all.28 = bf16[32,96,256]{2,1,0:T(8,128)(2,1)S(1)} all-to-all(bf16[32,96,256]{2,1,0:T(8,128)(2,1)S(1)} %mix.1), channel_id=1, replica_groups=mesh['z'=16,'y'=4,'x'=4,'c'=2] {'y','x','c'}, dimensions={0} | all-to-all | bytes 3145728 | tf_op jit(solution)/shard_map/all_to_all | solution.py:381
  166.5 0.2 convert_reduce_fusion
  166.8 0.7 add_convert_fusion
  (6 shorter events, 0.1 us)
Async XLA Ops:
  6.5 57.1 %all-gather.6.cloned.1.call-start = ((), (), s32[]{:S(2)}) async-start(), calls=%async_computation.6 | async-start | bytes 1179648 | tf_op jit(solution)/shard_map/all_gather | solution.py:350
  9.3 125.9 %all-gather.4.cloned.1.call-start = ((), (), s32[]{:S(2)}) async-start(), calls=%async_computation.5 | async-start | bytes 4460544 | tf_op jit(solution)/shard_map/all_gather | solution.py:359
  10.2 11.6 %collective-permute-start = (bf16[32,528]{1,0:T(8,128)(2,1)S(1)}, bf16[32,528]{1,0:T(8,128)(2,1)S(1)}, u32[]{:S(2)}, u32[]{:S(2)}) collective-permute-start(bf16[32,528]{1,0:T(8,128)(2,1)S(1)} %get-tuple-element.17), channel_id=1, source_target_pairs={{0,8},{8,16},{16,24},{24,0},{1,9},{9,17},{17,25},{25,1},{2,10},{10... | collective-permute-start | bytes 101384 | tf_op jit(solution)/shard_map/ppermute | solution.py:356
  14.2 7.5 %collective-permute-start.1 = (bf16[32,528]{1,0:T(8,128)(2,1)S(1)}, bf16[32,528]{1,0:T(8,128)(2,1)S(1)}, u32[]{:S(2)}, u32[]{:S(2)}) collective-permute-start(bf16[32,528]{1,0:T(8,128)(2,1)S(1)} %get-tuple-element.16), channel_id=1, source_target_pairs={{0,16},{8,24},{16,0},{24,8},{1,17},{9,25},{17,1},{25,9},{2,18},{10... | collective-permute-start | bytes 101384 | tf_op jit(solution)/shard_map/ppermute | solution.py:356
  18.8 5.0 %collective-permute-start.2 = (bf16[32,528]{1,0:T(8,128)(2,1)S(1)}, bf16[32,528]{1,0:T(8,128)(2,1)S(1)}, u32[]{:S(2)}, u32[]{:S(2)}) collective-permute-start(bf16[32,528]{1,0:T(8,128)(2,1)S(1)} %get-tuple-element.15), channel_id=1, source_target_pairs={{0,24},{8,0},{16,8},{24,16},{1,25},{9,1},{17,9},{25,17},{2,26},{10... | collective-permute-start | bytes 101384 | tf_op jit(solution)/shard_map/ppermute | solution.py:356
  24.5 39.1 %copy-start.4 = (bf16[192,1024]{1,0:T(8,128)(2,1)S(1)}, bf16[192,1024]{1,0:T(8,128)(2,1)}, u32[]{:S(2)}) copy-start(bf16[192,1024]{1,0:T(8,128)(2,1)} %q_ref.1) | copy-start | bytes 1179652
  24.6 39.1 %copy-start.5 = (bf16[192,512]{1,0:T(8,128)(2,1)S(1)}, bf16[192,512]{1,0:T(8,128)(2,1)}, u32[]{:S(2)}) copy-start(bf16[192,512]{1,0:T(8,128)(2,1)} %qr_ref.1) | copy-start | bytes 589828
  24.6 27.5 %all-to-all-start = ((bf16[16,8,960]{2,1,0:T(8,128)(2,1)}), bf16[16,8,960]{2,1,0:T(8,128)(2,1)S(1)}, u32[]{:S(2)}, u32[]{:S(2)}) async-start(bf16[16,8,960]{2,1,0:T(8,128)(2,1)} %get-tuple-element.10), calls=%async_computation | async-start | bytes 524288 | tf_op jit(solution)/shard_map/all_to_all | solution.py:352
  63.7 1.3 copy-start.3
  72.7 34.2 %copy-start = (bf16[1024,256]{1,0:T(8,128)(2,1)S(1)}, bf16[1024,256]{1,0:T(8,128)(2,1)}, u32[]{:S(2)}) copy-start(bf16[1024,256]{1,0:T(8,128)(2,1)} %w_ref.1) | copy-start | bytes 1572868
  72.7 34.2 %copy-start.1 = (bf16[192,256]{1,0:T(8,128)(2,1)S(1)}, bf16[192,256]{1,0:T(8,128)(2,1)}, u32[]{:S(2)}) copy-start(bf16[192,256]{1,0:T(8,128)(2,1)} %res_ref.1) | copy-start | bytes 294916
  107.3 27.9 %copy-start.2 = (f32[2048]{0:T(1024)S(1)}, f32[2048]{0:T(1024)}, u32[]{:S(2)}) copy-start(f32[2048]{0:T(1024)} %param.22) | copy-start | bytes 24580
Sparse Core Ops, SparseCore 0:
  9.5 36.7 all-gather.5
  48.4 73.5 all-gather.3

commit v5 on v4

--- a/solution.py
+++ b/solution.py
@@ -14,6 +14,7 @@
 DV = 128
 SPAN = 64
 NZ, NY, NX, NC = 16, 4, 4, 2
+NP = 2
 TOK = 192
 HALF = TOK // 2
 KEYS = 1536
@@ -33,14 +34,18 @@
 
 
 def prepare_kernel(
-    y_ref, lat_ref, rot_ref, gain_ref, cos_ref, sin_ref, k_ref, v_ref, gate_ref, up_ref, down_ref,
-    out_ref, kv_ref, cut_ref,
+    word_ref, lat_ref, rot_ref, gain_ref, cos_ref, sin_ref, k_ref, v_ref, gate_ref, up_ref,
+    down_ref, out_ref, kv_ref, same_ref, cross_ref,
 ):
-    for k in range(NY):
-        block = slice(k * 176, (k + 1) * 176)
-        cut_ref[(k + NY - y_ref[0]) % NY] = jnp.concatenate(
-            [gate_ref[:, block], up_ref[:, block], down_ref[:, block]], axis=1
-        )
+    even = word_ref[0] % NP == 0
+    halves = []
+    for k in range(NP):
+        block = slice(k * 352, (k + 1) * 352)
+        halves.append(
+            jnp.concatenate([gate_ref[:, block], up_ref[:, block], down_ref[:, block]], axis=1)
+        )
+    same_ref[...] = jnp.where(even, halves[0], halves[1])
+    cross_ref[...] = jnp.where(even, halves[1], halves[0])
     kv_ref[:, :DN] = k_ref[...]
     kv_ref[:, DN:] = v_ref[...]
     widened = lat_ref[...].astype(jnp.float32)
@@ -63,7 +68,8 @@
         out_shape=(
             jax.ShapeDtypeStruct((NZ, 8, 960), jnp.bfloat16),
             jax.ShapeDtypeStruct((256, 256), jnp.bfloat16),
-            jax.ShapeDtypeStruct((NY, 32, 528), jnp.bfloat16),
+            jax.ShapeDtypeStruct((32, 1056), jnp.bfloat16),
+            jax.ShapeDtypeStruct((32, 1056), jnp.bfloat16),
         ),
         in_specs=[pl.BlockSpec(memory_space=pltpu.SMEM)]
         + [pl.BlockSpec(memory_space=pltpu.VMEM)] * 10,
@@ -73,32 +79,34 @@
     )(*inputs)
 
 
-def put_kernel(y_ref, a_ref, b_ref, c_ref, d_ref, out_ref, all_ref):
-    y = y_ref[0]
+def put_kernel(word_ref, a_ref, b_ref, c_ref, d_ref, out_ref, all_ref):
+    y = word_ref[0]
     for s, ref in enumerate((a_ref, b_ref, c_ref, d_ref)):
-        all_ref[(y + NY - s) % NY, :, :528] = ref[...].astype(jnp.float32)
-    for k in range(5):
+        all_ref[(y + NY - s) % NY, :, :1056] = ref[...].astype(jnp.float32)
+    for k in range(9):
         lanes = jnp.concatenate(
             [all_ref[r, :, k * 128 : (k + 1) * 128] for r in range(NY)], axis=0
         )
-        rows = min(128, 528 - k * 128)
+        rows = min(128, 1056 - k * 128)
         out_ref[k * 128 : k * 128 + rows] = lanes.T[:rows].astype(jnp.bfloat16)
 
 
-def put(y, *pieces):
+def put(words, *pieces):
     small = pl.BlockSpec(memory_space=pltpu.VMEM)
     return pl.pallas_call(
         put_kernel,
         in_specs=[pl.BlockSpec(memory_space=pltpu.SMEM), small, small, small, small],
-        out_shape=jax.ShapeDtypeStruct((528, 128), jnp.bfloat16),
-        scratch_shapes=[pltpu.VMEM((NY, 32, 640), jnp.float32)],
-        compiler_params=pltpu.CompilerParams(vmem_limit_bytes=4 * 1024 * 1024),
-        cost_estimate=pl.CostEstimate(flops=100_000, bytes_accessed=300_000, transcendentals=0),
+        out_shape=jax.ShapeDtypeStruct((1056, 128), jnp.bfloat16),
+        scratch_shapes=[pltpu.VMEM((NY, 32, 1152), jnp.float32)],
+        compiler_params=pltpu.CompilerParams(vmem_limit_bytes=6 * 1024 * 1024),
+        cost_estimate=pl.CostEstimate(flops=100_000, bytes_accessed=600_000, transcendentals=0),
         name="put",
-    )(y, *pieces)
-
-
-def attend_kernel(q_ref, qr_ref, cos_ref, sin_ref, lat_ref, seg_ref, w_ref, out_ref, key_ref):
+    )(words, *pieces)
+
+
+def attend_kernel(
+    word_ref, q_ref, qr_ref, cos_ref, sin_ref, lat_ref, seg_ref, w0, w1, w2, w3, out_ref, key_ref
+):
     scale = LOG2E / math.sqrt(DN + DR)
 
     @pl.when(pl.program_id(0) == 0)
@@ -111,36 +119,37 @@
             for h in range(GROUP):
                 key_ref[h, rows, DN:] = tail
 
-    turned = qr_ref[...].astype(jnp.float32)
-    lane = lax.broadcasted_iota(jnp.int32, turned.shape, 1)
-    first = lane % DR < DR // 2
-    swapped = jnp.where(
-        first, pltpu.roll(turned, GROUP * DR - DR // 2, 1), pltpu.roll(turned, DR // 2, 1)
-    )
-    signed = jnp.where(first, -swapped, swapped)
-    cosine = jnp.concatenate([cos_ref[...]] * (GROUP // 2), axis=1)
-    sine = jnp.concatenate([sin_ref[...]] * (GROUP // 2), axis=1)
-    turned = (turned * cosine + signed * sine).astype(jnp.bfloat16)
+    parity = (word_ref[2] + pl.program_id(0)) % NC
     row = lax.broadcasted_iota(jnp.int32, (TOK, 64), 0)
     col = lax.broadcasted_iota(jnp.int32, (TOK, 64), 1)
     segment = jnp.where(row // SPAN == col, 1.0, 0.0).astype(jnp.bfloat16)
     ones = jnp.ones((KEYS, 128), jnp.bfloat16)
     r128 = lax.broadcasted_iota(jnp.int32, (128, 128), 0)
     c128 = lax.broadcasted_iota(jnp.int32, (128, 128), 1)
-    for h in range(GROUP):
+    lane = lax.broadcasted_iota(jnp.int32, (TOK, 2 * DR), 1)
+    first = lane % DR < DR // 2
+    for h, w_ref in enumerate((w0, w1, w2, w3)):
+        chip = (word_ref[1] + NX - h) % NX
+        head = chip * NC + parity
+        turned = qr_ref[:, pl.ds(pl.multiple_of(chip * 2 * DR, 128), 2 * DR)].astype(jnp.float32)
+        swapped = jnp.where(
+            first, pltpu.roll(turned, 2 * DR - DR // 2, 1), pltpu.roll(turned, DR // 2, 1)
+        )
+        signed = jnp.where(first, -swapped, swapped)
+        turned = (turned * cos_ref[...] + signed * sin_ref[...]).astype(jnp.bfloat16)
+        turned = jnp.where(parity == 0, turned[:, :DR], turned[:, DR:])
+        content = q_ref[:, pl.ds(pl.multiple_of(head * DN, 128), DN)]
         pair = jnp.concatenate(
             [
                 jnp.dot(
-                    lat_ref[:, j * 256 : (j + 1) * 256], w_ref[h],
+                    lat_ref[:, j * 256 : (j + 1) * 256], w_ref[0],
                     preferred_element_type=jnp.float32,
                 ).astype(jnp.bfloat16)
                 for j in range(3)
             ],
             axis=0,
         )
-        query = jnp.concatenate(
-            [q_ref[:, h * DN : (h + 1) * DN], turned[:, h * DR : (h + 1) * DR], segment], axis=1
-        )
+        query = jnp.concatenate([content, turned, segment], axis=1)
         key_ref[h, :, :DN] = pair[:, :DN]
         scores = lax.dot_general(
             query, key_ref[h], (((1,), (1,)), ((), ())), preferred_element_type=jnp.float32
@@ -150,7 +159,7 @@
         both = jnp.concatenate([pair[:, DN:], ones], axis=1)
         sums = jnp.dot(weights, both, preferred_element_type=jnp.float32)
         norm = sums[:, DV:]
-        out_ref[h, :TOK, :] = (sums[:, :DV] / norm).astype(jnp.bfloat16)
+        out_ref[head, :TOK, :] = (sums[:, :DV] / norm).astype(jnp.bfloat16)
         level = highest + jnp.log2(norm)
         upper = jnp.sum(jnp.where(r128 == c128, level[:128], 0.0), axis=0, keepdims=True)
         lower = jnp.sum(
@@ -163,23 +172,27 @@
             rows.append(part)
             rest = rest - part
         rows.append(jnp.zeros((PAD - TOK - 6, 128), jnp.float32))
-        out_ref[h, TOK:, :] = jnp.concatenate(rows, axis=0).astype(jnp.bfloat16)
-
-
-def attend(query, query_rotary, cosine, sine, lat, seg, weights):
+        out_ref[head, TOK:, :] = jnp.concatenate(rows, axis=0).astype(jnp.bfloat16)
+
+
+def attend(words, query, query_rotary, cosine, sine, lat, seg, weights):
+    def whole(*shape):
+        return pl.BlockSpec(shape, lambda i: (0,) * len(shape))
+
     return pl.pallas_call(
         attend_kernel,
-        grid=(H // GROUP,),
+        grid=(NC,),
         in_specs=[
-            pl.BlockSpec((TOK, GROUP * DN), lambda i: (0, i)),
-            pl.BlockSpec((TOK, GROUP * DR), lambda i: (0, i)),
-            pl.BlockSpec((TOK, 2 * DR), lambda i: (0, 0)),
-            pl.BlockSpec((TOK, 2 * DR), lambda i: (0, 0)),
-            pl.BlockSpec((ROWS, 960), lambda i: (0, 0)),
-            pl.BlockSpec((KEYS, 128), lambda i: (0, 0)),
-            pl.BlockSpec((GROUP, 256, 256), lambda i: (i, 0, 0)),
-        ],
-        out_specs=pl.BlockSpec((GROUP, PAD, 128), lambda i: (i, 0, 0)),
+            pl.BlockSpec(memory_space=pltpu.SMEM),
+            whole(TOK, H * DN),
+            whole(TOK, H * DR),
+            whole(TOK, 2 * DR),
+            whole(TOK, 2 * DR),
+            whole(ROWS, 960),
+            whole(KEYS, 128),
+        ]
+        + [pl.BlockSpec((1, 256, 256), lambda i: (i, 0, 0))] * NX,
+        out_specs=whole(H, PAD, 128),
         out_shape=jax.ShapeDtypeStruct((H, PAD, 128), jnp.bfloat16),
         scratch_shapes=[pltpu.VMEM((GROUP, KEYS, 256), jnp.bfloat16)],
         compiler_params=pltpu.CompilerParams(
@@ -189,7 +202,7 @@
             flops=3_000_000_000, bytes_accessed=4_000_000, transcendentals=2_400_000
         ),
         name="attend",
-    )(query, query_rotary, cosine, sine, lat, seg, weights)
+    )(words, query, query_rotary, cosine, sine, lat, seg, *weights)
 
 
 def merge_kernel(in_ref, out_ref):
@@ -237,7 +250,7 @@
     ]
     for copy in copies:
         copy.start()
-    for y in range(NY):
+    for y in range(NP):
         square = jnp.zeros((HALF, 256), jnp.float32)
         for f in range(H):
             piece = rows_ref[y * H + f].astype(jnp.float32)
@@ -248,29 +261,33 @@
             n_ref[y * HALF : (y + 1) * HALF, f * 256 : (f + 1) * 256] = (
                 piece * factor * gain_ref[:, f * 256 : (f + 1) * 256]
             ).astype(jnp.bfloat16)
-    for copy in copies:
-        copy.wait()
     dims = (((1,), (1,)), ((), ()))
-    hidden = []
-    for c in range(NC):
-        gate = lax.dot_general(
-            n_ref[...], w_ref[c * 528 : c * 528 + 176], dims, preferred_element_type=jnp.float32
-        )
-        up = lax.dot_general(
-            n_ref[...], w_ref[c * 528 + 176 : c * 528 + 352], dims,
-            preferred_element_type=jnp.float32,
-        )
-        hidden.append((gate / (1.0 + jnp.exp(-gate)) * up).astype(jnp.bfloat16))
+    totals = [None] * (2 * NC)
+    for chunk in range(4):
+        for copy in copies[chunk * 4 : (chunk + 1) * 4]:
+            copy.wait()
+        lanes = slice(chunk * 512, (chunk + 1) * 512)
+        for k in range(2 * NC):
+            start = k // 2 * 1056 + k % 2 * 352
+            part = lax.dot_general(
+                n_ref[:, lanes], w_ref[start : start + 352, lanes], dims,
+                preferred_element_type=jnp.float32,
+            )
+            totals[k] = part if totals[k] is None else totals[k] + part
+    hidden = [
+        (totals[2 * c] / (1.0 + jnp.exp(-totals[2 * c])) * totals[2 * c + 1]).astype(jnp.bfloat16)
+        for c in range(NC)
+    ]
     for f in range(H):
         lanes = slice(f * 256, (f + 1) * 256)
         part = sum(
             jnp.dot(
-                hidden[c], w_ref[c * 528 + 352 : (c + 1) * 528, lanes],
+                hidden[c], w_ref[c * 1056 + 704 : (c + 1) * 1056, lanes],
                 preferred_element_type=jnp.float32,
             )
             for c in range(NC)
         ).astype(jnp.bfloat16)
-        for y in range(NY):
+        for y in range(NP):
             out_ref[y * H + f] = part[y * HALF : (y + 1) * HALF]
 
 
@@ -280,15 +297,15 @@
         mix_kernel,
         in_specs=[whole, whole, pl.BlockSpec(memory_space=pltpu.HBM)],
         out_specs=whole,
-        out_shape=jax.ShapeDtypeStruct((NY * H, HALF, 256), jnp.bfloat16),
+        out_shape=jax.ShapeDtypeStruct((NP * H, HALF, 256), jnp.bfloat16),
         scratch_shapes=[
-            pltpu.VMEM((NY * HALF, 2048), jnp.bfloat16),
-            pltpu.VMEM((1056, 2048), jnp.bfloat16),
+            pltpu.VMEM((NP * HALF, 2048), jnp.bfloat16),
+            pltpu.VMEM((NC * 1056, 2048), jnp.bfloat16),
             pltpu.SemaphoreType.DMA((NZ,)),
         ],
         compiler_params=pltpu.CompilerParams(vmem_limit_bytes=52_000_000),
         cost_estimate=pl.CostEstimate(
-            flops=1_700_000_000, bytes_accessed=8_000_000, transcendentals=140_000
+            flops=1_700_000_000, bytes_accessed=10_000_000, transcendentals=140_000
         ),
         name="mix",
     )(rows, gain, weights)
@@ -301,7 +318,7 @@
         + jnp.dot(heads, w_ref[...], preferred_element_type=jnp.float32)
     ).astype(jnp.bfloat16)
     mixed_ref[...] = mixed
-    for d in range(NY * NX):
+    for d in range(NP * NX):
         for c in range(NC):
             sent_ref[d * NC + c] = mixed[c * HALF : (c + 1) * HALF]
 
@@ -311,7 +328,7 @@
         project_kernel,
         out_shape=(
             jax.ShapeDtypeStruct((TOK, 256), jnp.bfloat16),
-            jax.ShapeDtypeStruct((NY * NX * NC, HALF, 256), jnp.bfloat16),
+            jax.ShapeDtypeStruct((NP * NX * NC, HALF, 256), jnp.bfloat16),
         ),
         compiler_params=pltpu.CompilerParams(vmem_limit_bytes=12 * 1024 * 1024),
         cost_estimate=pl.CostEstimate(
@@ -336,31 +353,32 @@
     up_proj,
     down_proj,
 ):
-    zi, yi = lax.axis_index("z"), lax.axis_index("y")
+    zi, yi = lax.axis_index("z"), lax.axis_index("g") * NP + lax.axis_index("p")
     sp_index = zi * NY + yi
     tp_index = lax.axis_index("x") * NC + lax.axis_index("c")
 
     own_places = (sp_index * 8 + tp_index) * 24 + jnp.arange(24, dtype=jnp.int32)
     cosine, sine = tables(own_places)
-    y_word = yi.reshape(1).astype(jnp.int32)
-    own, kv, ahead = prepare(
-        y_word, latents, key_rotary, latent_gain.reshape(1, -1), cosine, sine, key_up, value_up,
+    words = jnp.stack([yi, lax.axis_index("x"), lax.axis_index("c")]).astype(jnp.int32)
+    own, kv, same, cross = prepare(
+        words, latents, key_rotary, latent_gain.reshape(1, -1), cosine, sine, key_up, value_up,
         gate_proj, up_proj, down_proj.T,
     )
-    kv = lax.all_gather(kv, ("x", "c"), axis=0, tiled=False)
+    back = [same] + [
+        lax.ppermute(piece, ("g", "p"), [(i, (i + s) % NY) for i in range(NY)])
+        for s, piece in ((1, cross), (2, same), (3, cross))
+    ]
+    mixer = lax.all_gather(put(words, *back), ("z", "c"), axis=0, tiled=True)
+    mixer = mixer.reshape(NZ, NC * 1056, 128)
 
     lat = lax.all_to_all(own, "z", split_axis=0, concat_axis=0, tiled=True)
     lat = lat.reshape(NZ * 8, 960)
-    pieces = [ahead[s] for s in range(NY)]
-    back = [
-        lax.ppermute(pieces[s], "y", [(i, (i + s) % NY) for i in range(NY)]) for s in range(1, NY)
+    pair = jnp.stack([kv, lax.ppermute(kv, "c", [(0, 1), (1, 0)])])
+    weights = [pair] + [
+        lax.ppermute(pair, "x", [(i, (i + s) % NX) for i in range(NX)]) for s in range(1, NX)
     ]
-    own_slice = put(y_word, pieces[0], *back)
-    mixer = lax.all_gather(own_slice, ("z", "c"), axis=0, tiled=True).reshape(
-        NZ, NC * 528, 128
-    )
-
-    lat = lax.all_gather(lat, "y", axis=0, tiled=True)
+
+    lat = lax.all_gather(lat, ("g", "p"), axis=0, tiled=True)
 
     index = jnp.arange(KEYS, dtype=jnp.int32)
     y_of, z_of, i_of = index // 128 % NY, index // 8 % NZ, index // 512 * 8 + index % 8
@@ -372,22 +390,22 @@
     cosine, sine = tables(sp_index * TOK + jnp.arange(TOK, dtype=jnp.int32))
     cosine, sine = (jnp.concatenate([t] * 4, axis=1) for t in (cosine, sine))
 
-    parts = attend(query_content, query_rotary, cosine, sine, lat, seg, kv)
+    parts = attend(words, query_content, query_rotary, cosine, sine, lat, seg, weights)
     parts = lax.all_to_all(parts, ("x", "c"), split_axis=0, concat_axis=0, tiled=True)
     heads = lax.all_to_all(merge(parts), ("x", "c"), split_axis=0, concat_axis=0, tiled=True)
     mixed_rows, sent = project(heads, out_proj, residual)
-    rows = lax.all_to_all(sent, ("y", "x", "c"), split_axis=0, concat_axis=0, tiled=True)
+    rows = lax.all_to_all(sent, ("p", "x", "c"), split_axis=0, concat_axis=0, tiled=True)
     partial_sums = mix(rows, mixer_gain.reshape(1, -1), mixer)
     arrived = lax.all_to_all(
-        partial_sums, ("y", "x", "c"), split_axis=0, concat_axis=0, tiled=True
+        partial_sums, ("p", "x", "c"), split_axis=0, concat_axis=0, tiled=True
     )
-    summed = arrived.reshape(NY * NX, TOK, 256).astype(jnp.float32).sum(axis=0)
+    summed = arrived.reshape(NP * NX, TOK, 256).astype(jnp.float32).sum(axis=0)
     return (mixed_rows.astype(jnp.float32) + summed).astype(jnp.bfloat16)
 
 
 def solution(mesh):
-    fine = Mesh(mesh.devices.reshape(NZ, NY, NX, NC), ("z", "y", "x", "c"))
-    sp, tp = ("z", "y"), ("x", "c")
+    fine = Mesh(mesh.devices.reshape(NZ, NY // NP, NP, NX, NC), ("z", "g", "p", "x", "c"))
+    sp, tp = ("z", "g", "p"), ("x", "c")
     return jax.shard_map(
         layer,
         mesh=fine,

time: 175 us -> 165 us (0.943)
  blocking collectives: 99.3 us -> 78 us
  starting transfers between devices: 26.4 us -> 41.2 us
  waiting for transfers between devices: 13.7 us -> 4.37 us
  local copies, waits for them, and re-layouts: 2.14 us -> 4.17 us
  Pallas kernels: 16.5 us -> 18.4 us
    all_to_all x2, blocking collectives: 54.2 us -> 32.7 us  [the longest x1 16.6 us: layer(): lax.all_to_all(sent, ('p', 'x', 'c'), split_axis=0, concat_axis=0, tiled=...]
    ppermute x3 -> x7, starting transfers between devices: 11.5 us -> 29.2 us  [the longest x3 11.5 us: layer(): lax.ppermute(piece, ('g', 'p'), [(i, (i + s) % NY) for i in range(NY)])]
    all_to_all x1, waiting for transfers between devices: 11.7 us -> 1.8 us  [layer(): lat = lax.all_to_all(own, 'z', split_axis=0, concat_axis=0, tiled=True)]
    unnamed x12 -> x16, local copies, waits for them, and re-layouts: 1.28 us -> 4.17 us
    all_to_all x1, starting transfers between devices: 14.8 us -> 12 us  [layer(): lat = lax.all_to_all(own, 'z', split_axis=0, concat_axis=0, tiled=True)]
  transfers between devices with their start and end apart: 6 -> 9, of which waited for: 2 -> 2; matrix products, arithmetic and copies ran while one was open for 1% -> 1% of each run, Pallas kernels for 5% -> 6%
where the time goes in v5:
time: 165 us; the launch traced here: 164 us
  blocking collectives  78 us (47%)
  starting transfers between devices  41.2 us (25%)
  Pallas kernels  18.4 us (11%)
  between operations  13.6 us (8%)
  waiting for transfers between devices  4.37 us (3%)
  local copies, waits for them, and re-layouts  4.17 us (3%)
  other arithmetic  4.05 us (2%)
    all_to_all x1, blocking collectives, layer(): lax.all_to_all(parts, ('x', 'c'), split_axis=0, concat_axis=0, tiled=True)  21.7 us
    all_to_all x1, blocking collectives, layer(): lax.all_to_all(sent, ('p', 'x', 'c'), split_axis=0, concat_axis=0, tiled=...  16.6 us
    all_to_all x1, blocking collectives, layer(): lax.all_to_all(partial_sums, ('p', 'x', 'c'), split_axis=0, concat_axis=0...  16 us
    all_gather x1, blocking collectives, layer(): lat = lax.all_gather(lat, ('g', 'p'), axis=0, tiled=True)  12.3 us
    all_to_all x1, starting transfers between devices, layer(): lat = lax.all_to_all(own, 'z', split_axis=0, concat_axis=0, tiled=True)  12 us
    ppermute x3, starting transfers between devices, layer(): lax.ppermute(piece, ('g', 'p'), [(i, (i + s) % NY) for i in range(NY)])  11.5 us
    all_to_all x1, blocking collectives, layer(): lax.all_to_all(merge(parts), ('x', 'c'), split_axis=0, concat_axis=0, til...  11.4 us
    ppermute x3, starting transfers between devices, layer(): lax.ppermute(pair, 'x', [(i, (i + s) % NX) for i in range(NX)])  10.5 us
  transfers between devices with their start and end apart: 9, of which 2 were waited for; matrix products, arithmetic and copies ran while one was open for 1% of the time, Pallas kernels for 6%

profile of v5, /device:TPU:1, one launch (start us, length us, event | category | flops | bytes accessed | tf_op | source)
XLA Modules:
  0.0 163.7 jit_solution(807293414018727008)
XLA Ops:
  6.5 0.0 all-gather.2.cloned.1.call-start
  6.6 0.7 multiply_sine_fusion.1
  7.3 0.7 pad_add_fusion.word_ref
  8.0 2.0 %prepare.1 = (bf16[16,8,960]{2,1,0:T(8,128)(2,1)}, bf16[256,256]{1,0:T(8,128)(2,1)}, bf16[32,1056]{1,0:T(8,128)(2,1)}, bf16[32,1056]{1,0:T(8,128)(2,1)}) custom-call(s32[3]{0:T(128)} %pad_add_fusion.word_ref, bf16[24,256]{1,0:T(8,128)(2,1)} %lat_ref.1, bf16[24,64]{1,0:T(8,128)(2,1)} %rot_ref.1, f32[1,256]{1,0:T(1,128)} %bitcast.21, ...), custom_call_target="tpu_custom_call" | custom-call | flops 100000 | bytes 300000 | tf_op jit(solution)/shard_map/prepare/pallas_call | solution.py:66
  10.0 4.0 %collective-permute-start.4 = (bf16[32,1056]{1,0:T(8,128)(2,1)}, bf16[32,1056]{1,0:T(8,128)(2,1)S(1)}, u32[]{:S(2)}, u32[]{:S(2)}) collective-permute-start(bf16[32,1056]{1,0:T(8,128)(2,1)} %get-tuple-element.16), channel_id=1, source_target_pairs={{0,8},{8,16},{16,24},{24,0},{1,9},{9,17},{17,25},{25,1},{2,10},{10... | collective-permute-start | bytes 202760 | tf_op jit(solution)/shard_map/ppermute | solution.py:368
  14.0 4.5 %collective-permute-start.5 = (bf16[32,1056]{1,0:T(8,128)(2,1)}, bf16[32,1056]{1,0:T(8,128)(2,1)S(1)}, u32[]{:S(2)}, u32[]{:S(2)}) collective-permute-start(bf16[32,1056]{1,0:T(8,128)(2,1)} %get-tuple-element.15.a_ref), channel_id=1, source_target_pairs={{0,16},{8,24},{16,0},{24,8},{1,17},{9,25},{17,1},{25,9},{2,18},{10... | collective-permute-start | bytes 202760 | tf_op jit(solution)/shard_map/ppermute | solution.py:368
  18.5 3.0 %collective-permute-start.6 = (bf16[32,1056]{1,0:T(8,128)(2,1)}, bf16[32,1056]{1,0:T(8,128)(2,1)S(1)}, u32[]{:S(2)}, u32[]{:S(2)}) collective-permute-start(bf16[32,1056]{1,0:T(8,128)(2,1)} %get-tuple-element.16), channel_id=1, source_target_pairs={{0,24},{8,0},{16,8},{24,16},{1,25},{9,1},{17,9},{25,17},{2,26},{10... | collective-permute-start | bytes 202760 | tf_op jit(solution)/shard_map/ppermute | solution.py:368
  21.5 0.0 collective-permute-done.4.b_ref
  21.5 0.0 collective-permute-done.5.c_ref
  21.5 2.5 %collective-permute-done.6.d_ref = bf16[32,1056]{1,0:T(8,128)(2,1)S(1)} collective-permute-done((bf16[32,1056]{1,0:T(8,128)(2,1)}, bf16[32,1056]{1,0:T(8,128)(2,1)S(1)}, u32[]{:S(2)}, u32[]{:S(2)}) %collective-permute-start.6) | collective-permute-done | bytes 67616 | tf_op jit(solution)/shard_map/ppermute | solution.py:368
  24.1 0.0 copy-start.2
  24.1 0.9 copy-done.2
  24.9 0.0 copy-start.4
  24.9 0.7 copy-done.4
  25.6 1.5 put.1
  27.1 0.0 all-gather.2.cloned.1.call-update
  27.1 7.1 %collective-permute-start = (bf16[256,256]{1,0:T(8,128)(2,1)}, bf16[256,256]{1,0:T(8,128)(2,1)S(1)}, u32[]{:S(2)}, u32[]{:S(2)}) collective-permute-start(bf16[256,256]{1,0:T(8,128)(2,1)} %get-tuple-element.12), channel_id=1, source_target_pairs={{0,1},{1,0},{2,3},{3,2},{4,5},{5,4},{6,7},{7,6},{8,9},{9,8},{10,11... | collective-permute-start | bytes 393224 | tf_op jit(solution)/shard_map/ppermute | solution.py:376
  34.3 12.0 %all-to-all-start = ((bf16[16,8,960]{2,1,0:T(8,128)(2,1)}), bf16[16,8,960]{2,1,0:T(8,128)(2,1)S(1)}, u32[]{:S(2)}, u32[]{:S(2)}) async-start(bf16[16,8,960]{2,1,0:T(8,128)(2,1)} %get-tuple-element.11), calls=%async_computation | async-start | bytes 524288 | tf_op jit(solution)/shard_map/all_to_all | solution.py:374
  46.3 0.3 select_convert_fusion.seg_ref
  46.6 0.4 multiply_sine_fusion
  47.0 0.2 pad_maximum_fusion.1
  47.2 0.0 collective-permute-done
  47.3 0.9 pad_maximum_fusion.w0
  48.2 3.1 %collective-permute-start.1 = (bf16[2,256,256]{2,1,0:T(8,128)(2,1)S(1)}, bf16[2,256,256]{2,1,0:T(8,128)(2,1)S(1)}, u32[]{:S(2)}, u32[]{:S(2)}) collective-permute-start(bf16[2,256,256]{2,1,0:T(8,128)(2,1)S(1)} %pad_maximum_fusion.w0), channel_id=1, source_target_pairs={{0,2},{2,4},{4,6},{6,0},{1,3},{3,5},{5,7},{7,1},{8,10},{10,12},{12... | collective-permute-start | bytes 786440 | tf_op jit(solution)/shard_map/ppermute | solution.py:378
  51.3 4.4 %collective-permute-start.2 = (bf16[2,256,256]{2,1,0:T(8,128)(2,1)S(1)}, bf16[2,256,256]{2,1,0:T(8,128)(2,1)S(1)}, u32[]{:S(2)}, u32[]{:S(2)}) collective-permute-start(bf16[2,256,256]{2,1,0:T(8,128)(2,1)S(1)} %pad_maximum_fusion.w0), channel_id=1, source_target_pairs={{0,4},{2,6},{4,0},{6,2},{1,5},{3,7},{5,1},{7,3},{8,12},{10,14},{12... | collective-permute-start | bytes 786440 | tf_op jit(solution)/shard_map/ppermute | solution.py:378
  55.7 3.1 %collective-permute-start.3 = (bf16[2,256,256]{2,1,0:T(8,128)(2,1)S(1)}, bf16[2,256,256]{2,1,0:T(8,128)(2,1)S(1)}, u32[]{:S(2)}, u32[]{:S(2)}) collective-permute-start(bf16[2,256,256]{2,1,0:T(8,128)(2,1)S(1)} %pad_maximum_fusion.w0), channel_id=1, source_target_pairs={{0,6},{2,0},{4,2},{6,4},{1,7},{3,1},{5,3},{7,5},{8,14},{10,8},{12,... | collective-permute-start | bytes 786440 | tf_op jit(solution)/shard_map/ppermute | solution.py:378
  58.8 1.8 %all-to-all-done = bf16[16,8,960]{2,1,0:T(8,128)(2,1)S(1)} async-done(((bf16[16,8,960]{2,1,0:T(8,128)(2,1)}), bf16[16,8,960]{2,1,0:T(8,128)(2,1)S(1)}, u32[]{:S(2)}, u32[]{:S(2)}) %all-to-all-start) | async-done | bytes 245792 | tf_op jit(solution)/shard_map/all_to_all | solution.py:374
  60.5 12.3 %all_gather.6.lat_ref = bf16[512,960]{1,0:T(8,128)(2,1)S(1)} all-gather(bf16[128,960]{1,0:T(8,128)(2,1)S(1)} %bitcast.17), channel_id=1, replica_groups=mesh['z'=16,'g'=2,'p'=2,'x'=4,'c'=2] {'g','p'}, dimensions={0}, use_global_device_ids=true | all-gather | bytes 1228800 | tf_op jit(solution)/shard_map/all_gather | solution.py:381
  72.8 0.0 collective-permute-done.1.w1
  72.8 0.0 collective-permute-done.2.w2
  72.8 0.0 collective-permute-done.3.w3
  72.8 0.0 copy-start.5
  72.8 0.7 copy-done.5
  73.5 1.0 copy-done.6
  74.5 0.9 copy-done.7
  75.4 8.5 %attend.1 = bf16[8,208,128]{2,1,0:T(8,128)(2,1)S(1)} custom-call(s32[3]{0:T(128)S(1)} %copy-done.5, bf16[192,1024]{1,0:T(8,128)(2,1)S(1)} %copy-done.6, bf16[192,512]{1,0:T(8,128)(2,1)S(1)} %copy-done.7, f32[192,128]{1,0:T(8,128)S(1)} %get-tuple-element.21.cos_ref, f32[192,128]{1,0:T(8,128)S(1)} %get-tuple-element.22.sin_ref, ...), custom_call_target="tpu_custom_call" | custom-call | flops 3000000000 | bytes 4000000 | tf_op jit(solution)/shard_map/attend/pallas_call | solution.py:182
  84.0 21.7 %all_to_all.25.in_ref = bf16[8,208,128]{2,1,0:T(8,128)(2,1)S(1)} all-to-all(bf16[8,208,128]{2,1,0:T(8,128)(2,1)S(1)} %attend.1), channel_id=1, replica_groups=mesh['z'=16,'g'=2,'p'=2,'x'=4,'c'=2] {'x','c'}, dimensions={0} | all-to-all | bytes 851968 | tf_op jit(solution)/shard_map/all_to_all | solution.py:394
  105.6 0.6 merge.1
  106.2 11.4 %all_to_all.26.heads_ref = bf16[8,192,128]{2,1,0:T(8,128)(2,1)S(1)} all-to-all(bf16[8,192,128]{2,1,0:T(8,128)(2,1)S(1)} %merge.1), channel_id=1, replica_groups=mesh['z'=16,'g'=2,'p'=2,'x'=4,'c'=2] {'x','c'}, dimensions={0} | all-to-all | bytes 786432 | tf_op jit(solution)/shard_map/all_to_all | solution.py:395
  117.6 0.0 copy-done
  117.6 0.0 copy-done.1
  117.6 0.3 project.1
  117.9 16.6 %all_to_all.27.rows_ref = bf16[16,96,256]{2,1,0:T(8,128)(2,1)S(1)} all-to-all(bf16[16,96,256]{2,1,0:T(8,128)(2,1)S(1)} %get-tuple-element.14), channel_id=1, replica_groups=mesh['z'=16,'g'=2,'p'=2,'x'=4,'c'=2] {'p','x','c'}, dimensions={0} | all-to-all | bytes 1572864 | tf_op jit(solution)/shard_map/all_to_all | solution.py:397
  134.5 0.0 copy-done.3
  134.5 5.6 %mix.1 = bf16[16,96,256]{2,1,0:T(8,128)(2,1)S(1)} custom-call(bf16[16,96,256]{2,1,0:T(8,128)(2,1)S(1)} %all_to_all.27.rows_ref, f32[1,2048]{1,0:T(1,128)S(1)} %bitcast.14, bf16[16,2112,128]{2,1,0:T(8,128)(2,1)} %bitcast.15), custom_call_target="tpu_custom_call" | custom-call | flops 1700000000 | bytes 10000000 | tf_op jit(solution)/shard_map/mix/pallas_call | solution.py:296
  140.1 16.0 %all_to_all.28 = bf16[16,96,256]{2,1,0:T(8,128)(2,1)S(1)} all-to-all(bf16[16,96,256]{2,1,0:T(8,128)(2,1)S(1)} %mix.1), channel_id=1, replica_groups=mesh['z'=16,'g'=2,'p'=2,'x'=4,'c'=2] {'p','x','c'}, dimensions={0} | all-to-all | bytes 1572864 | tf_op jit(solution)/shard_map/all_to_all | solution.py:399
  156.1 0.1 convert_reduce_fusion
  156.2 0.7 add_convert_fusion
  (12 shorter events, 0.1 us)
Async XLA Ops:
  6.5 128.0 %all-gather.2.cloned.1.call-start = ((), (), s32[]{:S(2)}) async-start(), calls=%async_computation.5 | async-start | bytes 8921088 | tf_op jit(solution)/shard_map/all_gather | solution.py:371
  10.0 11.5 %collective-permute-start.4 = (bf16[32,1056]{1,0:T(8,128)(2,1)}, bf16[32,1056]{1,0:T(8,128)(2,1)S(1)}, u32[]{:S(2)}, u32[]{:S(2)}) collective-permute-start(bf16[32,1056]{1,0:T(8,128)(2,1)} %get-tuple-element.16), channel_id=1, source_target_pairs={{0,8},{8,16},{16,24},{24,0},{1,9},{9,17},{17,25},{25,1},{2,10},{10... | collective-permute-start | bytes 202760 | tf_op jit(solution)/shard_map/ppermute | solution.py:368
  14.0 7.5 %collective-permute-start.5 = (bf16[32,1056]{1,0:T(8,128)(2,1)}, bf16[32,1056]{1,0:T(8,128)(2,1)S(1)}, u32[]{:S(2)}, u32[]{:S(2)}) collective-permute-start(bf16[32,1056]{1,0:T(8,128)(2,1)} %get-tuple-element.15.a_ref), channel_id=1, source_target_pairs={{0,16},{8,24},{16,0},{24,8},{1,17},{9,25},{17,1},{25,9},{2,18},{10... | collective-permute-start | bytes 202760 | tf_op jit(solution)/shard_map/ppermute | solution.py:368
  18.5 5.5 %collective-permute-start.6 = (bf16[32,1056]{1,0:T(8,128)(2,1)}, bf16[32,1056]{1,0:T(8,128)(2,1)S(1)}, u32[]{:S(2)}, u32[]{:S(2)}) collective-permute-start(bf16[32,1056]{1,0:T(8,128)(2,1)} %get-tuple-element.16), channel_id=1, source_target_pairs={{0,24},{8,0},{16,8},{24,16},{1,25},{9,1},{17,9},{25,17},{2,26},{10... | collective-permute-start | bytes 202760 | tf_op jit(solution)/shard_map/ppermute | solution.py:368
  24.1 0.9 copy-start.2
  24.9 0.7 copy-start.4
  27.1 90.5 %copy-start = (bf16[1024,256]{1,0:T(8,128)(2,1)S(1)}, bf16[1024,256]{1,0:T(8,128)(2,1)}, u32[]{:S(2)}) copy-start(bf16[1024,256]{1,0:T(8,128)(2,1)} %w_ref.1) | copy-start | bytes 1572868
  27.1 90.5 %copy-start.1 = (bf16[192,256]{1,0:T(8,128)(2,1)S(1)}, bf16[192,256]{1,0:T(8,128)(2,1)}, u32[]{:S(2)}) copy-start(bf16[192,256]{1,0:T(8,128)(2,1)} %res_ref.1) | copy-start | bytes 294916
  27.1 20.1 %collective-permute-start = (bf16[256,256]{1,0:T(8,128)(2,1)}, bf16[256,256]{1,0:T(8,128)(2,1)S(1)}, u32[]{:S(2)}, u32[]{:S(2)}) collective-permute-start(bf16[256,256]{1,0:T(8,128)(2,1)} %get-tuple-element.12), channel_id=1, source_target_pairs={{0,1},{1,0},{2,3},{3,2},{4,5},{5,4},{6,7},{7,6},{8,9},{9,8},{10,11... | collective-permute-start | bytes 393224 | tf_op jit(solution)/shard_map/ppermute | solution.py:376
  34.3 26.3 %all-to-all-start = ((bf16[16,8,960]{2,1,0:T(8,128)(2,1)}), bf16[16,8,960]{2,1,0:T(8,128)(2,1)S(1)}, u32[]{:S(2)}, u32[]{:S(2)}) async-start(bf16[16,8,960]{2,1,0:T(8,128)(2,1)} %get-tuple-element.11), calls=%async_computation | async-start | bytes 524288 | tf_op jit(solution)/shard_map/all_to_all | solution.py:374
  48.2 24.6 %collective-permute-start.1 = (bf16[2,256,256]{2,1,0:T(8,128)(2,1)S(1)}, bf16[2,256,256]{2,1,0:T(8,128)(2,1)S(1)}, u32[]{:S(2)}, u32[]{:S(2)}) collective-permute-start(bf16[2,256,256]{2,1,0:T(8,128)(2,1)S(1)} %pad_maximum_fusion.w0), channel_id=1, source_target_pairs={{0,2},{2,4},{4,6},{6,0},{1,3},{3,5},{5,7},{7,1},{8,10},{10,12},{12... | collective-permute-start | bytes 786440 | tf_op jit(solution)/shard_map/ppermute | solution.py:378
  51.3 21.5 %collective-permute-start.2 = (bf16[2,256,256]{2,1,0:T(8,128)(2,1)S(1)}, bf16[2,256,256]{2,1,0:T(8,128)(2,1)S(1)}, u32[]{:S(2)}, u32[]{:S(2)}) collective-permute-start(bf16[2,256,256]{2,1,0:T(8,128)(2,1)S(1)} %pad_maximum_fusion.w0), channel_id=1, source_target_pairs={{0,4},{2,6},{4,0},{6,2},{1,5},{3,7},{5,1},{7,3},{8,12},{10,14},{12... | collective-permute-start | bytes 786440 | tf_op jit(solution)/shard_map/ppermute | solution.py:378
  55.7 17.1 %collective-permute-start.3 = (bf16[2,256,256]{2,1,0:T(8,128)(2,1)S(1)}, bf16[2,256,256]{2,1,0:T(8,128)(2,1)S(1)}, u32[]{:S(2)}, u32[]{:S(2)}) collective-permute-start(bf16[2,256,256]{2,1,0:T(8,128)(2,1)S(1)} %pad_maximum_fusion.w0), channel_id=1, source_target_pairs={{0,6},{2,0},{4,2},{6,4},{1,7},{3,1},{5,3},{7,5},{8,14},{10,8},{12,... | collective-permute-start | bytes 786440 | tf_op jit(solution)/shard_map/ppermute | solution.py:378
  60.5 74.0 %copy-start.3 = (f32[2048]{0:T(1024)S(1)}, f32[2048]{0:T(1024)}, u32[]{:S(2)}) copy-start(f32[2048]{0:T(1024)} %param.22) | copy-start | bytes 24580
  72.8 0.7 copy-start.5
  73.5 1.0 copy-start.6
  74.5 0.9 copy-start.7
Sparse Core Ops, SparseCore 0:
  27.2 92.4 all-gather.1

commit v6 on v5

--- a/solution.py
+++ b/solution.py
@@ -34,18 +34,16 @@
 
 
 def prepare_kernel(
-    word_ref, lat_ref, rot_ref, gain_ref, cos_ref, sin_ref, k_ref, v_ref, gate_ref, up_ref,
-    down_ref, out_ref, kv_ref, same_ref, cross_ref,
+    lat_ref, rot_ref, gain_ref, cos_ref, sin_ref, k_ref, v_ref, gate_ref, up_ref, down_ref,
+    out_ref, kv_ref, cut_ref,
 ):
-    even = word_ref[0] % NP == 0
-    halves = []
     for k in range(NP):
         block = slice(k * 352, (k + 1) * 352)
-        halves.append(
-            jnp.concatenate([gate_ref[:, block], up_ref[:, block], down_ref[:, block]], axis=1)
-        )
-    same_ref[...] = jnp.where(even, halves[0], halves[1])
-    cross_ref[...] = jnp.where(even, halves[1], halves[0])
+        half = jnp.concatenate(
+            [gate_ref[:, block], up_ref[:, block], down_ref[:, block]], axis=1
+        )
+        for y in range(k, NY, NP):
+            cut_ref[y] = half
     kv_ref[:, :DN] = k_ref[...]
     kv_ref[:, DN:] = v_ref[...]
     widened = lat_ref[...].astype(jnp.float32)
@@ -68,21 +66,17 @@
         out_shape=(
             jax.ShapeDtypeStruct((NZ, 8, 960), jnp.bfloat16),
             jax.ShapeDtypeStruct((256, 256), jnp.bfloat16),
-            jax.ShapeDtypeStruct((32, 1056), jnp.bfloat16),
-            jax.ShapeDtypeStruct((32, 1056), jnp.bfloat16),
-        ),
-        in_specs=[pl.BlockSpec(memory_space=pltpu.SMEM)]
-        + [pl.BlockSpec(memory_space=pltpu.VMEM)] * 10,
+            jax.ShapeDtypeStruct((NY, 32, 1056), jnp.bfloat16),
+        ),
         compiler_params=pltpu.CompilerParams(vmem_limit_bytes=66_900_000),
         cost_estimate=pl.CostEstimate(flops=100_000, bytes_accessed=300_000, transcendentals=24),
         name="prepare",
     )(*inputs)
 
 
-def put_kernel(word_ref, a_ref, b_ref, c_ref, d_ref, out_ref, all_ref):
-    y = word_ref[0]
-    for s, ref in enumerate((a_ref, b_ref, c_ref, d_ref)):
-        all_ref[(y + NY - s) % NY, :, :1056] = ref[...].astype(jnp.float32)
+def put_kernel(in_ref, out_ref, all_ref):
+    for r in range(NY):
+        all_ref[r, :, :1056] = in_ref[r].astype(jnp.float32)
     for k in range(9):
         lanes = jnp.concatenate(
             [all_ref[r, :, k * 128 : (k + 1) * 128] for r in range(NY)], axis=0
@@ -91,21 +85,50 @@
         out_ref[k * 128 : k * 128 + rows] = lanes.T[:rows].astype(jnp.bfloat16)
 
 
-def put(words, *pieces):
-    small = pl.BlockSpec(memory_space=pltpu.VMEM)
+def put(pieces):
     return pl.pallas_call(
         put_kernel,
-        in_specs=[pl.BlockSpec(memory_space=pltpu.SMEM), small, small, small, small],
         out_shape=jax.ShapeDtypeStruct((1056, 128), jnp.bfloat16),
         scratch_shapes=[pltpu.VMEM((NY, 32, 1152), jnp.float32)],
         compiler_params=pltpu.CompilerParams(vmem_limit_bytes=6 * 1024 * 1024),
         cost_estimate=pl.CostEstimate(flops=100_000, bytes_accessed=600_000, transcendentals=0),
         name="put",
-    )(words, *pieces)
+    )(pieces)
+
+
+def turn_kernel(q_ref, qr_ref, cos_ref, sin_ref, out_ref):
+    lane = lax.broadcasted_iota(jnp.int32, (TOK, 2 * DR), 1)
+    first = lane % DR < DR // 2
+    row = lax.broadcasted_iota(jnp.int32, (TOK, 64), 0)
+    col = lax.broadcasted_iota(jnp.int32, (TOK, 64), 1)
+    segment = jnp.where(row // SPAN == col, 1.0, 0.0).astype(jnp.bfloat16)
+    for pair in range(H // 2):
+        turned = qr_ref[:, pair * 2 * DR : (pair + 1) * 2 * DR].astype(jnp.float32)
+        swapped = jnp.where(
+            first, pltpu.roll(turned, 2 * DR - DR // 2, 1), pltpu.roll(turned, DR // 2, 1)
+        )
+        signed = jnp.where(first, -swapped, swapped)
+        turned = (turned * cos_ref[...] + signed * sin_ref[...]).astype(jnp.bfloat16)
+        for k in range(2):
+            h = pair * 2 + k
+            out_ref[h, :, :DN] = q_ref[:, h * DN : (h + 1) * DN]
+            out_ref[h, :, DN:] = jnp.concatenate(
+                [turned[:, k * DR : (k + 1) * DR], segment], axis=1
+            )
+
+
+def turn(*inputs):
+    return pl.pallas_call(
+        turn_kernel,
+        out_shape=jax.ShapeDtypeStruct((H, TOK, 256), jnp.bfloat16),
+        compiler_params=pltpu.CompilerParams(vmem_limit_bytes=8 * 1024 * 1024),
+        cost_estimate=pl.CostEstimate(flops=500_000, bytes_accessed=1_500_000, transcendentals=0),
+        name="turn",
+    )(*inputs)
 
 
 def attend_kernel(
-    word_ref, q_ref, qr_ref, cos_ref, sin_ref, lat_ref, seg_ref, w0, w1, w2, w3, out_ref, key_ref
+    q_ref, lat_ref, seg_ref, w0, w1, w2, w3, out_ref, key_ref
 ):
     scale = LOG2E / math.sqrt(DN + DR)
 
@@ -119,26 +142,13 @@
             for h in range(GROUP):
                 key_ref[h, rows, DN:] = tail
 
-    parity = (word_ref[2] + pl.program_id(0)) % NC
-    row = lax.broadcasted_iota(jnp.int32, (TOK, 64), 0)
-    col = lax.broadcasted_iota(jnp.int32, (TOK, 64), 1)
-    segment = jnp.where(row // SPAN == col, 1.0, 0.0).astype(jnp.bfloat16)
+    parity = (lax.axis_index("c") + pl.program_id(0)) % NC
     ones = jnp.ones((KEYS, 128), jnp.bfloat16)
     r128 = lax.broadcasted_iota(jnp.int32, (128, 128), 0)
     c128 = lax.broadcasted_iota(jnp.int32, (128, 128), 1)
-    lane = lax.broadcasted_iota(jnp.int32, (TOK, 2 * DR), 1)
-    first = lane % DR < DR // 2
     for h, w_ref in enumerate((w0, w1, w2, w3)):
-        chip = (word_ref[1] + NX - h) % NX
+        chip = (lax.axis_index("x") + NX - h) % NX
         head = chip * NC + parity
-        turned = qr_ref[:, pl.ds(pl.multiple_of(chip * 2 * DR, 128), 2 * DR)].astype(jnp.float32)
-        swapped = jnp.where(
-            first, pltpu.roll(turned, 2 * DR - DR // 2, 1), pltpu.roll(turned, DR // 2, 1)
-        )
-        signed = jnp.where(first, -swapped, swapped)
-        turned = (turned * cos_ref[...] + signed * sin_ref[...]).astype(jnp.bfloat16)
-        turned = jnp.where(parity == 0, turned[:, :DR], turned[:, DR:])
-        content = q_ref[:, pl.ds(pl.multiple_of(head * DN, 128), DN)]
         pair = jnp.concatenate(
             [
                 jnp.dot(
@@ -149,10 +159,9 @@
             ],
             axis=0,
         )
-        query = jnp.concatenate([content, turned, segment], axis=1)
         key_ref[h, :, :DN] = pair[:, :DN]
         scores = lax.dot_general(
-            query, key_ref[h], (((1,), (1,)), ((), ())), preferred_element_type=jnp.float32
+            q_ref[head], key_ref[h], (((1,), (1,)), ((), ())), preferred_element_type=jnp.float32
         )
         highest = jnp.max(scores, axis=1, keepdims=True) * scale
         weights = jnp.exp2(scores * scale - highest).astype(jnp.bfloat16)
@@ -175,7 +184,7 @@
         out_ref[head, TOK:, :] = jnp.concatenate(rows, axis=0).astype(jnp.bfloat16)
 
 
-def attend(words, query, query_rotary, cosine, sine, lat, seg, weights):
+def attend(query, lat, seg, weights):
     def whole(*shape):
         return pl.BlockSpec(shape, lambda i: (0,) * len(shape))
 
@@ -183,11 +192,7 @@
         attend_kernel,
         grid=(NC,),
         in_specs=[
-            pl.BlockSpec(memory_space=pltpu.SMEM),
-            whole(TOK, H * DN),
-            whole(TOK, H * DR),
-            whole(TOK, 2 * DR),
-            whole(TOK, 2 * DR),
+            whole(H, TOK, 256),
             whole(ROWS, 960),
             whole(KEYS, 128),
         ]
@@ -202,7 +207,7 @@
             flops=3_000_000_000, bytes_accessed=4_000_000, transcendentals=2_400_000
         ),
         name="attend",
-    )(words, query, query_rotary, cosine, sine, lat, seg, *weights)
+    )(query, lat, seg, *weights)
 
 
 def merge_kernel(in_ref, out_ref):
@@ -359,21 +364,18 @@
 
     own_places = (sp_index * 8 + tp_index) * 24 + jnp.arange(24, dtype=jnp.int32)
     cosine, sine = tables(own_places)
-    words = jnp.stack([yi, lax.axis_index("x"), lax.axis_index("c")]).astype(jnp.int32)
-    own, kv, same, cross = prepare(
-        words, latents, key_rotary, latent_gain.reshape(1, -1), cosine, sine, key_up, value_up,
+    own, kv, cut = prepare(
+        latents, key_rotary, latent_gain.reshape(1, -1), cosine, sine, key_up, value_up,
         gate_proj, up_proj, down_proj.T,
     )
-    back = [same] + [
-        lax.ppermute(piece, ("g", "p"), [(i, (i + s) % NY) for i in range(NY)])
-        for s, piece in ((1, cross), (2, same), (3, cross))
-    ]
-    mixer = lax.all_gather(put(words, *back), ("z", "c"), axis=0, tiled=True)
+    cut = lax.all_to_all(cut, ("g", "p"), split_axis=0, concat_axis=0, tiled=True)
+    mixer = lax.all_gather(put(cut), ("z", "c"), axis=0, tiled=True)
     mixer = mixer.reshape(NZ, NC * 1056, 128)
 
     lat = lax.all_to_all(own, "z", split_axis=0, concat_axis=0, tiled=True)
     lat = lat.reshape(NZ * 8, 960)
-    pair = jnp.stack([kv, lax.ppermute(kv, "c", [(0, 1), (1, 0)])])
+    partner = lax.ppermute(kv, "c", [(0, 1), (1, 0)])
+    pair = jnp.stack([kv, partner])
     weights = [pair] + [
         lax.ppermute(pair, "x", [(i, (i + s) % NX) for i in range(NX)]) for s in range(1, NX)
     ]
@@ -390,7 +392,8 @@
     cosine, sine = tables(sp_index * TOK + jnp.arange(TOK, dtype=jnp.int32))
     cosine, sine = (jnp.concatenate([t] * 4, axis=1) for t in (cosine, sine))
 
-    parts = attend(words, query_content, query_rotary, cosine, sine, lat, seg, weights)
+    query = turn(query_content, query_rotary, cosine, sine)
+    parts = attend(query, lat, seg, weights)
     parts = lax.all_to_all(parts, ("x", "c"), split_axis=0, concat_axis=0, tiled=True)
     heads = lax.all_to_all(merge(parts), ("x", "c"), split_axis=0, concat_axis=0, tiled=True)
     mixed_rows, sent = project(heads, out_proj, residual)

time: 165 us -> 154 us (0.933)
  starting transfers between devices: 41.2 us -> 29.7 us
  blocking collectives: 78 us -> 87.4 us
  waiting for transfers between devices: 4.37 us -> 0.03 us
  local copies, waits for them, and re-layouts: 4.17 us -> 2.03 us
    all_to_all x0 -> x1, blocking collectives: none -> 10.7 us  [layer(): lax.all_to_all(cut, ('g', 'p'), split_axis=0, concat_axis=0, tiled=True)]
    ppermute x4 -> x1, starting transfers between devices: 18.7 us -> 8.31 us  [layer(): partner = lax.ppermute(kv, 'c', [(0, 1), (1, 0)])]
    ppermute x4 -> x1, waiting for transfers between devices: 2.55 us -> 0.01 us  [layer(): partner = lax.ppermute(kv, 'c', [(0, 1), (1, 0)])]
    unnamed x16 -> x10, local copies, waits for them, and re-layouts: 4.17 us -> 2.03 us
    all_to_all x1, waiting for transfers between devices: 1.8 us -> 0.01 us  [layer(): lat = lax.all_to_all(own, 'z', split_axis=0, concat_axis=0, tiled=True)]
    pallas_call x2 -> x3, Pallas kernels: 9.97 us -> 9.04 us  [the longest x1 7.76 us: attend(): pl.pallas_call(attend_kernel, grid=(NC,), in_specs=[whole(H, TOK, 256), w...]
  transfers between devices with their start and end apart: 9 -> 6, of which waited for: 2 -> 0; matrix products, arithmetic and copies ran while one was open for 1% -> 1% of each run, Pallas kernels for 6% -> 6%
where the time goes in v6:
time: 154 us
  blocking collectives  87.4 us (57%)
  starting transfers between devices  29.7 us (19%)
  Pallas kernels  17.4 us (11%)
  between operations  13.6 us (9%)
  other arithmetic  3.39 us (2%)
  local copies, waits for them, and re-layouts  2.03 us (1%)
    all_to_all x1, blocking collectives, layer(): lax.all_to_all(parts, ('x', 'c'), split_axis=0, concat_axis=0, tiled=True)  21 us
    all_to_all x1, blocking collectives, layer(): lax.all_to_all(sent, ('p', 'x', 'c'), split_axis=0, concat_axis=0, tiled=...  16.2 us
    all_to_all x1, blocking collectives, layer(): lax.all_to_all(partial_sums, ('p', 'x', 'c'), split_axis=0, concat_axis=0...  16.1 us
    all_gather x1, blocking collectives, layer(): lat = lax.all_gather(lat, ('g', 'p'), axis=0, tiled=True)  12.1 us
    all_to_all x1, blocking collectives, layer(): lax.all_to_all(merge(parts), ('x', 'c'), split_axis=0, concat_axis=0, til...  11.3 us
    all_to_all x1, starting transfers between devices, layer(): lat = lax.all_to_all(own, 'z', split_axis=0, concat_axis=0, tiled=True)  10.8 us
    all_to_all x1, blocking collectives, layer(): lax.all_to_all(cut, ('g', 'p'), split_axis=0, concat_axis=0, tiled=True)  10.7 us
    ppermute x3, starting transfers between devices, layer(): lax.ppermute(pair, 'x', [(i, (i + s) % NX) for i in range(NX)])  10.6 us
  transfers between devices with their start and end apart: 6, of which 0 were waited for; matrix products, arithmetic and copies ran while one was open for 1% of the time, Pallas kernels for 6%

profile of v6, /device:TPU:1, one launch (start us, length us, event | category | flops | bytes accessed | tf_op | source)
XLA Modules:
  0.0 153.6 jit_solution(10657676516774657301)
XLA Ops:
  6.5 0.0 all-gather.2.cloned.1.call-start
  6.6 0.7 multiply_sine_fusion.1
  7.3 2.0 %prepare.1 = (bf16[16,8,960]{2,1,0:T(8,128)(2,1)}, bf16[256,256]{1,0:T(8,128)(2,1)}, bf16[4,32,1056]{2,1,0:T(8,128)(2,1)}) custom-call(bf16[24,256]{1,0:T(8,128)(2,1)} %lat_ref.1, bf16[24,64]{1,0:T(8,128)(2,1)} %rot_ref.1, f32[1,256]{1,0:T(1,128)} %bitcast.18, f32[24,32]{1,0:T(8,128)} %get-tuple-element.18.cos_ref, f32[24,32]{1,0:T(8,128)} %get-tuple-element.17.sin_ref, ...), custom_call_target="tpu_custom_call" | custom-call | flops 100000 | bytes 300000 | tf_op jit(solution)/shard_map/prepare/pallas_call | solution.py:64
  9.3 10.7 %all_to_all.30.in_ref = bf16[4,32,1056]{2,1,0:T(8,128)(2,1)S(1)} all-to-all(bf16[4,32,1056]{2,1,0:T(8,128)(2,1)} %get-tuple-element.14), channel_id=1, replica_groups=mesh['z'=16,'g'=2,'p'=2,'x'=4,'c'=2] {'g','p'}, dimensions={0} | all-to-all | bytes 540672 | tf_op jit(solution)/shard_map/all_to_all | solution.py:371
  20.0 0.9 put.1
  20.9 0.0 all-gather.2.cloned.1.call-update
  20.9 8.3 %collective-permute-start = (bf16[256,256]{1,0:T(8,128)(2,1)}, bf16[256,256]{1,0:T(8,128)(2,1)S(1)}, u32[]{:S(2)}, u32[]{:S(2)}) collective-permute-start(bf16[256,256]{1,0:T(8,128)(2,1)} %get-tuple-element.11), channel_id=1, source_target_pairs={{0,1},{1,0},{2,3},{3,2},{4,5},{5,4},{6,7},{7,6},{8,9},{9,8},{10,11... | collective-permute-start | bytes 393224 | tf_op jit(solution)/shard_map/ppermute | solution.py:377
  29.2 10.8 %all-to-all-start = ((bf16[16,8,960]{2,1,0:T(8,128)(2,1)}), bf16[16,8,960]{2,1,0:T(8,128)(2,1)S(1)}, u32[]{:S(2)}, u32[]{:S(2)}) async-start(bf16[16,8,960]{2,1,0:T(8,128)(2,1)} %get-tuple-element.10), calls=%async_computation | async-start | bytes 524288 | tf_op jit(solution)/shard_map/all_to_all | solution.py:375
  40.1 0.3 select_convert_fusion.seg_ref
  40.3 0.4 multiply_sine_fusion
  40.8 0.0 copy-start
  40.8 0.2 pad_maximum_fusion.1
  41.0 0.0 copy-start.1
  41.0 1.1 copy-done.1
  42.1 0.0 copy-start.2
  42.1 0.9 copy-done.2
  43.0 0.0 copy-start.3
  43.0 0.4 turn.1.q_ref
  43.5 0.0 collective-permute-done
  43.5 0.9 pad_maximum_fusion.w0
  44.4 3.1 %collective-permute-start.1 = (bf16[2,256,256]{2,1,0:T(8,128)(2,1)S(1)}, bf16[2,256,256]{2,1,0:T(8,128)(2,1)S(1)}, u32[]{:S(2)}, u32[]{:S(2)}) collective-permute-start(bf16[2,256,256]{2,1,0:T(8,128)(2,1)S(1)} %pad_maximum_fusion.w0), channel_id=1, source_target_pairs={{0,2},{2,4},{4,6},{6,0},{1,3},{3,5},{5,7},{7,1},{8,10},{10,12},{12... | collective-permute-start | bytes 786440 | tf_op jit(solution)/shard_map/ppermute | solution.py:380
  47.5 4.4 %collective-permute-start.2 = (bf16[2,256,256]{2,1,0:T(8,128)(2,1)S(1)}, bf16[2,256,256]{2,1,0:T(8,128)(2,1)S(1)}, u32[]{:S(2)}, u32[]{:S(2)}) collective-permute-start(bf16[2,256,256]{2,1,0:T(8,128)(2,1)S(1)} %pad_maximum_fusion.w0), channel_id=1, source_target_pairs={{0,4},{2,6},{4,0},{6,2},{1,5},{3,7},{5,1},{7,3},{8,12},{10,14},{12... | collective-permute-start | bytes 786440 | tf_op jit(solution)/shard_map/ppermute | solution.py:380
  51.9 3.1 %collective-permute-start.3 = (bf16[2,256,256]{2,1,0:T(8,128)(2,1)S(1)}, bf16[2,256,256]{2,1,0:T(8,128)(2,1)S(1)}, u32[]{:S(2)}, u32[]{:S(2)}) collective-permute-start(bf16[2,256,256]{2,1,0:T(8,128)(2,1)S(1)} %pad_maximum_fusion.w0), channel_id=1, source_target_pairs={{0,6},{2,0},{4,2},{6,4},{1,7},{3,1},{5,3},{7,5},{8,14},{10,8},{12,... | collective-permute-start | bytes 786440 | tf_op jit(solution)/shard_map/ppermute | solution.py:380
  55.0 0.0 all-to-all-done
  55.0 0.0 copy-start.4
  55.0 12.1 %all_gather.6.lat_ref = bf16[512,960]{1,0:T(8,128)(2,1)S(1)} all-gather(bf16[128,960]{1,0:T(8,128)(2,1)S(1)} %bitcast.14), channel_id=1, replica_groups=mesh['z'=16,'g'=2,'p'=2,'x'=4,'c'=2] {'g','p'}, dimensions={0}, use_global_device_ids=true | all-gather | bytes 1228800 | tf_op jit(solution)/shard_map/all_gather | solution.py:383
  67.2 0.0 collective-permute-done.1.w1
  67.2 0.0 collective-permute-done.2.w2
  67.2 0.0 collective-permute-done.3.w3
  67.2 7.8 %attend.1 = bf16[8,208,128]{2,1,0:T(8,128)(2,1)S(1)} custom-call(bf16[8,192,256]{2,1,0:T(8,128)(2,1)S(1)} %turn.1.q_ref, bf16[512,960]{1,0:T(8,128)(2,1)S(1)} %all_gather.6.lat_ref, bf16[1536,128]{1,0:T(8,128)(2,1)S(1)} %select_convert_fusion.seg_ref, bf16[2,256,256]{2,1,0:T(8,128)(2,1)S(1)} %pad_maximum_fusion.w0, ...), custom_call_target="tpu_custom_call" | custom-call | flops 3000000000 | bytes 4000000 | tf_op jit(solution)/shard_map/attend/pallas_call | solution.py:191
  74.9 21.0 %all_to_all.31.in_ref = bf16[8,208,128]{2,1,0:T(8,128)(2,1)S(1)} all-to-all(bf16[8,208,128]{2,1,0:T(8,128)(2,1)S(1)} %attend.1), channel_id=1, replica_groups=mesh['z'=16,'g'=2,'p'=2,'x'=4,'c'=2] {'x','c'}, dimensions={0} | all-to-all | bytes 851968 | tf_op jit(solution)/shard_map/all_to_all | solution.py:397
  96.0 0.6 merge.1
  96.6 11.3 %all_to_all.32.heads_ref = bf16[8,192,128]{2,1,0:T(8,128)(2,1)S(1)} all-to-all(bf16[8,192,128]{2,1,0:T(8,128)(2,1)S(1)} %merge.1), channel_id=1, replica_groups=mesh['z'=16,'g'=2,'p'=2,'x'=4,'c'=2] {'x','c'}, dimensions={0} | all-to-all | bytes 786432 | tf_op jit(solution)/shard_map/all_to_all | solution.py:398
  107.8 0.0 copy-done
  107.8 0.0 copy-done.3
  107.9 0.3 project.1
  108.1 16.2 %all_to_all.33.rows_ref = bf16[16,96,256]{2,1,0:T(8,128)(2,1)S(1)} all-to-all(bf16[16,96,256]{2,1,0:T(8,128)(2,1)S(1)} %get-tuple-element.13), channel_id=1, replica_groups=mesh['z'=16,'g'=2,'p'=2,'x'=4,'c'=2] {'p','x','c'}, dimensions={0} | all-to-all | bytes 1572864 | tf_op jit(solution)/shard_map/all_to_all | solution.py:400
  124.3 0.0 all-gather.2.cloned.1.call-done
  124.3 0.0 copy-done.4
  124.3 5.6 %mix.1 = bf16[16,96,256]{2,1,0:T(8,128)(2,1)S(1)} custom-call(bf16[16,96,256]{2,1,0:T(8,128)(2,1)S(1)} %all_to_all.33.rows_ref, f32[1,2048]{1,0:T(1,128)S(1)} %bitcast.11, bf16[16,2112,128]{2,1,0:T(8,128)(2,1)} %bitcast.12), custom_call_target="tpu_custom_call" | custom-call | flops 1700000000 | bytes 10000000 | tf_op jit(solution)/shard_map/mix/pallas_call | solution.py:301
  129.9 16.1 %all_to_all.34 = bf16[16,96,256]{2,1,0:T(8,128)(2,1)S(1)} all-to-all(bf16[16,96,256]{2,1,0:T(8,128)(2,1)S(1)} %mix.1), channel_id=1, replica_groups=mesh['z'=16,'g'=2,'p'=2,'x'=4,'c'=2] {'p','x','c'}, dimensions={0} | all-to-all | bytes 1572864 | tf_op jit(solution)/shard_map/all_to_all | solution.py:402
  146.0 0.1 convert_reduce_fusion
  146.1 0.7 add_convert_fusion
  (6 shorter events, 0.1 us)
Async XLA Ops:
  6.5 117.8 %all-gather.2.cloned.1.call-start = ((), (), s32[]{:S(2)}) async-start(), calls=%async_computation.6 | async-start | bytes 8921088 | tf_op jit(solution)/shard_map/all_gather | solution.py:372
  20.9 22.6 %collective-permute-start = (bf16[256,256]{1,0:T(8,128)(2,1)}, bf16[256,256]{1,0:T(8,128)(2,1)S(1)}, u32[]{:S(2)}, u32[]{:S(2)}) collective-permute-start(bf16[256,256]{1,0:T(8,128)(2,1)} %get-tuple-element.11), channel_id=1, source_target_pairs={{0,1},{1,0},{2,3},{3,2},{4,5},{5,4},{6,7},{7,6},{8,9},{9,8},{10,11... | collective-permute-start | bytes 393224 | tf_op jit(solution)/shard_map/ppermute | solution.py:377
  29.2 25.8 %all-to-all-start = ((bf16[16,8,960]{2,1,0:T(8,128)(2,1)}), bf16[16,8,960]{2,1,0:T(8,128)(2,1)S(1)}, u32[]{:S(2)}, u32[]{:S(2)}) async-start(bf16[16,8,960]{2,1,0:T(8,128)(2,1)} %get-tuple-element.10), calls=%async_computation | async-start | bytes 524288 | tf_op jit(solution)/shard_map/all_to_all | solution.py:375
  40.8 67.1 %copy-start = (bf16[1024,256]{1,0:T(8,128)(2,1)S(1)}, bf16[1024,256]{1,0:T(8,128)(2,1)}, u32[]{:S(2)}) copy-start(bf16[1024,256]{1,0:T(8,128)(2,1)} %w_ref.1) | copy-start | bytes 1572868
  41.0 1.1 copy-start.1
  42.1 0.9 copy-start.2
  43.0 64.8 %copy-start.3 = (bf16[192,256]{1,0:T(8,128)(2,1)S(1)}, bf16[192,256]{1,0:T(8,128)(2,1)}, u32[]{:S(2)}) copy-start(bf16[192,256]{1,0:T(8,128)(2,1)} %res_ref.1) | copy-start | bytes 294916
  44.4 22.8 %collective-permute-start.1 = (bf16[2,256,256]{2,1,0:T(8,128)(2,1)S(1)}, bf16[2,256,256]{2,1,0:T(8,128)(2,1)S(1)}, u32[]{:S(2)}, u32[]{:S(2)}) collective-permute-start(bf16[2,256,256]{2,1,0:T(8,128)(2,1)S(1)} %pad_maximum_fusion.w0), channel_id=1, source_target_pairs={{0,2},{2,4},{4,6},{6,0},{1,3},{3,5},{5,7},{7,1},{8,10},{10,12},{12... | collective-permute-start | bytes 786440 | tf_op jit(solution)/shard_map/ppermute | solution.py:380
  47.5 19.6 %collective-permute-start.2 = (bf16[2,256,256]{2,1,0:T(8,128)(2,1)S(1)}, bf16[2,256,256]{2,1,0:T(8,128)(2,1)S(1)}, u32[]{:S(2)}, u32[]{:S(2)}) collective-permute-start(bf16[2,256,256]{2,1,0:T(8,128)(2,1)S(1)} %pad_maximum_fusion.w0), channel_id=1, source_target_pairs={{0,4},{2,6},{4,0},{6,2},{1,5},{3,7},{5,1},{7,3},{8,12},{10,14},{12... | collective-permute-start | bytes 786440 | tf_op jit(solution)/shard_map/ppermute | solution.py:380
  51.9 15.2 %collective-permute-start.3 = (bf16[2,256,256]{2,1,0:T(8,128)(2,1)S(1)}, bf16[2,256,256]{2,1,0:T(8,128)(2,1)S(1)}, u32[]{:S(2)}, u32[]{:S(2)}) collective-permute-start(bf16[2,256,256]{2,1,0:T(8,128)(2,1)S(1)} %pad_maximum_fusion.w0), channel_id=1, source_target_pairs={{0,6},{2,0},{4,2},{6,4},{1,7},{3,1},{5,3},{7,5},{8,14},{10,8},{12,... | collective-permute-start | bytes 786440 | tf_op jit(solution)/shard_map/ppermute | solution.py:380
  55.0 69.3 %copy-start.4 = (f32[2048]{0:T(1024)S(1)}, f32[2048]{0:T(1024)}, u32[]{:S(2)}) copy-start(f32[2048]{0:T(1024)} %param.22) | copy-start | bytes 24580
Sparse Core Ops, SparseCore 0:
  21.0 92.6 all-gather.1

commit v7 on v6

--- a/solution.py
+++ b/solution.py
@@ -2,6 +2,7 @@
 
 import jax
 import jax.numpy as jnp
+import numpy as np
 from jax import lax
 from jax.experimental import pallas as pl
 from jax.experimental.pallas import tpu as pltpu
@@ -28,13 +29,22 @@
 
 
 def tables(places):
-    inverse = 10000.0 ** (-jnp.arange(0, DR, 2, dtype=jnp.float32) / DR)
-    angles = places.astype(jnp.float32)[:, None] * inverse[None, :]
-    return jnp.cos(angles), jnp.sin(angles)
+    inverse = 10000.0 ** (-np.arange(0, DR, 2) / DR)
+    angles = np.tile(places[:, None] * inverse[None, :], (1, 4))
+    return jnp.asarray(np.concatenate([np.cos(angles), np.sin(angles)], axis=1), jnp.float32)
+
+
+def joined(block, inside):
+    cos_a, sin_a, cos_b, sin_b = block[:, :128], block[:, 128:], inside[:, :128], inside[:, 128:]
+    return cos_a * cos_b - sin_a * sin_b, sin_a * cos_b + cos_a * sin_b
+
+
+def block_index():
+    return lax.axis_index("z") * NY + lax.axis_index("g") * NP + lax.axis_index("p")
 
 
 def prepare_kernel(
-    lat_ref, rot_ref, gain_ref, cos_ref, sin_ref, k_ref, v_ref, gate_ref, up_ref, down_ref,
+    lat_ref, rot_ref, gain_ref, block_ref, inside_ref, k_ref, v_ref, gate_ref, up_ref, down_ref,
     out_ref, kv_ref, cut_ref,
 ):
     for k in range(NP):
@@ -51,7 +61,12 @@
     normed = (widened * factor * gain_ref[...]).astype(jnp.bfloat16)
     widened = rot_ref[...].astype(jnp.float32)
     a, b = widened[:, : DR // 2], widened[:, DR // 2 :]
-    cosine, sine = cos_ref[...], sin_ref[...]
+    tp = lax.axis_index("x") * NC + lax.axis_index("c")
+    cosine, sine = joined(
+        block_ref[pl.ds(block_index(), 1), :],
+        inside_ref[pl.ds(pl.multiple_of(tp * 24, 8), 24), :],
+    )
+    cosine, sine = cosine[:, : DR // 2], sine[:, : DR // 2]
     turned = jnp.concatenate([a * cosine - b * sine, b * cosine + a * sine], axis=-1)
     turned = turned.astype(jnp.bfloat16)
     keys = [slice(j * 8, (j + 1) * 8) for j in range(3)]
@@ -96,7 +111,8 @@
     )(pieces)
 
 
-def turn_kernel(q_ref, qr_ref, cos_ref, sin_ref, out_ref):
+def turn_kernel(q_ref, qr_ref, block_ref, inside_ref, out_ref):
+    cosine, sine = joined(block_ref[pl.ds(block_index(), 1), :], inside_ref[...])
     lane = lax.broadcasted_iota(jnp.int32, (TOK, 2 * DR), 1)
     first = lane % DR < DR // 2
     row = lax.broadcasted_iota(jnp.int32, (TOK, 64), 0)
@@ -108,7 +124,7 @@
             first, pltpu.roll(turned, 2 * DR - DR // 2, 1), pltpu.roll(turned, DR // 2, 1)
         )
         signed = jnp.where(first, -swapped, swapped)
-        turned = (turned * cos_ref[...] + signed * sin_ref[...]).astype(jnp.bfloat16)
+        turned = (turned * cosine + signed * sine).astype(jnp.bfloat16)
         for k in range(2):
             h = pair * 2 + k
             out_ref[h, :, :DN] = q_ref[:, h * DN : (h + 1) * DN]
@@ -362,10 +378,9 @@
     sp_index = zi * NY + yi
     tp_index = lax.axis_index("x") * NC + lax.axis_index("c")
 
-    own_places = (sp_index * 8 + tp_index) * 24 + jnp.arange(24, dtype=jnp.int32)
-    cosine, sine = tables(own_places)
+    block, inside = tables(np.arange(NZ * NY) * TOK), tables(np.arange(TOK))
     own, kv, cut = prepare(
-        latents, key_rotary, latent_gain.reshape(1, -1), cosine, sine, key_up, value_up,
+        latents, key_rotary, latent_gain.reshape(1, -1), block, inside, key_up, value_up,
         gate_proj, up_proj, down_proj.T,
     )
     cut = lax.all_to_all(cut, ("g", "p"), split_axis=0, concat_axis=0, tiled=True)
@@ -389,10 +404,7 @@
     lane = jnp.arange(128, dtype=jnp.int32)[None, :] - DR
     hidden_from = (lane >= 0) & (lane < TOK // SPAN) & (ahead_of > lane)
     seg = jnp.where(hidden_from, masked_score, 0.0).astype(jnp.bfloat16)
-    cosine, sine = tables(sp_index * TOK + jnp.arange(TOK, dtype=jnp.int32))
-    cosine, sine = (jnp.concatenate([t] * 4, axis=1) for t in (cosine, sine))
-
-    query = turn(query_content, query_rotary, cosine, sine)
+    query = turn(query_content, query_rotary, block, inside)
     parts = attend(query, lat, seg, weights)
     parts = lax.all_to_all(parts, ("x", "c"), split_axis=0, concat_axis=0, tiled=True)
     heads = lax.all_to_all(merge(parts), ("x", "c"), split_axis=0, concat_axis=0, tiled=True)

time: 154 us -> 149 us (0.968)
  blocking collectives: 87.4 us -> 81.6 us
  local copies, waits for them, and re-layouts: 2.03 us -> 3.7 us
    all_to_all x1, blocking collectives: 21 us -> 15.2 us  [layer(): lax.all_to_all(parts, ('x', 'c'), split_axis=0, concat_axis=0, tiled=True)]
    all_to_all x1, starting transfers between devices: 10.8 us -> 15.1 us  [layer(): lat = lax.all_to_all(own, 'z', split_axis=0, concat_axis=0, tiled=True)]
    ppermute x1, starting transfers between devices: 8.31 us -> 4.29 us  [layer(): partner = lax.ppermute(kv, 'c', [(0, 1), (1, 0)])]
    unnamed x10 -> x14, local copies, waits for them, and re-layouts: 2.03 us -> 3.7 us
where the time goes in v7:
time: 149 us; the launch traced here: 148 us
  blocking collectives  81.6 us (55%)
  starting transfers between devices  29.9 us (20%)
  Pallas kernels  17.5 us (12%)
  between operations  13.6 us (9%)
  local copies, waits for them, and re-layouts  3.7 us (2%)
  other arithmetic  2 us (1%)
    all_to_all x1, blocking collectives, layer(): lax.all_to_all(sent, ('p', 'x', 'c'), split_axis=0, concat_axis=0, tiled=...  16.1 us
    all_to_all x1, blocking collectives, layer(): lax.all_to_all(partial_sums, ('p', 'x', 'c'), split_axis=0, concat_axis=0...  16.1 us
    all_to_all x1, blocking collectives, layer(): lax.all_to_all(parts, ('x', 'c'), split_axis=0, concat_axis=0, tiled=True)  15.2 us
    all_to_all x1, starting transfers between devices, layer(): lat = lax.all_to_all(own, 'z', split_axis=0, concat_axis=0, tiled=True)  15.1 us
    all_gather x1, blocking collectives, layer(): lat = lax.all_gather(lat, ('g', 'p'), axis=0, tiled=True)  12.2 us
    all_to_all x1, blocking collectives, layer(): lax.all_to_all(merge(parts), ('x', 'c'), split_axis=0, concat_axis=0, til...  11.3 us
    all_to_all x1, blocking collectives, layer(): lax.all_to_all(cut, ('g', 'p'), split_axis=0, concat_axis=0, tiled=True)  10.7 us
    ppermute x3, starting transfers between devices, layer(): lax.ppermute(pair, 'x', [(i, (i + s) % NX) for i in range(NX)])  10.5 us
  transfers between devices with their start and end apart: 6, of which 0 were waited for; matrix products, arithmetic and copies ran while one was open for 1% of the time, Pallas kernels for 6%

profile of v7, /device:TPU:1, one launch (start us, length us, event | category | flops | bytes accessed | tf_op | source)
XLA Modules:
  0.0 148.4 jit_solution(6671532664924726608)
XLA Ops:
  6.5 0.0 all-gather.2.cloned.1.call-start
  6.5 2.1 %prepare.1 = (bf16[16,8,960]{2,1,0:T(8,128)(2,1)}, bf16[256,256]{1,0:T(8,128)(2,1)}, bf16[4,32,1056]{2,1,0:T(8,128)(2,1)}) custom-call(bf16[24,256]{1,0:T(8,128)(2,1)} %lat_ref.1, bf16[24,64]{1,0:T(8,128)(2,1)} %rot_ref.1, f32[1,256]{1,0:T(1,128)} %bitcast.18, f32[64,256]{1,0:T(8,128)} %constant.128.clone.block_ref, f32[192,256]{1,0:T(8,128)} %constant.129.clone.inside_ref, ...), custom_call_target="tpu_custom_call" | custom-call | flops 100000 | bytes 300000 | tf_op jit(solution)/shard_map/prepare/pallas_call | solution.py:79
  8.6 10.7 %all_to_all.30.in_ref = bf16[4,32,1056]{2,1,0:T(8,128)(2,1)S(1)} all-to-all(bf16[4,32,1056]{2,1,0:T(8,128)(2,1)} %get-tuple-element.14), channel_id=1, replica_groups=mesh['z'=16,'g'=2,'p'=2,'x'=4,'c'=2] {'g','p'}, dimensions={0} | all-to-all | bytes 540672 | tf_op jit(solution)/shard_map/all_to_all | solution.py:386
  19.3 0.9 put.1
  20.2 0.0 all-gather.2.cloned.1.call-update
  20.2 15.1 %all-to-all-start = ((bf16[16,8,960]{2,1,0:T(8,128)(2,1)}), bf16[16,8,960]{2,1,0:T(8,128)(2,1)S(1)}, u32[]{:S(2)}, u32[]{:S(2)}) async-start(bf16[16,8,960]{2,1,0:T(8,128)(2,1)} %get-tuple-element.10), calls=%async_computation | async-start | bytes 524288 | tf_op jit(solution)/shard_map/all_to_all | solution.py:390
  35.3 4.3 %collective-permute-start = (bf16[256,256]{1,0:T(8,128)(2,1)}, bf16[256,256]{1,0:T(8,128)(2,1)S(1)}, u32[]{:S(2)}, u32[]{:S(2)}) collective-permute-start(bf16[256,256]{1,0:T(8,128)(2,1)} %get-tuple-element.11), channel_id=1, source_target_pairs={{0,1},{1,0},{2,3},{3,2},{4,5},{5,4},{6,7},{7,6},{8,9},{9,8},{10,11... | collective-permute-start | bytes 393224 | tf_op jit(solution)/shard_map/ppermute | solution.py:392
  39.7 0.0 copy-start.5
  39.7 0.3 select_convert_fusion.seg_ref
  40.0 0.0 copy-start
  40.0 0.9 copy-done
  40.9 0.0 copy-start.2
  40.9 1.0 copy-done.2
  41.9 0.0 copy-start.3
  41.9 0.8 copy-done.3
  42.8 0.0 copy-start.4
  42.8 0.9 copy-done.4
  43.7 0.0 copy-start.1
  43.7 0.4 turn.1.q_ref
  44.1 0.0 collective-permute-done
  44.1 0.9 pad_maximum_fusion.w0
  45.1 3.1 %collective-permute-start.1 = (bf16[2,256,256]{2,1,0:T(8,128)(2,1)S(1)}, bf16[2,256,256]{2,1,0:T(8,128)(2,1)S(1)}, u32[]{:S(2)}, u32[]{:S(2)}) collective-permute-start(bf16[2,256,256]{2,1,0:T(8,128)(2,1)S(1)} %pad_maximum_fusion.w0), channel_id=1, source_target_pairs={{0,2},{2,4},{4,6},{6,0},{1,3},{3,5},{5,7},{7,1},{8,10},{10,12},{12... | collective-permute-start | bytes 786440 | tf_op jit(solution)/shard_map/ppermute | solution.py:395
  48.2 4.4 %collective-permute-start.2 = (bf16[2,256,256]{2,1,0:T(8,128)(2,1)S(1)}, bf16[2,256,256]{2,1,0:T(8,128)(2,1)S(1)}, u32[]{:S(2)}, u32[]{:S(2)}) collective-permute-start(bf16[2,256,256]{2,1,0:T(8,128)(2,1)S(1)} %pad_maximum_fusion.w0), channel_id=1, source_target_pairs={{0,4},{2,6},{4,0},{6,2},{1,5},{3,7},{5,1},{7,3},{8,12},{10,14},{12... | collective-permute-start | bytes 786440 | tf_op jit(solution)/shard_map/ppermute | solution.py:395
  52.5 3.1 %collective-permute-start.3 = (bf16[2,256,256]{2,1,0:T(8,128)(2,1)S(1)}, bf16[2,256,256]{2,1,0:T(8,128)(2,1)S(1)}, u32[]{:S(2)}, u32[]{:S(2)}) collective-permute-start(bf16[2,256,256]{2,1,0:T(8,128)(2,1)S(1)} %pad_maximum_fusion.w0), channel_id=1, source_target_pairs={{0,6},{2,0},{4,2},{6,4},{1,7},{3,1},{5,3},{7,5},{8,14},{10,8},{12,... | collective-permute-start | bytes 786440 | tf_op jit(solution)/shard_map/ppermute | solution.py:395
  55.6 0.0 all-to-all-done
  55.6 0.0 copy-start.6
  55.6 12.2 %all_gather.6.lat_ref = bf16[512,960]{1,0:T(8,128)(2,1)S(1)} all-gather(bf16[128,960]{1,0:T(8,128)(2,1)S(1)} %bitcast.14), channel_id=1, replica_groups=mesh['z'=16,'g'=2,'p'=2,'x'=4,'c'=2] {'g','p'}, dimensions={0}, use_global_device_ids=true | all-gather | bytes 1228800 | tf_op jit(solution)/shard_map/all_gather | solution.py:398
  67.8 0.0 collective-permute-done.1.w1
  67.8 0.0 collective-permute-done.2.w2
  67.8 0.0 collective-permute-done.3.w3
  67.8 7.8 %attend.1 = bf16[8,208,128]{2,1,0:T(8,128)(2,1)S(1)} custom-call(bf16[8,192,256]{2,1,0:T(8,128)(2,1)S(1)} %turn.1.q_ref, bf16[512,960]{1,0:T(8,128)(2,1)S(1)} %all_gather.6.lat_ref, bf16[1536,128]{1,0:T(8,128)(2,1)S(1)} %select_convert_fusion.seg_ref, bf16[2,256,256]{2,1,0:T(8,128)(2,1)S(1)} %pad_maximum_fusion.w0, ...), custom_call_target="tpu_custom_call" | custom-call | flops 3000000000 | bytes 4000000 | tf_op jit(solution)/shard_map/attend/pallas_call | solution.py:207
  75.6 15.2 %all_to_all.31.in_ref = bf16[8,208,128]{2,1,0:T(8,128)(2,1)S(1)} all-to-all(bf16[8,208,128]{2,1,0:T(8,128)(2,1)S(1)} %attend.1), channel_id=1, replica_groups=mesh['z'=16,'g'=2,'p'=2,'x'=4,'c'=2] {'x','c'}, dimensions={0} | all-to-all | bytes 851968 | tf_op jit(solution)/shard_map/all_to_all | solution.py:409
  90.8 0.6 merge.1
  91.4 11.3 %all_to_all.32.heads_ref = bf16[8,192,128]{2,1,0:T(8,128)(2,1)S(1)} all-to-all(bf16[8,192,128]{2,1,0:T(8,128)(2,1)S(1)} %merge.1), channel_id=1, replica_groups=mesh['z'=16,'g'=2,'p'=2,'x'=4,'c'=2] {'x','c'}, dimensions={0} | all-to-all | bytes 786432 | tf_op jit(solution)/shard_map/all_to_all | solution.py:410
  102.7 0.0 copy-done.5
  102.7 0.0 copy-done.1
  102.7 0.3 project.1
  103.0 16.1 %all_to_all.33.rows_ref = bf16[16,96,256]{2,1,0:T(8,128)(2,1)S(1)} all-to-all(bf16[16,96,256]{2,1,0:T(8,128)(2,1)S(1)} %get-tuple-element.13), channel_id=1, replica_groups=mesh['z'=16,'g'=2,'p'=2,'x'=4,'c'=2] {'p','x','c'}, dimensions={0} | all-to-all | bytes 1572864 | tf_op jit(solution)/shard_map/all_to_all | solution.py:412
  119.1 0.0 all-gather.2.cloned.1.call-done
  119.1 0.0 copy-done.6
  119.1 5.5 %mix.1 = bf16[16,96,256]{2,1,0:T(8,128)(2,1)S(1)} custom-call(bf16[16,96,256]{2,1,0:T(8,128)(2,1)S(1)} %all_to_all.33.rows_ref, f32[1,2048]{1,0:T(1,128)S(1)} %bitcast.11, bf16[16,2112,128]{2,1,0:T(8,128)(2,1)} %bitcast.12), custom_call_target="tpu_custom_call" | custom-call | flops 1700000000 | bytes 10000000 | tf_op jit(solution)/shard_map/mix/pallas_call | solution.py:317
  124.7 16.1 %all_to_all.34 = bf16[16,96,256]{2,1,0:T(8,128)(2,1)S(1)} all-to-all(bf16[16,96,256]{2,1,0:T(8,128)(2,1)S(1)} %mix.1), channel_id=1, replica_groups=mesh['z'=16,'g'=2,'p'=2,'x'=4,'c'=2] {'p','x','c'}, dimensions={0} | all-to-all | bytes 1572864 | tf_op jit(solution)/shard_map/all_to_all | solution.py:414
  140.8 0.1 convert_reduce_fusion
  140.9 0.7 add_convert_fusion
  (3 shorter events, 0.0 us)
Async XLA Ops:
  6.5 112.6 %all-gather.2.cloned.1.call-start = ((), (), s32[]{:S(2)}) async-start(), calls=%async_computation.6 | async-start | bytes 8921088 | tf_op jit(solution)/shard_map/all_gather | solution.py:387
  20.2 35.4 %all-to-all-start = ((bf16[16,8,960]{2,1,0:T(8,128)(2,1)}), bf16[16,8,960]{2,1,0:T(8,128)(2,1)S(1)}, u32[]{:S(2)}, u32[]{:S(2)}) async-start(bf16[16,8,960]{2,1,0:T(8,128)(2,1)} %get-tuple-element.10), calls=%async_computation | async-start | bytes 524288 | tf_op jit(solution)/shard_map/all_to_all | solution.py:390
  35.3 8.8 %collective-permute-start = (bf16[256,256]{1,0:T(8,128)(2,1)}, bf16[256,256]{1,0:T(8,128)(2,1)S(1)}, u32[]{:S(2)}, u32[]{:S(2)}) collective-permute-start(bf16[256,256]{1,0:T(8,128)(2,1)} %get-tuple-element.11), channel_id=1, source_target_pairs={{0,1},{1,0},{2,3},{3,2},{4,5},{5,4},{6,7},{7,6},{8,9},{9,8},{10,11... | collective-permute-start | bytes 393224 | tf_op jit(solution)/shard_map/ppermute | solution.py:392
  39.7 63.0 %copy-start.5 = (bf16[192,256]{1,0:T(8,128)(2,1)S(1)}, bf16[192,256]{1,0:T(8,128)(2,1)}, u32[]{:S(2)}) copy-start(bf16[192,256]{1,0:T(8,128)(2,1)} %res_ref.1) | copy-start | bytes 294916
  40.0 0.9 copy-start
  40.9 1.0 copy-start.2
  41.9 0.8 copy-start.3
  42.8 0.9 copy-start.4
  43.7 59.0 %copy-start.1 = (bf16[1024,256]{1,0:T(8,128)(2,1)S(1)}, bf16[1024,256]{1,0:T(8,128)(2,1)}, u32[]{:S(2)}) copy-start(bf16[1024,256]{1,0:T(8,128)(2,1)} %w_ref.1) | copy-start | bytes 1572868
  45.1 22.7 %collective-permute-start.1 = (bf16[2,256,256]{2,1,0:T(8,128)(2,1)S(1)}, bf16[2,256,256]{2,1,0:T(8,128)(2,1)S(1)}, u32[]{:S(2)}, u32[]{:S(2)}) collective-permute-start(bf16[2,256,256]{2,1,0:T(8,128)(2,1)S(1)} %pad_maximum_fusion.w0), channel_id=1, source_target_pairs={{0,2},{2,4},{4,6},{6,0},{1,3},{3,5},{5,7},{7,1},{8,10},{10,12},{12... | collective-permute-start | bytes 786440 | tf_op jit(solution)/shard_map/ppermute | solution.py:395
  48.2 19.6 %collective-permute-start.2 = (bf16[2,256,256]{2,1,0:T(8,128)(2,1)S(1)}, bf16[2,256,256]{2,1,0:T(8,128)(2,1)S(1)}, u32[]{:S(2)}, u32[]{:S(2)}) collective-permute-start(bf16[2,256,256]{2,1,0:T(8,128)(2,1)S(1)} %pad_maximum_fusion.w0), channel_id=1, source_target_pairs={{0,4},{2,6},{4,0},{6,2},{1,5},{3,7},{5,1},{7,3},{8,12},{10,14},{12... | collective-permute-start | bytes 786440 | tf_op jit(solution)/shard_map/ppermute | solution.py:395
  52.5 15.3 %collective-permute-start.3 = (bf16[2,256,256]{2,1,0:T(8,128)(2,1)S(1)}, bf16[2,256,256]{2,1,0:T(8,128)(2,1)S(1)}, u32[]{:S(2)}, u32[]{:S(2)}) collective-permute-start(bf16[2,256,256]{2,1,0:T(8,128)(2,1)S(1)} %pad_maximum_fusion.w0), channel_id=1, source_target_pairs={{0,6},{2,0},{4,2},{6,4},{1,7},{3,1},{5,3},{7,5},{8,14},{10,8},{12,... | collective-permute-start | bytes 786440 | tf_op jit(solution)/shard_map/ppermute | solution.py:395
  55.6 63.5 %copy-start.6 = (f32[2048]{0:T(1024)S(1)}, f32[2048]{0:T(1024)}, u32[]{:S(2)}) copy-start(f32[2048]{0:T(1024)} %param.24) | copy-start | bytes 24580
Sparse Core Ops, SparseCore 0:
  20.4 88.6 all-gather.1

commit v8 on v7

--- a/solution.py
+++ b/solution.py
@@ -20,7 +20,6 @@
 HALF = TOK // 2
 KEYS = 1536
 PAD = 208
-GROUP = 4
 ROWS = KEYS // 3
 
 epsilon = 1e-06
@@ -143,45 +142,49 @@
     )(*inputs)
 
 
-def attend_kernel(
-    q_ref, lat_ref, seg_ref, w0, w1, w2, w3, out_ref, key_ref
-):
+def attend_kernel(q_ref, lat_ref, seg_ref, w0, w1, w2, w3, out_ref, key_ref):
     scale = LOG2E / math.sqrt(DN + DR)
-
-    @pl.when(pl.program_id(0) == 0)
-    def _():
-        low = lax.broadcasted_iota(jnp.int32, (ROWS, 128), 1) < DR
-        for j in range(3):
-            rows = slice(j * ROWS, (j + 1) * ROWS)
-            pair = lat_ref[:, 768 + j * DR : 832 + j * DR]
-            tail = jnp.where(low, jnp.concatenate([pair, pair], axis=1), seg_ref[rows])
-            for h in range(GROUP):
-                key_ref[h, rows, DN:] = tail
-
-    parity = (lax.axis_index("c") + pl.program_id(0)) % NC
+    low = lax.broadcasted_iota(jnp.int32, (ROWS, 128), 1) < DR
+    for j in range(3):
+        rows = slice(j * ROWS, (j + 1) * ROWS)
+        pair = lat_ref[:, 768 + j * DR : 832 + j * DR]
+        tail = jnp.where(low, jnp.concatenate([pair, pair], axis=1), seg_ref[rows])
+        for h in range(H):
+            key_ref[h, rows, DN:] = tail
+
     ones = jnp.ones((KEYS, 128), jnp.bfloat16)
     r128 = lax.broadcasted_iota(jnp.int32, (128, 128), 0)
     c128 = lax.broadcasted_iota(jnp.int32, (128, 128), 1)
-    for h, w_ref in enumerate((w0, w1, w2, w3)):
-        chip = (lax.axis_index("x") + NX - h) % NX
-        head = chip * NC + parity
+
+    def scored(turn_at):
+        chip = (lax.axis_index("x") + NX - turn_at // NC) % NX
+        head = chip * NC + (lax.axis_index("c") + turn_at) % NC
+        w_ref = (w0, w1, w2, w3)[turn_at // NC]
         pair = jnp.concatenate(
             [
                 jnp.dot(
-                    lat_ref[:, j * 256 : (j + 1) * 256], w_ref[0],
+                    lat_ref[:, j * 256 : (j + 1) * 256], w_ref[turn_at % NC],
                     preferred_element_type=jnp.float32,
                 ).astype(jnp.bfloat16)
                 for j in range(3)
             ],
             axis=0,
         )
-        key_ref[h, :, :DN] = pair[:, :DN]
+        key_ref[turn_at, :, :DN] = pair[:, :DN]
         scores = lax.dot_general(
-            q_ref[head], key_ref[h], (((1,), (1,)), ((), ())), preferred_element_type=jnp.float32
-        )
+            q_ref[head], key_ref[turn_at], (((1,), (1,)), ((), ())),
+            preferred_element_type=jnp.float32,
+        )
+        return head, pair[:, DN:], scores
+
+    following = scored(0)
+    for turn_at in range(H):
+        head, values, scores = following
+        if turn_at + 1 < H:
+            following = scored(turn_at + 1)
         highest = jnp.max(scores, axis=1, keepdims=True) * scale
         weights = jnp.exp2(scores * scale - highest).astype(jnp.bfloat16)
-        both = jnp.concatenate([pair[:, DN:], ones], axis=1)
+        both = jnp.concatenate([values, ones], axis=1)
         sums = jnp.dot(weights, both, preferred_element_type=jnp.float32)
         norm = sums[:, DV:]
         out_ref[head, :TOK, :] = (sums[:, :DV] / norm).astype(jnp.bfloat16)
@@ -201,24 +204,11 @@
 
 
 def attend(query, lat, seg, weights):
-    def whole(*shape):
-        return pl.BlockSpec(shape, lambda i: (0,) * len(shape))
-
     return pl.pallas_call(
         attend_kernel,
-        grid=(NC,),
-        in_specs=[
-            whole(H, TOK, 256),
-            whole(ROWS, 960),
-            whole(KEYS, 128),
-        ]
-        + [pl.BlockSpec((1, 256, 256), lambda i: (i, 0, 0))] * NX,
-        out_specs=whole(H, PAD, 128),
         out_shape=jax.ShapeDtypeStruct((H, PAD, 128), jnp.bfloat16),
-        scratch_shapes=[pltpu.VMEM((GROUP, KEYS, 256), jnp.bfloat16)],
-        compiler_params=pltpu.CompilerParams(
-            dimension_semantics=("arbitrary",), vmem_limit_bytes=24 * 1024 * 1024
-        ),
+        scratch_shapes=[pltpu.VMEM((H, KEYS, 256), jnp.bfloat16)],
+        compiler_params=pltpu.CompilerParams(vmem_limit_bytes=30 * 1024 * 1024),
         cost_estimate=pl.CostEstimate(
             flops=3_000_000_000, bytes_accessed=4_000_000, transcendentals=2_400_000
         ),

time: 149 us -> 147 us (0.987)
  Pallas kernels: 17.5 us -> 16 us
    pallas_call x1, Pallas kernels: 7.77 us -> 6.18 us  [attend(): pl.pallas_call(attend_kernel, out_shape=jax.ShapeDtypeStruct((H, PAD, 128...]
  transfers between devices with their start and end apart: 6 -> 6, of which waited for: 0 -> 0; matrix products, arithmetic and copies ran while one was open for 1% -> 1% of each run, Pallas kernels for 6% -> 5%
where the time goes in v8:
time: 147 us
  blocking collectives  81.6 us (56%)
  starting transfers between devices  29.9 us (20%)
  Pallas kernels  16 us (11%)
  between operations  13.6 us (9%)
  local copies, waits for them, and re-layouts  3.7 us (3%)
  other arithmetic  2 us (1%)
    all_to_all x1, blocking collectives, layer(): lax.all_to_all(sent, ('p', 'x', 'c'), split_axis=0, concat_axis=0, tiled=...  16.1 us
    all_to_all x1, blocking collectives, layer(): lax.all_to_all(partial_sums, ('p', 'x', 'c'), split_axis=0, concat_axis=0...  16.1 us
    all_to_all x1, blocking collectives, layer(): lax.all_to_all(parts, ('x', 'c'), split_axis=0, concat_axis=0, tiled=True)  15.2 us
    all_to_all x1, starting transfers between devices, layer(): lat = lax.all_to_all(own, 'z', split_axis=0, concat_axis=0, tiled=True)  15.1 us
    all_gather x1, blocking collectives, layer(): lat = lax.all_gather(lat, ('g', 'p'), axis=0, tiled=True)  12.2 us
    all_to_all x1, blocking collectives, layer(): lax.all_to_all(merge(parts), ('x', 'c'), split_axis=0, concat_axis=0, til...  11.4 us
    all_to_all x1, blocking collectives, layer(): lax.all_to_all(cut, ('g', 'p'), split_axis=0, concat_axis=0, tiled=True)  10.7 us
    ppermute x3, starting transfers between devices, layer(): lax.ppermute(pair, 'x', [(i, (i + s) % NX) for i in range(NX)])  10.5 us
  transfers between devices with their start and end apart: 6, of which 0 were waited for; matrix products, arithmetic and copies ran while one was open for 1% of the time, Pallas kernels for 5%

profile of v8, /device:TPU:1, one launch (start us, length us, event | category | flops | bytes accessed | tf_op | source)
XLA Modules:
  0.0 146.8 jit_solution(7459722879572373040)
XLA Ops:
  6.5 0.0 all-gather.2.cloned.1.call-start
  6.5 2.1 %prepare.1 = (bf16[16,8,960]{2,1,0:T(8,128)(2,1)}, bf16[256,256]{1,0:T(8,128)(2,1)}, bf16[4,32,1056]{2,1,0:T(8,128)(2,1)}) custom-call(bf16[24,256]{1,0:T(8,128)(2,1)} %lat_ref.1, bf16[24,64]{1,0:T(8,128)(2,1)} %rot_ref.1, f32[1,256]{1,0:T(1,128)} %bitcast.18, f32[64,256]{1,0:T(8,128)} %constant.128.clone.block_ref, f32[192,256]{1,0:T(8,128)} %constant.129.clone.inside_ref, ...), custom_call_target="tpu_custom_call" | custom-call | flops 100000 | bytes 300000 | tf_op jit(solution)/shard_map/prepare/pallas_call | solution.py:78
  8.6 10.7 %all_to_all.30.in_ref = bf16[4,32,1056]{2,1,0:T(8,128)(2,1)S(1)} all-to-all(bf16[4,32,1056]{2,1,0:T(8,128)(2,1)} %get-tuple-element.14), channel_id=1, replica_groups=mesh['z'=16,'g'=2,'p'=2,'x'=4,'c'=2] {'g','p'}, dimensions={0} | all-to-all | bytes 540672 | tf_op jit(solution)/shard_map/all_to_all | solution.py:376
  19.3 0.9 put.1
  20.2 0.0 all-gather.2.cloned.1.call-update
  20.2 15.1 %all-to-all-start = ((bf16[16,8,960]{2,1,0:T(8,128)(2,1)}), bf16[16,8,960]{2,1,0:T(8,128)(2,1)S(1)}, u32[]{:S(2)}, u32[]{:S(2)}) async-start(bf16[16,8,960]{2,1,0:T(8,128)(2,1)} %get-tuple-element.10), calls=%async_computation | async-start | bytes 524288 | tf_op jit(solution)/shard_map/all_to_all | solution.py:380
  35.3 4.3 %collective-permute-start = (bf16[256,256]{1,0:T(8,128)(2,1)}, bf16[256,256]{1,0:T(8,128)(2,1)S(1)}, u32[]{:S(2)}, u32[]{:S(2)}) collective-permute-start(bf16[256,256]{1,0:T(8,128)(2,1)} %get-tuple-element.11), channel_id=1, source_target_pairs={{0,1},{1,0},{2,3},{3,2},{4,5},{5,4},{6,7},{7,6},{8,9},{9,8},{10,11... | collective-permute-start | bytes 393224 | tf_op jit(solution)/shard_map/ppermute | solution.py:382
  39.7 0.0 copy-start.5
  39.7 0.3 select_convert_fusion.seg_ref
  40.0 0.0 copy-start
  40.0 0.9 copy-done
  40.9 0.0 copy-start.2
  40.9 1.0 copy-done.2
  41.9 0.0 copy-start.3
  41.9 0.8 copy-done.3
  42.8 0.0 copy-start.4
  42.8 0.9 copy-done.4
  43.7 0.0 copy-start.1
  43.7 0.4 turn.1.q_ref
  44.1 0.0 collective-permute-done
  44.1 0.9 pad_maximum_fusion.w0
  45.1 3.1 %collective-permute-start.1 = (bf16[2,256,256]{2,1,0:T(8,128)(2,1)S(1)}, bf16[2,256,256]{2,1,0:T(8,128)(2,1)S(1)}, u32[]{:S(2)}, u32[]{:S(2)}) collective-permute-start(bf16[2,256,256]{2,1,0:T(8,128)(2,1)S(1)} %pad_maximum_fusion.w0), channel_id=1, source_target_pairs={{0,2},{2,4},{4,6},{6,0},{1,3},{3,5},{5,7},{7,1},{8,10},{10,12},{12... | collective-permute-start | bytes 786440 | tf_op jit(solution)/shard_map/ppermute | solution.py:385
  48.2 4.4 %collective-permute-start.2 = (bf16[2,256,256]{2,1,0:T(8,128)(2,1)S(1)}, bf16[2,256,256]{2,1,0:T(8,128)(2,1)S(1)}, u32[]{:S(2)}, u32[]{:S(2)}) collective-permute-start(bf16[2,256,256]{2,1,0:T(8,128)(2,1)S(1)} %pad_maximum_fusion.w0), channel_id=1, source_target_pairs={{0,4},{2,6},{4,0},{6,2},{1,5},{3,7},{5,1},{7,3},{8,12},{10,14},{12... | collective-permute-start | bytes 786440 | tf_op jit(solution)/shard_map/ppermute | solution.py:385
  52.5 3.1 %collective-permute-start.3 = (bf16[2,256,256]{2,1,0:T(8,128)(2,1)S(1)}, bf16[2,256,256]{2,1,0:T(8,128)(2,1)S(1)}, u32[]{:S(2)}, u32[]{:S(2)}) collective-permute-start(bf16[2,256,256]{2,1,0:T(8,128)(2,1)S(1)} %pad_maximum_fusion.w0), channel_id=1, source_target_pairs={{0,6},{2,0},{4,2},{6,4},{1,7},{3,1},{5,3},{7,5},{8,14},{10,8},{12,... | collective-permute-start | bytes 786440 | tf_op jit(solution)/shard_map/ppermute | solution.py:385
  55.6 0.0 all-to-all-done
  55.6 0.0 copy-start.6
  55.6 12.2 %all_gather.6.lat_ref = bf16[512,960]{1,0:T(8,128)(2,1)S(1)} all-gather(bf16[128,960]{1,0:T(8,128)(2,1)S(1)} %bitcast.14), channel_id=1, replica_groups=mesh['z'=16,'g'=2,'p'=2,'x'=4,'c'=2] {'g','p'}, dimensions={0}, use_global_device_ids=true | all-gather | bytes 1228800 | tf_op jit(solution)/shard_map/all_gather | solution.py:388
  67.8 0.0 collective-permute-done.1.w1
  67.8 0.0 collective-permute-done.2.w2
  67.8 0.0 collective-permute-done.3.w3
  67.8 6.2 %attend.1 = bf16[8,208,128]{2,1,0:T(8,128)(2,1)S(1)} custom-call(bf16[8,192,256]{2,1,0:T(8,128)(2,1)S(1)} %turn.1.q_ref, bf16[512,960]{1,0:T(8,128)(2,1)S(1)} %all_gather.6.lat_ref, bf16[1536,128]{1,0:T(8,128)(2,1)S(1)} %select_convert_fusion.seg_ref, bf16[2,256,256]{2,1,0:T(8,128)(2,1)S(1)} %pad_maximum_fusion.w0, ...), custom_call_target="tpu_custom_call" | custom-call | flops 3000000000 | bytes 4000000 | tf_op jit(solution)/shard_map/attend/pallas_call | solution.py:207
  74.0 15.2 %all_to_all.31.in_ref = bf16[8,208,128]{2,1,0:T(8,128)(2,1)S(1)} all-to-all(bf16[8,208,128]{2,1,0:T(8,128)(2,1)S(1)} %attend.1), channel_id=1, replica_groups=mesh['z'=16,'g'=2,'p'=2,'x'=4,'c'=2] {'x','c'}, dimensions={0} | all-to-all | bytes 851968 | tf_op jit(solution)/shard_map/all_to_all | solution.py:399
  89.1 0.6 merge.1
  89.7 11.4 %all_to_all.32.heads_ref = bf16[8,192,128]{2,1,0:T(8,128)(2,1)S(1)} all-to-all(bf16[8,192,128]{2,1,0:T(8,128)(2,1)S(1)} %merge.1), channel_id=1, replica_groups=mesh['z'=16,'g'=2,'p'=2,'x'=4,'c'=2] {'x','c'}, dimensions={0} | all-to-all | bytes 786432 | tf_op jit(solution)/shard_map/all_to_all | solution.py:400
  101.1 0.0 copy-done.5
  101.1 0.0 copy-done.1
  101.1 0.3 project.1
  101.4 16.1 %all_to_all.33.rows_ref = bf16[16,96,256]{2,1,0:T(8,128)(2,1)S(1)} all-to-all(bf16[16,96,256]{2,1,0:T(8,128)(2,1)S(1)} %get-tuple-element.13), channel_id=1, replica_groups=mesh['z'=16,'g'=2,'p'=2,'x'=4,'c'=2] {'p','x','c'}, dimensions={0} | all-to-all | bytes 1572864 | tf_op jit(solution)/shard_map/all_to_all | solution.py:402
  117.5 0.0 all-gather.2.cloned.1.call-done
  117.5 0.0 copy-done.6
  117.5 5.5 %mix.1 = bf16[16,96,256]{2,1,0:T(8,128)(2,1)S(1)} custom-call(bf16[16,96,256]{2,1,0:T(8,128)(2,1)S(1)} %all_to_all.33.rows_ref, f32[1,2048]{1,0:T(1,128)S(1)} %bitcast.11, bf16[16,2112,128]{2,1,0:T(8,128)(2,1)} %bitcast.12), custom_call_target="tpu_custom_call" | custom-call | flops 1700000000 | bytes 10000000 | tf_op jit(solution)/shard_map/mix/pallas_call | solution.py:307
  123.1 16.1 %all_to_all.34 = bf16[16,96,256]{2,1,0:T(8,128)(2,1)S(1)} all-to-all(bf16[16,96,256]{2,1,0:T(8,128)(2,1)S(1)} %mix.1), channel_id=1, replica_groups=mesh['z'=16,'g'=2,'p'=2,'x'=4,'c'=2] {'p','x','c'}, dimensions={0} | all-to-all | bytes 1572864 | tf_op jit(solution)/shard_map/all_to_all | solution.py:404
  139.2 0.1 convert_reduce_fusion
  139.3 0.7 add_convert_fusion
  (3 shorter events, 0.0 us)
Async XLA Ops:
  6.5 111.0 %all-gather.2.cloned.1.call-start = ((), (), s32[]{:S(2)}) async-start(), calls=%async_computation.6 | async-start | bytes 8921088 | tf_op jit(solution)/shard_map/all_gather | solution.py:377
  20.2 35.4 %all-to-all-start = ((bf16[16,8,960]{2,1,0:T(8,128)(2,1)}), bf16[16,8,960]{2,1,0:T(8,128)(2,1)S(1)}, u32[]{:S(2)}, u32[]{:S(2)}) async-start(bf16[16,8,960]{2,1,0:T(8,128)(2,1)} %get-tuple-element.10), calls=%async_computation | async-start | bytes 524288 | tf_op jit(solution)/shard_map/all_to_all | solution.py:380
  35.3 8.8 %collective-permute-start = (bf16[256,256]{1,0:T(8,128)(2,1)}, bf16[256,256]{1,0:T(8,128)(2,1)S(1)}, u32[]{:S(2)}, u32[]{:S(2)}) collective-permute-start(bf16[256,256]{1,0:T(8,128)(2,1)} %get-tuple-element.11), channel_id=1, source_target_pairs={{0,1},{1,0},{2,3},{3,2},{4,5},{5,4},{6,7},{7,6},{8,9},{9,8},{10,11... | collective-permute-start | bytes 393224 | tf_op jit(solution)/shard_map/ppermute | solution.py:382
  39.7 61.4 %copy-start.5 = (bf16[192,256]{1,0:T(8,128)(2,1)S(1)}, bf16[192,256]{1,0:T(8,128)(2,1)}, u32[]{:S(2)}) copy-start(bf16[192,256]{1,0:T(8,128)(2,1)} %res_ref.1) | copy-start | bytes 294916
  40.0 0.9 copy-start
  40.9 1.0 copy-start.2
  41.9 0.8 copy-start.3
  42.8 0.9 copy-start.4
  43.7 57.4 %copy-start.1 = (bf16[1024,256]{1,0:T(8,128)(2,1)S(1)}, bf16[1024,256]{1,0:T(8,128)(2,1)}, u32[]{:S(2)}) copy-start(bf16[1024,256]{1,0:T(8,128)(2,1)} %w_ref.1) | copy-start | bytes 1572868
  45.1 22.7 %collective-permute-start.1 = (bf16[2,256,256]{2,1,0:T(8,128)(2,1)S(1)}, bf16[2,256,256]{2,1,0:T(8,128)(2,1)S(1)}, u32[]{:S(2)}, u32[]{:S(2)}) collective-permute-start(bf16[2,256,256]{2,1,0:T(8,128)(2,1)S(1)} %pad_maximum_fusion.w0), channel_id=1, source_target_pairs={{0,2},{2,4},{4,6},{6,0},{1,3},{3,5},{5,7},{7,1},{8,10},{10,12},{12... | collective-permute-start | bytes 786440 | tf_op jit(solution)/shard_map/ppermute | solution.py:385
  48.2 19.6 %collective-permute-start.2 = (bf16[2,256,256]{2,1,0:T(8,128)(2,1)S(1)}, bf16[2,256,256]{2,1,0:T(8,128)(2,1)S(1)}, u32[]{:S(2)}, u32[]{:S(2)}) collective-permute-start(bf16[2,256,256]{2,1,0:T(8,128)(2,1)S(1)} %pad_maximum_fusion.w0), channel_id=1, source_target_pairs={{0,4},{2,6},{4,0},{6,2},{1,5},{3,7},{5,1},{7,3},{8,12},{10,14},{12... | collective-permute-start | bytes 786440 | tf_op jit(solution)/shard_map/ppermute | solution.py:385
  52.5 15.3 %collective-permute-start.3 = (bf16[2,256,256]{2,1,0:T(8,128)(2,1)S(1)}, bf16[2,256,256]{2,1,0:T(8,128)(2,1)S(1)}, u32[]{:S(2)}, u32[]{:S(2)}) collective-permute-start(bf16[2,256,256]{2,1,0:T(8,128)(2,1)S(1)} %pad_maximum_fusion.w0), channel_id=1, source_target_pairs={{0,6},{2,0},{4,2},{6,4},{1,7},{3,1},{5,3},{7,5},{8,14},{10,8},{12,... | collective-permute-start | bytes 786440 | tf_op jit(solution)/shard_map/ppermute | solution.py:385
  55.6 61.9 %copy-start.6 = (f32[2048]{0:T(1024)S(1)}, f32[2048]{0:T(1024)}, u32[]{:S(2)}) copy-start(f32[2048]{0:T(1024)} %param.24) | copy-start | bytes 24580
Sparse Core Ops, SparseCore 0:
  20.4 88.5 all-gather.1

commit v9 on v8

--- a/solution.py
+++ b/solution.py
@@ -255,11 +255,18 @@
 
 
 def mix_kernel(rows_ref, gain_ref, w_hbm, out_ref, n_ref, w_ref, sem):
-    copies = [
-        pltpu.make_async_copy(w_hbm.at[z], w_ref.at[:, pl.ds(z * 128, 128)], sem.at[z])
-        for z in range(NZ)
+    def bring(z, c, part, start, rows):
+        rows = pl.ds(c * 1056 + start, rows)
+        return pltpu.make_async_copy(
+            w_hbm.at[z, rows], w_ref.at[rows, pl.ds(z * 128, 128)], sem.at[z, c, part]
+        )
+
+    waves = [
+        [bring(z, c, 0, 0, 704) for z in range(k * 4, k * 4 + 4) for c in range(NC)]
+        for k in range(4)
     ]
-    for copy in copies:
+    last = [bring(z, c, 1, 704, 352) for z in range(NZ) for c in range(NC)]
+    for copy in waves[0] + waves[1]:
         copy.start()
     for y in range(NP):
         square = jnp.zeros((HALF, 256), jnp.float32)
@@ -275,8 +282,10 @@
     dims = (((1,), (1,)), ((), ()))
     totals = [None] * (2 * NC)
     for chunk in range(4):
-        for copy in copies[chunk * 4 : (chunk + 1) * 4]:
+        for copy in waves[chunk]:
             copy.wait()
+        for copy in (waves[2], waves[3], last, [])[chunk]:
+            copy.start()
         lanes = slice(chunk * 512, (chunk + 1) * 512)
         for k in range(2 * NC):
             start = k // 2 * 1056 + k % 2 * 352
@@ -285,6 +294,8 @@
                 preferred_element_type=jnp.float32,
             )
             totals[k] = part if totals[k] is None else totals[k] + part
+    for copy in last:
+        copy.wait()
     hidden = [
         (totals[2 * c] / (1.0 + jnp.exp(-totals[2 * c])) * totals[2 * c + 1]).astype(jnp.bfloat16)
         for c in range(NC)
@@ -312,7 +323,7 @@
         scratch_shapes=[
             pltpu.VMEM((NP * HALF, 2048), jnp.bfloat16),
             pltpu.VMEM((NC * 1056, 2048), jnp.bfloat16),
-            pltpu.SemaphoreType.DMA((NZ,)),
+            pltpu.SemaphoreType.DMA((NZ, NC, 2)),
         ],
         compiler_params=pltpu.CompilerParams(vmem_limit_bytes=52_000_000),
         cost_estimate=pl.CostEstimate(

time: 147 us -> 148 us (level)
  no operation moved by 1% of the time
where the time goes in v9:
time: 148 us; the launch traced here: 147 us
  blocking collectives  81.6 us (55%)
  starting transfers between devices  29.9 us (20%)
  Pallas kernels  16.7 us (11%)
  between operations  13.6 us (9%)
  local copies, waits for them, and re-layouts  3.7 us (2%)
  other arithmetic  2 us (1%)
    all_to_all x1, blocking collectives, layer(): lax.all_to_all(sent, ('p', 'x', 'c'), split_axis=0, concat_axis=0, tiled=...  16.2 us
    all_to_all x1, blocking collectives, layer(): lax.all_to_all(partial_sums, ('p', 'x', 'c'), split_axis=0, concat_axis=0...  16.1 us
    all_to_all x1, blocking collectives, layer(): lax.all_to_all(parts, ('x', 'c'), split_axis=0, concat_axis=0, tiled=True)  15.1 us
    all_to_all x1, starting transfers between devices, layer(): lat = lax.all_to_all(own, 'z', split_axis=0, concat_axis=0, tiled=True)  15.1 us
    all_gather x1, blocking collectives, layer(): lat = lax.all_gather(lat, ('g', 'p'), axis=0, tiled=True)  12.2 us
    all_to_all x1, blocking collectives, layer(): lax.all_to_all(merge(parts), ('x', 'c'), split_axis=0, concat_axis=0, til...  11.3 us
    all_to_all x1, blocking collectives, layer(): lax.all_to_all(cut, ('g', 'p'), split_axis=0, concat_axis=0, tiled=True)  10.7 us
    ppermute x3, starting transfers between devices, layer(): lax.ppermute(pair, 'x', [(i, (i + s) % NX) for i in range(NX)])  10.5 us
  transfers between devices with their start and end apart: 6, of which 0 were waited for; matrix products, arithmetic and copies ran while one was open for 1% of the time, Pallas kernels for 5%

profile of v9, /device:TPU:1, one launch (start us, length us, event | category | flops | bytes accessed | tf_op | source)
XLA Modules:
  0.0 147.5 jit_solution(13315772894101224157)
XLA Ops:
  6.5 0.0 all-gather.2.cloned.1.call-start
  6.5 2.1 %prepare.1 = (bf16[16,8,960]{2,1,0:T(8,128)(2,1)}, bf16[256,256]{1,0:T(8,128)(2,1)}, bf16[4,32,1056]{2,1,0:T(8,128)(2,1)}) custom-call(bf16[24,256]{1,0:T(8,128)(2,1)} %lat_ref.1, bf16[24,64]{1,0:T(8,128)(2,1)} %rot_ref.1, f32[1,256]{1,0:T(1,128)} %bitcast.18, f32[64,256]{1,0:T(8,128)} %constant.128.clone.block_ref, f32[192,256]{1,0:T(8,128)} %constant.129.clone.inside_ref, ...), custom_call_target="tpu_custom_call" | custom-call | flops 100000 | bytes 300000 | tf_op jit(solution)/shard_map/prepare/pallas_call | solution.py:78
  8.6 10.7 %all_to_all.30.in_ref = bf16[4,32,1056]{2,1,0:T(8,128)(2,1)S(1)} all-to-all(bf16[4,32,1056]{2,1,0:T(8,128)(2,1)} %get-tuple-element.14), channel_id=1, replica_groups=mesh['z'=16,'g'=2,'p'=2,'x'=4,'c'=2] {'g','p'}, dimensions={0} | all-to-all | bytes 540672 | tf_op jit(solution)/shard_map/all_to_all | solution.py:387
  19.3 0.9 put.1
  20.2 0.0 all-gather.2.cloned.1.call-update
  20.2 15.1 %all-to-all-start = ((bf16[16,8,960]{2,1,0:T(8,128)(2,1)}), bf16[16,8,960]{2,1,0:T(8,128)(2,1)S(1)}, u32[]{:S(2)}, u32[]{:S(2)}) async-start(bf16[16,8,960]{2,1,0:T(8,128)(2,1)} %get-tuple-element.10), calls=%async_computation | async-start | bytes 524288 | tf_op jit(solution)/shard_map/all_to_all | solution.py:391
  35.3 4.3 %collective-permute-start = (bf16[256,256]{1,0:T(8,128)(2,1)}, bf16[256,256]{1,0:T(8,128)(2,1)S(1)}, u32[]{:S(2)}, u32[]{:S(2)}) collective-permute-start(bf16[256,256]{1,0:T(8,128)(2,1)} %get-tuple-element.11), channel_id=1, source_target_pairs={{0,1},{1,0},{2,3},{3,2},{4,5},{5,4},{6,7},{7,6},{8,9},{9,8},{10,11... | collective-permute-start | bytes 393224 | tf_op jit(solution)/shard_map/ppermute | solution.py:393
  39.7 0.0 copy-start.5
  39.7 0.3 select_convert_fusion.seg_ref
  40.0 0.0 copy-start
  40.0 0.9 copy-done
  40.9 0.0 copy-start.2
  40.9 1.0 copy-done.2
  41.9 0.0 copy-start.3
  41.9 0.8 copy-done.3
  42.8 0.0 copy-start.4
  42.8 0.9 copy-done.4
  43.7 0.0 copy-start.1
  43.7 0.4 turn.1.q_ref
  44.1 0.0 collective-permute-done
  44.1 0.9 pad_maximum_fusion.w0
  45.1 3.1 %collective-permute-start.1 = (bf16[2,256,256]{2,1,0:T(8,128)(2,1)S(1)}, bf16[2,256,256]{2,1,0:T(8,128)(2,1)S(1)}, u32[]{:S(2)}, u32[]{:S(2)}) collective-permute-start(bf16[2,256,256]{2,1,0:T(8,128)(2,1)S(1)} %pad_maximum_fusion.w0), channel_id=1, source_target_pairs={{0,2},{2,4},{4,6},{6,0},{1,3},{3,5},{5,7},{7,1},{8,10},{10,12},{12... | collective-permute-start | bytes 786440 | tf_op jit(solution)/shard_map/ppermute | solution.py:396
  48.2 4.4 %collective-permute-start.2 = (bf16[2,256,256]{2,1,0:T(8,128)(2,1)S(1)}, bf16[2,256,256]{2,1,0:T(8,128)(2,1)S(1)}, u32[]{:S(2)}, u32[]{:S(2)}) collective-permute-start(bf16[2,256,256]{2,1,0:T(8,128)(2,1)S(1)} %pad_maximum_fusion.w0), channel_id=1, source_target_pairs={{0,4},{2,6},{4,0},{6,2},{1,5},{3,7},{5,1},{7,3},{8,12},{10,14},{12... | collective-permute-start | bytes 786440 | tf_op jit(solution)/shard_map/ppermute | solution.py:396
  52.5 3.1 %collective-permute-start.3 = (bf16[2,256,256]{2,1,0:T(8,128)(2,1)S(1)}, bf16[2,256,256]{2,1,0:T(8,128)(2,1)S(1)}, u32[]{:S(2)}, u32[]{:S(2)}) collective-permute-start(bf16[2,256,256]{2,1,0:T(8,128)(2,1)S(1)} %pad_maximum_fusion.w0), channel_id=1, source_target_pairs={{0,6},{2,0},{4,2},{6,4},{1,7},{3,1},{5,3},{7,5},{8,14},{10,8},{12,... | collective-permute-start | bytes 786440 | tf_op jit(solution)/shard_map/ppermute | solution.py:396
  55.6 0.0 all-to-all-done
  55.6 0.0 copy-start.6
  55.6 12.2 %all_gather.6.lat_ref = bf16[512,960]{1,0:T(8,128)(2,1)S(1)} all-gather(bf16[128,960]{1,0:T(8,128)(2,1)S(1)} %bitcast.14), channel_id=1, replica_groups=mesh['z'=16,'g'=2,'p'=2,'x'=4,'c'=2] {'g','p'}, dimensions={0}, use_global_device_ids=true | all-gather | bytes 1228800 | tf_op jit(solution)/shard_map/all_gather | solution.py:399
  67.8 0.0 collective-permute-done.1.w1
  67.8 0.0 collective-permute-done.2.w2
  67.8 0.0 collective-permute-done.3.w3
  67.8 6.2 %attend.1 = bf16[8,208,128]{2,1,0:T(8,128)(2,1)S(1)} custom-call(bf16[8,192,256]{2,1,0:T(8,128)(2,1)S(1)} %turn.1.q_ref, bf16[512,960]{1,0:T(8,128)(2,1)S(1)} %all_gather.6.lat_ref, bf16[1536,128]{1,0:T(8,128)(2,1)S(1)} %select_convert_fusion.seg_ref, bf16[2,256,256]{2,1,0:T(8,128)(2,1)S(1)} %pad_maximum_fusion.w0, ...), custom_call_target="tpu_custom_call" | custom-call | flops 3000000000 | bytes 4000000 | tf_op jit(solution)/shard_map/attend/pallas_call | solution.py:207
  74.0 15.1 %all_to_all.31.in_ref = bf16[8,208,128]{2,1,0:T(8,128)(2,1)S(1)} all-to-all(bf16[8,208,128]{2,1,0:T(8,128)(2,1)S(1)} %attend.1), channel_id=1, replica_groups=mesh['z'=16,'g'=2,'p'=2,'x'=4,'c'=2] {'x','c'}, dimensions={0} | all-to-all | bytes 851968 | tf_op jit(solution)/shard_map/all_to_all | solution.py:410
  89.1 0.6 merge.1
  89.7 11.3 %all_to_all.32.heads_ref = bf16[8,192,128]{2,1,0:T(8,128)(2,1)S(1)} all-to-all(bf16[8,192,128]{2,1,0:T(8,128)(2,1)S(1)} %merge.1), channel_id=1, replica_groups=mesh['z'=16,'g'=2,'p'=2,'x'=4,'c'=2] {'x','c'}, dimensions={0} | all-to-all | bytes 786432 | tf_op jit(solution)/shard_map/all_to_all | solution.py:411
  101.1 0.0 copy-done.5
  101.1 0.0 copy-done.1
  101.1 0.3 project.1
  101.4 16.2 %all_to_all.33.rows_ref = bf16[16,96,256]{2,1,0:T(8,128)(2,1)S(1)} all-to-all(bf16[16,96,256]{2,1,0:T(8,128)(2,1)S(1)} %get-tuple-element.13), channel_id=1, replica_groups=mesh['z'=16,'g'=2,'p'=2,'x'=4,'c'=2] {'p','x','c'}, dimensions={0} | all-to-all | bytes 1572864 | tf_op jit(solution)/shard_map/all_to_all | solution.py:413
  117.5 0.0 all-gather.2.cloned.1.call-done
  117.5 0.0 copy-done.6
  117.5 6.3 %mix.1 = bf16[16,96,256]{2,1,0:T(8,128)(2,1)S(1)} custom-call(bf16[16,96,256]{2,1,0:T(8,128)(2,1)S(1)} %all_to_all.33.rows_ref, f32[1,2048]{1,0:T(1,128)S(1)} %bitcast.11, bf16[16,2112,128]{2,1,0:T(8,128)(2,1)} %bitcast.12), custom_call_target="tpu_custom_call" | custom-call | flops 1700000000 | bytes 10000000 | tf_op jit(solution)/shard_map/mix/pallas_call | solution.py:318
  123.8 16.1 %all_to_all.34 = bf16[16,96,256]{2,1,0:T(8,128)(2,1)S(1)} all-to-all(bf16[16,96,256]{2,1,0:T(8,128)(2,1)S(1)} %mix.1), channel_id=1, replica_groups=mesh['z'=16,'g'=2,'p'=2,'x'=4,'c'=2] {'p','x','c'}, dimensions={0} | all-to-all | bytes 1572864 | tf_op jit(solution)/shard_map/all_to_all | solution.py:415
  139.9 0.1 convert_reduce_fusion
  140.0 0.7 add_convert_fusion
  (3 shorter events, 0.0 us)
Async XLA Ops:
  6.5 111.0 %all-gather.2.cloned.1.call-start = ((), (), s32[]{:S(2)}) async-start(), calls=%async_computation.6 | async-start | bytes 8921088 | tf_op jit(solution)/shard_map/all_gather | solution.py:388
  20.2 35.4 %all-to-all-start = ((bf16[16,8,960]{2,1,0:T(8,128)(2,1)}), bf16[16,8,960]{2,1,0:T(8,128)(2,1)S(1)}, u32[]{:S(2)}, u32[]{:S(2)}) async-start(bf16[16,8,960]{2,1,0:T(8,128)(2,1)} %get-tuple-element.10), calls=%async_computation | async-start | bytes 524288 | tf_op jit(solution)/shard_map/all_to_all | solution.py:391
  35.3 8.8 %collective-permute-start = (bf16[256,256]{1,0:T(8,128)(2,1)}, bf16[256,256]{1,0:T(8,128)(2,1)S(1)}, u32[]{:S(2)}, u32[]{:S(2)}) collective-permute-start(bf16[256,256]{1,0:T(8,128)(2,1)} %get-tuple-element.11), channel_id=1, source_target_pairs={{0,1},{1,0},{2,3},{3,2},{4,5},{5,4},{6,7},{7,6},{8,9},{9,8},{10,11... | collective-permute-start | bytes 393224 | tf_op jit(solution)/shard_map/ppermute | solution.py:393
  39.7 61.4 %copy-start.5 = (bf16[192,256]{1,0:T(8,128)(2,1)S(1)}, bf16[192,256]{1,0:T(8,128)(2,1)}, u32[]{:S(2)}) copy-start(bf16[192,256]{1,0:T(8,128)(2,1)} %res_ref.1) | copy-start | bytes 294916
  40.0 0.9 copy-start
  40.9 1.0 copy-start.2
  41.9 0.8 copy-start.3
  42.8 0.9 copy-start.4
  43.7 57.4 %copy-start.1 = (bf16[1024,256]{1,0:T(8,128)(2,1)S(1)}, bf16[1024,256]{1,0:T(8,128)(2,1)}, u32[]{:S(2)}) copy-start(bf16[1024,256]{1,0:T(8,128)(2,1)} %w_ref.1) | copy-start | bytes 1572868
  45.1 22.7 %collective-permute-start.1 = (bf16[2,256,256]{2,1,0:T(8,128)(2,1)S(1)}, bf16[2,256,256]{2,1,0:T(8,128)(2,1)S(1)}, u32[]{:S(2)}, u32[]{:S(2)}) collective-permute-start(bf16[2,256,256]{2,1,0:T(8,128)(2,1)S(1)} %pad_maximum_fusion.w0), channel_id=1, source_target_pairs={{0,2},{2,4},{4,6},{6,0},{1,3},{3,5},{5,7},{7,1},{8,10},{10,12},{12... | collective-permute-start | bytes 786440 | tf_op jit(solution)/shard_map/ppermute | solution.py:396
  48.2 19.6 %collective-permute-start.2 = (bf16[2,256,256]{2,1,0:T(8,128)(2,1)S(1)}, bf16[2,256,256]{2,1,0:T(8,128)(2,1)S(1)}, u32[]{:S(2)}, u32[]{:S(2)}) collective-permute-start(bf16[2,256,256]{2,1,0:T(8,128)(2,1)S(1)} %pad_maximum_fusion.w0), channel_id=1, source_target_pairs={{0,4},{2,6},{4,0},{6,2},{1,5},{3,7},{5,1},{7,3},{8,12},{10,14},{12... | collective-permute-start | bytes 786440 | tf_op jit(solution)/shard_map/ppermute | solution.py:396
  52.5 15.3 %collective-permute-start.3 = (bf16[2,256,256]{2,1,0:T(8,128)(2,1)S(1)}, bf16[2,256,256]{2,1,0:T(8,128)(2,1)S(1)}, u32[]{:S(2)}, u32[]{:S(2)}) collective-permute-start(bf16[2,256,256]{2,1,0:T(8,128)(2,1)S(1)} %pad_maximum_fusion.w0), channel_id=1, source_target_pairs={{0,6},{2,0},{4,2},{6,4},{1,7},{3,1},{5,3},{7,5},{8,14},{10,8},{12,... | collective-permute-start | bytes 786440 | tf_op jit(solution)/shard_map/ppermute | solution.py:396
  55.6 61.9 %copy-start.6 = (f32[2048]{0:T(1024)S(1)}, f32[2048]{0:T(1024)}, u32[]{:S(2)}) copy-start(f32[2048]{0:T(1024)} %param.24) | copy-start | bytes 24580
Sparse Core Ops, SparseCore 0:
  20.4 88.5 all-gather.1
